TPU v7x, 256 devices: a whole 4x4x8 slice. The times are simulated.
256 devices in a mesh: sp: 32 (over z, y), tp: 8 (over x, core).
Axes of the slice: x: 4, y: 4, z: 8, core: 2. Of those that a mesh axis runs over, the one named last changes fastest.
Arguments:
- hidden: bfloat16 [4096, 2048], P('sp'), may hold values from -6 to 6
- value_weight: bfloat16 [2048, 4096], P(None, 'tp'), may hold values from -0.125 to 0.125
- key_vecs: bfloat16 [4096, 8, 128], P('sp', 'tp'), may hold values from -0.29882812 to 0.29882812
- queries: bfloat16 [4096, 8, 128], P('sp', 'tp'), may hold values from -0.29882812 to 0.29882812
- decay_pre: float32 [4096, 64], P('sp', 'tp'), may hold values from -4 to 4
- decay_rate: float32 [64], P('tp'), may hold values from 1.4648437e-05 to 0.0009033203
- cotangent: bfloat16 [4096, 64, 64], P('sp', 'tp'), may hold values from -1.1953125 to 1.1953125
Outputs:
- grad_keys: bfloat16 [4096, 8, 128], P('sp', 'tp')
- grad_queries: bfloat16 [4096, 8, 128], P('sp', 'tp')
- grad_decay: float32 [4096, 64], P('sp', 'tp')
- grad_hidden: bfloat16 [4096, 2048], P(('sp', 'tp'))
- grad_weight: float32 [2048, 4096], P('sp', 'tp')
All inputs are finite; a program needn't handle non-finite values.
Results may differ from a plain program's by a relative error of at most 0.003.
Values sent between devices are 32-bit elements.
A program may use at most 64 MiB of HBM per device.

v0:
```python
import functools

import jax
import jax.numpy as jnp
from jax import lax
from jax.experimental import pallas as pl
from jax.experimental.pallas import tpu as pltpu
from jax.sharding import PartitionSpec as P

MESH = pl.DeviceIdType.MESH
F32 = jnp.float32
BF16 = jnp.bfloat16


def inner_size(count):
    size = 1
    while size * size * 4 <= count:
        size *= 2
    while count % size:
        size -= 1
    return size


def remote(src, dst, send, recv, axis, index):
    return pltpu.make_async_remote_copy(
        src_ref=src, dst_ref=dst, send_sem=send, recv_sem=recv, device_id={axis: index}, device_id_type=MESH
    )


def scan_kernel(ny, nz, ntp, skew, pieces, both_ref, dec_ref, hid_ref, out_ref, hcol_ref,
                ybuf, ydec, pin, pout, hid_f, hland,
                ysend, yrecv, dsend, drecv, psend, precv, hsend, hrecv, fsend, frecv):
    me = lax.axis_index("sp")
    z, y = me // ny, me % ny
    heads = both_ref.shape[0]
    span = hland.shape[2]

    barrier = pltpu.get_barrier_semaphore()
    for dy in range(1, ny):
        pl.semaphore_signal(barrier, inc=1, device_id={"sp": z * ny + (y + dy) % ny}, device_id_type=MESH)
    for dz in range(1, nz):
        pl.semaphore_signal(barrier, inc=1, device_id={"sp": ((z + dz) % nz) * ny + y}, device_id_type=MESH)
    mine = lax.axis_index("tp")
    halves = 2 if ntp % 2 == 0 else 1
    half = mine % halves
    other = mine + 1 - 2 * half
    if halves == 2:
        pl.semaphore_signal(barrier, inc=1, device_id={"tp": other}, device_id_type=MESH)
    pl.semaphore_wait(barrier, ny - 1 + nz - 1 + halves - 1)
    half_rows = hland.shape[1] // halves
    piece_rows = half_rows // pieces

    def ycopy(h, dy):
        there = (y + dy) % ny
        return remote(both_ref.at[h], ybuf.at[y, h], ysend.at[there, h], yrecv.at[y, h], "sp", z * ny + there)

    def yarrive(h, there):
        return remote(both_ref.at[h], ybuf.at[there, h], ysend.at[there, h], yrecv.at[there, h], "sp", z * ny + there)

    def dcopy(dy):
        there = (y + dy) % ny
        return remote(dec_ref, ydec.at[y], dsend.at[there], drecv.at[y], "sp", z * ny + there)

    def darrive(dy):
        there = (y + dy) % ny
        return remote(dec_ref, ydec.at[there], dsend.at[there], drecv.at[there], "sp", z * ny + there)

    for dy in range(1, ny):
        dcopy(dy).start()

    def launch(h, carry):
        for dy in range(1, ny):
            ycopy(h, dy).start()
        return carry

    lax.fori_loop(0, heads, launch, 0)

    def piece(p):
        return pl.ds(pl.multiple_of(half * half_rows + p * piece_rows, 8), piece_rows)

    def columns_of(plane):
        return pl.ds(pl.multiple_of(plane * span, 128), span)

    def hcopy(dz, p):
        there = (z + dz) % nz
        return remote(
            hid_f.at[piece(p), columns_of(there)], hland.at[z, piece(p)],
            hsend.at[there, p], hrecv.at[z, p], "sp", there * ny + y,
        )

    def harrive(dz, p):
        there = (z + dz) % nz
        return remote(
            hid_f.at[piece(p), columns_of(there)], hland.at[there, piece(p)],
            hsend.at[there, p], hrecv.at[there, p], "sp", there * ny + y,
        )

    def share(dz, part):
        there = (z + dz) % nz
        block = hland.at[there, pl.ds(pl.multiple_of(part * half_rows, 8), half_rows)]
        return remote(block, block, fsend.at[there], frecv.at[there], "tp", other)

    hid_f[...] = hid_ref[...].astype(F32)
    ybuf[y] = both_ref[...]
    ydec[y] = dec_ref[...]
    for dy in range(1, ny):
        darrive(dy).wait_recv()

    @pl.when(z == 0)
    def _():
        pin[0] = jnp.zeros_like(pin[0])

    @pl.when(z == nz - 1)
    def _():
        pin[1] = jnp.zeros_like(pin[1])

    def up(h):
        return remote(pout.at[0, h], pin.at[0, h], psend.at[0, h], precv.at[0, h], "sp", me + ny)

    def down(h):
        return remote(pout.at[1, h], pin.at[1, h], psend.at[1, h], precv.at[1, h], "sp", me - ny)

    def ready(h, first):
        @pl.when(first)
        def _():
            for dy in range(1, ny):
                yarrive(h, (y + dy) % ny).wait_recv()

    def step(t, carry):
        a = t - skew * z
        b = t - skew * (nz - 1 - z)

        @pl.when((a >= 0) & (a < heads))
        def _():
            ready(a, (2 * z <= nz - 1))

            @pl.when(z > 0)
            def _():
                up(a).wait_recv()

            now = pin[0, a]
            for yy in range(ny):
                @pl.when(y == yy)
                def _():
                    out_ref[a, 0] = now

                now = ydec[yy, a] * now + ybuf[yy, a, 0]
            pout[0, a] = now

            @pl.when(z < nz - 1)
            def _():
                up(a).start()

        @pl.when((b >= 0) & (b < heads))
        def _():
            ready(b, (2 * z > nz - 1))

            @pl.when(z < nz - 1)
            def _():
                down(b).wait_recv()

            now = pin[1, b]
            for yy in reversed(range(ny)):
                @pl.when(y == yy)
                def _():
                    out_ref[b, 1] = now

                now = ydec[yy, b] * now + ybuf[yy, b, 1]
            pout[1, b] = now

            @pl.when(z > 0)
            def _():
                down(b).start()

        @pl.when(t < pieces * (nz - 1))
        def _():
            hcopy(1 + t // pieces, t % pieces).start()

        return carry

    lax.fori_loop(0, max(heads + skew * (nz - 1), pieces * (nz - 1)), step, 0)

    for dz in range(1, nz):
        for p in range(pieces):
            harrive(dz, p).wait_recv()
        if halves == 2:
            share(dz, half).start()

    hcol_ref[pl.ds(pl.multiple_of(z * hland.shape[1], 128), hland.shape[1]), :] = (
        hid_f[:, pl.ds(pl.multiple_of(z * span, 128), span)].astype(BF16)
    )
    for dz in range(1, nz):
        there = (z + dz) % nz
        if halves == 2:
            share(dz, 1 - half).wait_recv()
        hcol_ref[pl.ds(pl.multiple_of(there * hland.shape[1], 128), hland.shape[1]), :] = hland[there].astype(BF16)
    for dz in range(1, nz):
        for p in range(pieces):
            hcopy(dz, p).wait_send()
        if halves == 2:
            share(dz, half).wait_send()
    for dy in range(1, ny):
        dcopy(dy).wait_send()

    def drain(h, carry):
        for dy in range(1, ny):
            ycopy(h, dy).wait_send()

        @pl.when(z < nz - 1)
        def _():
            up(h).wait_send()

        @pl.when(z > 0)
        def _():
            down(h).wait_send()

        return carry

    lax.fori_loop(0, heads, drain, 0)


def grads_kernel(ny, nz, ntp, width, gv_ref, hct_ref, ghp_ref, gw_ref, gh_ref,
                 gath, part, land, ghland,
                 upsend, dnsend, grecv, ysend, yrecv, hsend, hrecv):
    me = lax.axis_index("sp")
    mine = lax.axis_index("tp")
    z, y = me // ny, me % ny
    rows = gw_ref.shape[0]
    chunks = gv_ref.shape[1] // width
    length = gv_ref.shape[0]
    own_rows = gh_ref.shape[0]

    barrier = pltpu.get_barrier_semaphore()
    for dy in range(1, ny):
        pl.semaphore_signal(barrier, inc=1, device_id={"sp": z * ny + (y + dy) % ny}, device_id_type=MESH)
    for dz in (1, nz - 1):
        pl.semaphore_signal(barrier, inc=1, device_id={"sp": ((z + dz) % nz) * ny + y}, device_id_type=MESH)
    for dt in range(1, ntp):
        pl.semaphore_signal(barrier, inc=1, device_id={"tp": (mine + dt) % ntp}, device_id_type=MESH)
    pl.semaphore_wait(barrier, ny - 1 + 2 + ntp - 1)

    def cols(c):
        return pl.ds(pl.multiple_of(c * width, 128), width)

    def up(b, c):
        return remote(gath.at[b, c], gath.at[b, c], upsend.at[b, c], grecv.at[b, c], "sp", me + ny)

    def down(b, c):
        return remote(gath.at[b, c], gath.at[b, c], dnsend.at[b, c], grecv.at[b, c], "sp", me - ny)

    def launch(c, carry):
        gath[z, c] = gv_ref[:, cols(c)]

        @pl.when(z < nz - 1)
        def _():
            up(z, c).start()

        @pl.when(z > 0)
        def _():
            down(z, c).start()

        return carry

    ahead = min(5, chunks)
    lax.fori_loop(0, ahead, launch, 0)

    def hcopy(dt):
        there = (mine + dt) % ntp
        return remote(
            ghp_ref.at[pl.ds(pl.multiple_of(there * own_rows, 8), own_rows), :], ghland.at[mine],
            hsend.at[there], hrecv.at[mine], "tp", there,
        )

    def harrive(dt):
        there = (mine + dt) % ntp
        return remote(
            ghp_ref.at[pl.ds(pl.multiple_of(there * own_rows, 8), own_rows), :], ghland.at[there],
            hsend.at[there], hrecv.at[there], "tp", there,
        )

    for dt in range(1, ntp):
        hcopy(dt).start()

    def ycopy(c, there):
        return remote(
            part.at[there, c], land.at[y, c], ysend.at[there, c], yrecv.at[y, c], "sp", z * ny + there
        )

    def yarrive(c, there):
        return remote(
            part.at[there, c], land.at[there, c], ysend.at[there, c], yrecv.at[there, c], "sp", z * ny + there
        )

    def work(c, carry):
        for d in range(1, nz):
            low, high = z - d, z + d

            @pl.when(low >= 0)
            def _():
                down(jnp.maximum(low, 0), c).wait_recv()

                @pl.when(z < nz - 1)
                def _():
                    up(jnp.maximum(low, 0), c).start()

            @pl.when(high < nz)
            def _():
                up(jnp.minimum(high, nz - 1), c).wait_recv()

                @pl.when(z > 0)
                def _():
                    down(jnp.minimum(high, nz - 1), c).start()

        @pl.when(c + ahead < chunks)
        def _():
            launch(c + ahead, 0)

        block = gath[:, c].reshape(nz * length, width).astype(BF16)
        for dy in range(1, ny):
            there = (y + dy) % ny
            part[there, c] = jnp.dot(
                hct_ref[pl.ds(pl.multiple_of(there * rows, 8), rows), :], block, preferred_element_type=F32
            )
            ycopy(c, there).start()
        gw_ref[:, cols(c)] = jnp.dot(
            hct_ref[pl.ds(pl.multiple_of(y * rows, 8), rows), :], block, preferred_element_type=F32
        )
        return carry

    lax.fori_loop(0, chunks, work, 0)

    total = ghp_ref[pl.ds(pl.multiple_of(mine * own_rows, 8), own_rows), :]
    for dt in range(1, ntp):
        harrive(dt).wait_recv()
        total = total + ghland[(mine + dt) % ntp]
    gh_ref[...] = total.astype(gh_ref.dtype)

    def collect(c, carry):
        for dy in range(1, ny):
            there = (y + dy) % ny
            yarrive(c, there).wait_recv()
            gw_ref[:, cols(c)] += land[there, c]
        return carry

    lax.fori_loop(0, chunks, collect, 0)

    def drain(c, carry):
        for dy in range(1, ny):
            ycopy(c, (y + dy) % ny).wait_send()
        for b in range(nz):
            @pl.when((b <= z) & (z < nz - 1))
            def _():
                up(b, c).wait_send()

            @pl.when((b >= z) & (z > 0))
            def _():
                down(b, c).wait_send()

        return carry

    lax.fori_loop(0, chunks, drain, 0)
    for dt in range(1, ntp):
        hcopy(dt).wait_send()


VM = pl.BlockSpec(memory_space=pltpu.VMEM)
LIMIT = 48 * 1024 * 1024


def split(x):
    hi = lax.reduce_precision(x, 8, 7)
    return hi.astype(BF16), (x - hi).astype(BF16)


def two_pass(spec, x, y):
    hi, lo = split(x)
    return jnp.einsum(spec, hi, y, preferred_element_type=F32) + jnp.einsum(spec, lo, y, preferred_element_type=F32)


def per_device(sp, tp, hidden, value_weight, key_vecs, queries, decay_pre, decay_rate, cotangent):
    length = hidden.shape[0]
    heads = decay_rate.shape[0]
    head_width = cotangent.shape[2]
    groups = key_vecs.shape[1]
    state = key_vecs.shape[2]
    per = heads // groups
    features = hidden.shape[1]
    columns = value_weight.shape[1]
    ny = inner_size(sp)
    nz = sp // ny
    values = jnp.dot(hidden, value_weight, preferred_element_type=F32).astype(BF16)
    v = values.reshape(length, groups, per, head_width)
    cot = cotangent.reshape(length, groups, per, head_width)
    log_decay = -decay_rate[None, :] * jax.nn.softplus(decay_pre)
    tri = jnp.tril(jnp.ones((length, length), F32))
    cum = jnp.dot(tri, log_decay, precision=lax.Precision.HIGHEST)
    tot = cum[-1]
    to_end = jnp.exp(tot[None] - cum).reshape(length, groups, per, 1)
    ecum = jnp.exp(cum).reshape(length, groups, per, 1)
    local_state = two_pass("sgip,sgn->gipn", to_end * v.astype(F32), key_vecs)
    local_pull = two_pass("sgip,sgn->gipn", ecum * cot.astype(F32), queries)
    both = jnp.stack([local_state, local_pull], axis=2).reshape(heads, 2, head_width, state)
    dec = jnp.broadcast_to(jnp.exp(tot)[:, None, None], (heads, 1, state))
    span = features // nz
    pieces = 4
    scanned, hcol = pl.pallas_call(
        functools.partial(scan_kernel, ny, nz, tp, 4, pieces),
        out_shape=(
            jax.ShapeDtypeStruct(both.shape, F32),
            jax.ShapeDtypeStruct((nz * length, span), BF16),
        ),
        in_specs=[VM] * 3,
        out_specs=(VM, VM),
        scratch_shapes=[
            pltpu.VMEM((ny,) + both.shape, F32),
            pltpu.VMEM((ny,) + dec.shape, F32),
            pltpu.VMEM((2, heads, head_width, state), F32),
            pltpu.VMEM((2, heads, head_width, state), F32),
            pltpu.VMEM((length, features), F32),
            pltpu.VMEM((nz, length, span), F32),
            pltpu.SemaphoreType.DMA((ny, heads)),
            pltpu.SemaphoreType.DMA((ny, heads)),
            pltpu.SemaphoreType.DMA((ny,)),
            pltpu.SemaphoreType.DMA((ny,)),
            pltpu.SemaphoreType.DMA((2, heads)),
            pltpu.SemaphoreType.DMA((2, heads)),
            pltpu.SemaphoreType.DMA((nz, pieces)),
            pltpu.SemaphoreType.DMA((nz, pieces)),
            pltpu.SemaphoreType.DMA((nz,)),
            pltpu.SemaphoreType.DMA((nz,)),
        ],
        compiler_params=pltpu.CompilerParams(collective_id=0, has_side_effects=True, vmem_limit_bytes=LIMIT),
        name="scan_states",
    )(both, dec, hidden)
    state_in = scanned[:, 0].reshape(groups, per, head_width, state)
    state_grad = scanned[:, 1].reshape(groups, per, head_width, state)

    cum_h = cum.T
    causal = jnp.tril(jnp.ones((length, length), dtype=bool))[None]
    across = cum_h[:, :, None] - cum_h[:, None, :]
    damping = jnp.where(causal, jnp.exp(jnp.where(causal, across, 0.0)), 0.0).reshape(groups, per, length, length)
    scores = jnp.einsum("tgn,sgn->gts", queries, key_vecs, preferred_element_type=F32)
    pair = jnp.einsum("tgip,sgip->gits", cot, v, preferred_element_type=F32)
    dscore = pair * damping
    flux = dscore * scores[:, None]
    net = (jnp.sum(flux, axis=3) - jnp.sum(flux, axis=2)).reshape(heads, length).T
    dsum = jnp.sum(dscore, axis=1)
    mixed = scores[:, None] * damping
    gq_heads = ecum * two_pass("gipn,tgip->tgin", state_in, cot)
    gk_heads = to_end * two_pass("gipn,tgip->tgin", state_grad, v)
    gv = two_pass("gits,tgip->sgip", mixed, cot) + to_end * two_pass(
        "gipn,sgn->sgip", state_grad, key_vecs
    )
    gq = two_pass("gts,sgn->tgn", dsum, key_vecs) + jnp.sum(gq_heads, axis=2)
    gk = two_pass("gts,tgn->sgn", dsum, queries) + jnp.sum(gk_heads, axis=2)
    qgq = jnp.sum(gq_heads * queries.astype(F32)[:, :, None], axis=3).reshape(length, heads)
    kgk = jnp.sum(gk_heads * key_vecs.astype(F32)[:, :, None], axis=3).reshape(length, heads)
    through = jnp.exp(tot) * jnp.sum(state_in * state_grad, axis=(2, 3)).reshape(heads)
    suffix = jnp.dot(tri.T, net + qgq, precision=lax.Precision.HIGHEST)
    prefix = jnp.dot(tri - jnp.eye(length, dtype=F32), kgk, precision=lax.Precision.HIGHEST)
    grad_decay = (suffix + prefix + through[None]) * -decay_rate[None] * jax.nn.sigmoid(decay_pre)

    grad_flat = gv.reshape(length, columns).astype(BF16)
    ghp = lax.dot_general(grad_flat, value_weight, (((1,), (1,)), ((), ())), preferred_element_type=F32)
    rows = features // sp
    width = min(columns, 128)
    chunks = columns // width
    grad_weight, grad_hidden = pl.pallas_call(
        functools.partial(grads_kernel, ny, nz, tp, width),
        out_shape=(
            jax.ShapeDtypeStruct((rows, columns), F32),
            jax.ShapeDtypeStruct((length // tp, features), BF16),
        ),
        in_specs=[VM] * 3,
        out_specs=(VM, VM),
        scratch_shapes=[
            pltpu.VMEM((nz, chunks, length, width), F32),
            pltpu.VMEM((ny, chunks, rows, width), F32),
            pltpu.VMEM((ny, chunks, rows, width), F32),
            pltpu.VMEM((tp, length // tp, features), F32),
            pltpu.SemaphoreType.DMA((nz, chunks)),
            pltpu.SemaphoreType.DMA((nz, chunks)),
            pltpu.SemaphoreType.DMA((nz, chunks)),
            pltpu.SemaphoreType.DMA((ny, chunks)),
            pltpu.SemaphoreType.DMA((ny, chunks)),
            pltpu.SemaphoreType.DMA((tp,)),
            pltpu.SemaphoreType.DMA((tp,)),
        ],
        compiler_params=pltpu.CompilerParams(collective_id=1, has_side_effects=True, vmem_limit_bytes=LIMIT),
        name="weight_grads",
    )(grad_flat.astype(F32), hcol.T, ghp)
    return (gq_cast(gk), gq_cast(gq), grad_decay, grad_hidden, grad_weight)


def gq_cast(x):
    return x.astype(BF16)


def solution(mesh):
    return jax.shard_map(
        functools.partial(per_device, mesh.shape["sp"], mesh.shape["tp"]),
        mesh=mesh,
        in_specs=(
            P("sp", None),
            P(None, "tp"),
            P("sp", "tp", None),
            P("sp", "tp", None),
            P("sp", "tp"),
            P("tp"),
            P("sp", "tp", None),
        ),
        out_specs=(
            P("sp", "tp", None),
            P("sp", "tp", None),
            P("sp", "tp"),
            P(("sp", "tp"), None),
            P("sp", "tp"),
        ),
        check_vma=False,
    )
```

profile of v0, /device:TPU:2, one launch (start us, length us, event | category | flops | bytes accessed | tf_op | source)
XLA Modules:
  0.0 175.8 jit_solution(18169284273339646527)
XLA Ops:
  0.6 1.1 fusion.70
  1.7 0.7 neg.12
  2.4 0.9 fusion.56
  3.8 2.2 %fusion.26 = (bf16[128,512]{1,0:T(8,128)(2,1)}, bf16[128,512]{1,0:T(8,128)(2,1)}, bf16[128,512]{1,0:T(8,128)(2,1)S(1)}) fusion(f32[128,512]{1,0:T(8,128)S(1)} %copy.39, bf16[128,2048]{1,0:T(8,128)(2,1)} %hid_ref.1, bf16[2048,512]{1,0:T(8,128)(2,1)S(1)} %copy-done), kind=kOutput, calls=%fused_computation.54 | convolution fusion | flops 268894208 | bytes 3276800 | tf_op jit(solution)/shard_map/dot_general | solution.py:391
  6.2 1.1 multiply_reduce_fusion.2
  7.3 0.8 fusion.74
  8.1 0.7 copy.46
  9.1 1.7 copy.40
  10.8 1.1 fusion.65
  11.9 1.6 copy.41
  13.5 1.1 fusion.10
  14.8 64.4 %scan_states.1 = (f32[8,2,64,128]{3,2,1,0:T(8,128)S(1)}, bf16[1024,256]{1,0:T(8,128)(2,1)S(1)}) custom-call(f32[8,2,64,128]{3,2,1,0:T(8,128)S(1)} %maximum_bitcast_fusion.both_ref, f32[8,1,128]{2,1,0:T(1,128)S(1)} %broadcast_in_dim.48.dec_ref, bf16[128,2048]{1,0:T(8,128)(2,1)S(1)} %copy-done.1), custom_call_target="tpu_custom_call" | custom-call | tf_op jit(solution)/shard_map/scan_states/pallas_call | solution.py:406
  79.2 0.8 copy-done.2
  80.7 1.6 fusion.18
  82.9 0.3 multiply_reduce_fusion.1
  83.3 0.8 fusion.17
  84.8 0.8 fusion.21
  86.0 0.4 fusion.25
  86.4 0.4 fusion.12
  86.9 0.5 copy-done.8
  87.7 1.7 fusion.103.ghp_ref
  89.4 85.1 %weight_grads.1 = (f32[64,512]{1,0:T(8,128)S(1)}, bf16[16,2048]{1,0:T(8,128)(2,1)S(1)}) custom-call(f32[128,512]{1,0:T(8,128)S(1)} %convert_element_type.165.gv_ref, bf16[256,1024]{1,0:T(8,128)(2,1)S(1)} %bitcast.142, f32[128,2048]{1,0:T(8,128)S(1)} %fusion.103.ghp_ref), custom_call_target="tpu_custom_call" | custom-call | tf_op jit(solution)/shard_map/weight_grads/pallas_call | solution.py:468
  174.5 0.6 copy.57
  175.2 0.7 copy.58
  (65 shorter events, 3.8 us)
Async XLA Ops:
  0.6 3.1 %copy-start = (bf16[2048,512]{1,0:T(8,128)(2,1)S(1)}, bf16[2048,512]{1,0:T(8,128)(2,1)}, u32[]{:S(2)}) copy-start(bf16[2048,512]{1,0:T(8,128)(2,1)} %param.8) | copy-start | bytes 6291460
  1.7 4.5 %copy-start.10 = (f32[128,128]{0,1:T(8,128)}, f32[128,128]{0,1:T(8,128)S(1)}, u32[]{:S(2)}) copy-start(f32[128,128]{0,1:T(8,128)S(1)} %fusion.70) | copy-start | bytes 196612
  2.4 1.2 copy-start.15
  3.3 2.8 %copy-start.12 = (pred[128,128]{0,1:T(8,128)(4,1)}, pred[128,128]{0,1:T(8,128)(4,1)S(1)}, u32[]{:S(2)}) copy-start(pred[128,128]{0,1:T(8,128)(4,1)S(1)} %iota_compare_fusion.1) | copy-start | bytes 49156
  3.6 2.5 %copy-start.4 = (bf16[128,8,64]{0,2,1:T(8,128)(2,1)S(1)}, bf16[128,8,64]{0,2,1:T(8,128)(2,1)}, u32[]{:S(2)}) copy-start(bf16[128,8,64]{0,2,1:T(8,128)(2,1)} %param.13) | copy-start | bytes 393220
  3.8 3.5 %copy-start.7 = (bf16[128,1,128]{2,0,1:T(8,128)(2,1)S(1)}, bf16[128,1,128]{2,0,1:T(8,128)(2,1)}, u32[]{:S(2)}) copy-start(bf16[128,1,128]{2,0,1:T(8,128)(2,1)} %param.10) | copy-start | bytes 98308
  3.8 4.2 %copy-start.5 = (bf16[128,1,128]{2,0,1:T(8,128)(2,1)S(1)}, bf16[128,1,128]{2,0,1:T(8,128)(2,1)}, u32[]{:S(2)}) copy-start(bf16[128,1,128]{2,0,1:T(8,128)(2,1)} %param.9) | copy-start | bytes 98308
  7.3 7.5 %copy-start.1 = (bf16[128,2048]{1,0:T(8,128)(2,1)S(1)}, bf16[128,2048]{1,0:T(8,128)(2,1)}, u32[]{:S(2)}) copy-start(bf16[128,2048]{1,0:T(8,128)(2,1)} %hid_ref.1) | copy-start | bytes 1572868
  13.5 66.7 %copy-start.9 = (f32[128,128]{0,1:T(8,128)S(1)}, f32[128,128]{0,1:T(8,128)}, u32[]{:S(2)}) copy-start(f32[128,128]{0,1:T(8,128)} %copy.46) | copy-start | bytes 196612
  79.2 0.8 copy-start.2
  80.2 3.9 %copy-start.17 = (f32[8,128]{1,0:T(8,128)S(1)}, f32[8,128]{1,0:T(8,128)}, u32[]{:S(2)}) copy-start(f32[8,128]{1,0:T(8,128)} %get-tuple-element.13) | copy-start | bytes 12292
  80.3 3.9 %copy-start.18 = (f32[8,128]{1,0:T(8,128)S(1)}, f32[8,128]{1,0:T(8,128)}, u32[]{:S(2)}) copy-start(f32[8,128]{1,0:T(8,128)} %get-tuple-element.14) | copy-start | bytes 12292
  80.6 4.2 %copy-start.14 = (f32[128,8]{0,1:T(8,128)S(1)}, f32[128,8]{0,1:T(8,128)}, u32[]{:S(2)}) copy-start(f32[128,8]{0,1:T(8,128)} %param.11) | copy-start | bytes 12292
  80.6 4.2 %copy-start.16 = (f32[8]{0:T(128)S(1)}, f32[8]{0:T(128)}, u32[]{:S(2)}) copy-start(f32[8]{0:T(128)} %copy-done.15) | copy-start | bytes 100
  80.7 5.1 %copy-start.6 = (bf16[128,1,128]{2,0,1:T(8,128)(2,1)S(1)}, bf16[128,1,128]{2,0,1:T(8,128)(2,1)}, u32[]{:S(2)}) copy-start(bf16[128,1,128]{2,0,1:T(8,128)(2,1)} %param.9) | copy-start | bytes 98308
  82.6 3.4 %copy-start.11 = (f32[128,128]{0,1:T(8,128)S(1)}, f32[128,128]{0,1:T(8,128)}, u32[]{:S(2)}) copy-start(f32[128,128]{0,1:T(8,128)} %copy-done.10) | copy-start | bytes 196612
  82.6 3.4 %copy-start.13 = (pred[128,128]{0,1:T(8,128)(4,1)S(1)}, pred[128,128]{0,1:T(8,128)(4,1)}, u32[]{:S(2)}) copy-start(pred[128,128]{0,1:T(8,128)(4,1)} %copy-done.12) | copy-start | bytes 49156
  85.8 1.7 copy-start.3
  86.8 0.7 copy-start.8
where the time goes:
time: 176 us
  Pallas kernels  150 us (85%)
  matrix products  16.1 us (9%)
  local copies, waits for them, and re-layouts  7.88 us (4%)
    pallas_call x1, Pallas kernels, per_device(): pl.pallas_call(functools.partial(grads_kernel, ny, nz, tp, width), out_sh...  85.1 us
    pallas_call x1, Pallas kernels, per_device(): pl.pallas_call(functools.partial(scan_kernel, ny, nz, tp, 4, pieces), out...  64.4 us
    dot_general x8, matrix products, two_pass(): jnp.einsum(spec, lo, y, preferred_element_type=F32)  4.9 us

commit v1 on v0

v1 whole, which is shorter than its diff:
```python
import functools

import jax
import jax.numpy as jnp
from jax import lax
from jax.experimental import pallas as pl
from jax.experimental.pallas import tpu as pltpu
from jax.sharding import PartitionSpec as P

MESH = pl.DeviceIdType.MESH
F32 = jnp.float32
BF16 = jnp.bfloat16


def inner_size(count):
    size = 1
    while size * size * 4 <= count:
        size *= 2
    while count % size:
        size -= 1
    return size


def remote(src, dst, send, recv, axis, index):
    return pltpu.make_async_remote_copy(
        src_ref=src, dst_ref=dst, send_sem=send, recv_sem=recv, device_id={axis: index}, device_id_type=MESH
    )


def scan_kernel(ny, nz, ntp, both_ref, dec_ref, ht_ref, out_ref, hcol_ref,
                ybuf, ydec, tz, zbuf, cz, zcar, ob, scr, hg,
                dsend, drecv, ysend, yrecv, tsend, trecv, csend, crecv, osend, orecv, hsend, hrecv, fsend, frecv):
    me = lax.axis_index("sp")
    mine = lax.axis_index("tp")
    z, y = me // ny, me % ny
    heads = both_ref.shape[0]
    hq = heads // ny
    pr = zbuf.shape[3]
    state = both_ref.shape[3]
    halves = 2 if ntp % 2 == 0 else 1
    half = mine % halves
    other = mine + 1 - 2 * half
    hz = nz // halves
    ydev = [z * ny + (y + dy) % ny for dy in range(ny)]
    zdev = [((z + dz) % nz) * ny + y for dz in range(nz)]

    barrier = pltpu.get_barrier_semaphore()
    for dev in ydev[1:] + zdev[1:]:
        pl.semaphore_signal(barrier, inc=1, device_id={"sp": dev}, device_id_type=MESH)
    if halves == 2:
        pl.semaphore_signal(barrier, inc=1, device_id={"tp": other}, device_id_type=MESH)
    pl.semaphore_wait(barrier, ny - 1 + nz - 1 + halves - 1)

    def dcopy(dy, arrive=False):
        there = (y + dy) % ny
        slot = there if arrive else y
        return remote(dec_ref.at[pl.ds(there * hq, hq)], ydec.at[slot], dsend.at[there], drecv.at[slot], "sp", ydev[dy])

    def ycopy(h, dy, arrive=False):
        there = (y + dy) % ny
        slot = there if arrive else y
        return remote(both_ref.at[there * hq + h], ybuf.at[slot, h], ysend.at[there, h], yrecv.at[slot, h], "sp", ydev[dy])

    def tcopy(h, dz, arrive=False):
        there = (z + dz) % nz
        slot = there if arrive else z
        return remote(tz.at[there, h], zbuf.at[slot, h], tsend.at[there, h], trecv.at[slot, h], "sp", zdev[dz])

    def ccopy(h, dz, arrive=False):
        there = (z + dz) % nz
        slot = there if arrive else z
        return remote(cz.at[there, h], zcar.at[slot, h], csend.at[there, h], crecv.at[slot, h], "sp", zdev[dz])

    def ocopy(h, dy, arrive=False):
        there = (y + dy) % ny
        slot = there if arrive else y
        return remote(ob.at[there, h], scr.at[slot, h], osend.at[there, h], orecv.at[slot, h], "sp", ydev[dy])

    def part(k):
        return pl.ds(pl.multiple_of(k * hz, hz), hz)

    def hcopy(dy, arrive=False):
        there = (y + dy) % ny
        slot = there if arrive else y
        return remote(ht_ref.at[there, part(half)], hg.at[slot, part(half)], hsend.at[there], hrecv.at[slot], "sp", ydev[dy])

    def share(dy, which):
        there = (y + dy) % ny
        block = hg.at[there, part(which)]
        return remote(block, block, fsend.at[there], frecv.at[there], "tp", other)

    for dy in range(1, ny):
        dcopy(dy).start()
    for h in range(hq):
        for dy in range(1, ny):
            ycopy(h, dy).start()
    for dy in range(1, ny):
        hcopy(dy).start()

    ydec[y] = dec_ref[pl.ds(y * hq, hq)]
    ybuf[y] = both_ref[pl.ds(y * hq, hq)]
    for dy in range(1, ny):
        dcopy(dy, True).wait_recv()

    for h in range(hq):
        for dy in range(1, ny):
            ycopy(h, dy, True).wait_recv()
        up = ybuf[0, h, 0]
        down = ybuf[ny - 1, h, 1]
        prod = ydec[0, h]
        for yy in range(1, ny):
            up = ydec[yy, h][:1] * up + ybuf[yy, h, 0]
            down = ydec[ny - 1 - yy, h][:1] * down + ybuf[ny - 1 - yy, h, 1]
            prod = prod * ydec[yy, h]
        for p in range(nz):
            tz[p, h, 0] = up[p * pr:(p + 1) * pr]
            tz[p, h, 1] = down[p * pr:(p + 1) * pr]
            tz[p, h, 2] = prod[:pr]
        for dz in range(1, nz):
            tcopy(h, dz).start()
        zbuf[z, h] = tz[z, h]

    for h in range(hq):
        for dz in range(1, nz):
            tcopy(h, dz, True).wait_recv()
        run = jnp.zeros((pr, state), F32)
        for zz in range(nz):
            cz[zz, h, 0] = run
            run = zbuf[zz, h, 2] * run + zbuf[zz, h, 0]
        run = jnp.zeros((pr, state), F32)
        for zz in reversed(range(nz)):
            cz[zz, h, 1] = run
            run = zbuf[zz, h, 2] * run + zbuf[zz, h, 1]
        for dz in range(1, nz):
            ccopy(h, dz).start()
        zcar[z, h] = cz[z, h]

    for h in range(hq):
        for dz in range(1, nz):
            ccopy(h, dz, True).wait_recv()
        now = zcar[:, h, 0].reshape(nz * pr, state)
        for yy in range(ny):
            ob[yy, h, 0] = now
            now = ydec[yy, h][:1] * now + ybuf[yy, h, 0]
        now = zcar[:, h, 1].reshape(nz * pr, state)
        for yy in reversed(range(ny)):
            ob[yy, h, 1] = now
            now = ydec[yy, h][:1] * now + ybuf[yy, h, 1]
        for dy in range(1, ny):
            ocopy(h, dy).start()
        scr[y, h] = ob[y, h]

    length = hg.shape[3]
    for dy in range(1, ny):
        hcopy(dy, True).wait_recv()
        if halves == 2:
            share(dy, half).start()
    hcol_ref[:, :, pl.ds(pl.multiple_of(y * length, 128), length)] = ht_ref[y].astype(BF16)
    for dy in range(1, ny):
        there = (y + dy) % ny
        if halves == 2:
            share(dy, 1 - half).wait_recv()
        hcol_ref[:, :, pl.ds(pl.multiple_of(there * length, 128), length)] = hg[there].astype(BF16)

    for h in range(hq):
        for dy in range(1, ny):
            ocopy(h, dy, True).wait_recv()
    for yy in range(ny):
        out_ref[yy * hq:(yy + 1) * hq] = scr[yy]

    for dy in range(1, ny):
        dcopy(dy).wait_send()
        hcopy(dy).wait_send()
        if halves == 2:
            share(dy, half).wait_send()
    for h in range(hq):
        for dy in range(1, ny):
            ycopy(h, dy).wait_send()
            ocopy(h, dy).wait_send()
        for dz in range(1, nz):
            tcopy(h, dz).wait_send()
            ccopy(h, dz).wait_send()


def grads_kernel(ny, nz, ntp, width, gv_ref, hct_ref, ghp_ref, gw_ref, gh_ref,
                 gath, part, ring, pland, red, xland,
                 ysend, yrecv, rsend, rrecv, psend, precv, xsend, xrecv):
    me = lax.axis_index("sp")
    mine = lax.axis_index("tp")
    z, y = me // ny, me % ny
    rows = gw_ref.shape[0]
    chunks = gv_ref.shape[1] // width
    length = gv_ref.shape[0]
    halves = 2 if ntp % 2 == 0 else 1
    nx = ntp // halves
    core = mine % halves
    x = mine // halves
    ydev = [z * ny + (y + dy) % ny for dy in range(ny)]
    zup, zdn = ((z + 1) % nz) * ny + y, ((z + nz - 1) % nz) * ny + y

    barrier = pltpu.get_barrier_semaphore()
    for dev in ydev[1:] + [zup, zdn]:
        pl.semaphore_signal(barrier, inc=1, device_id={"sp": dev}, device_id_type=MESH)
    if halves == 2:
        pl.semaphore_signal(barrier, inc=1, device_id={"tp": mine + 1 - 2 * core}, device_id_type=MESH)
    for dx in range(1, nx):
        pl.semaphore_signal(barrier, inc=1, device_id={"tp": ((x + dx) % nx) * halves + core}, device_id_type=MESH)
    pl.semaphore_wait(barrier, ny - 1 + 2 + halves - 1 + nx - 1)

    def ycopy(c, dy, arrive=False):
        there = (y + dy) % ny
        slot = there if arrive else y
        return remote(gath.at[slot, c], gath.at[slot, c], ysend.at[there, c], yrecv.at[slot, c], "sp", ydev[dy])

    def pair():
        return remote(ghp_ref.at[1 - core], pland, psend, precv, "tp", mine + 1 - 2 * core)

    def xcopy(dx, arrive=False):
        there = (x + dx) % nx
        slot = there if arrive else x
        return remote(red.at[there], xland.at[slot], xsend.at[there], xrecv.at[slot], "tp", there * halves + core)

    def reach(c, d):
        far = nz // 2
        return far if (c + d) % 2 == 0 else nz - 1 - far

    def rcopy(c, d, j):
        target = (z + reach(c, d)) % nz if d == 0 else (z + nz - reach(c, d)) % nz
        src = part.at[c, target] if j == 0 else ring.at[d, c, j - 1]
        return remote(src, ring.at[d, c, j], rsend.at[d, c, j], rrecv.at[d, c, j], "sp", zup if d == 0 else zdn)

    for c in range(chunks):
        gath[y, c] = gv_ref[:, c * width:(c + 1) * width]
        for dy in range(1, ny):
            ycopy(c, dy).start()
    if halves == 2:
        pair().start()

    def multiply(c):
        for dy in range(1, ny):
            ycopy(c, dy, True).wait_recv()
        block = gath[:, c].reshape(ny * length, width).astype(BF16)
        part[c] = jnp.dot(hct_ref[...], block, preferred_element_type=F32).reshape(nz, rows, width)
        for d in range(2):
            if reach(c, d) > 0:
                rcopy(c, d, 0).start()

    def hop(c, d, j):
        rcopy(c, d, j).wait_recv()
        left = reach(c, d) - 1 - j
        if left > 0:
            target = (z + left) % nz if d == 0 else (z + nz - left) % nz
            ring[d, c, j] = ring[d, c, j] + part[c, target]
            rcopy(c, d, j + 1).start()

    def pairs():
        if halves == 2:
            pair().wait_recv()
            red[...] = ghp_ref[core] + pland[...]
        else:
            red[...] = ghp_ref[0]
        for dx in range(1, nx):
            xcopy(dx).start()

    tasks = [(0.0, pairs)]
    for c in range(chunks):
        ready = 4.0 + 2.5 * c
        tasks.append((ready, functools.partial(multiply, c)))
        for d in range(2):
            for j in range(reach(c, d)):
                tasks.append((ready + 3.4 * (j + 1), functools.partial(hop, c, d, j)))
    for _, task in sorted(tasks, key=lambda item: item[0]):
        task()

    for c in range(chunks):
        total = part[c, z]
        for d in range(2):
            if reach(c, d) > 0:
                total = total + ring[d, c, reach(c, d) - 1]
        gw_ref[:, c * width:(c + 1) * width] = total

    total = red[x]
    for dx in range(1, nx):
        xcopy(dx, True).wait_recv()
        total = total + xland[(x + dx) % nx]
    gh_ref[...] = total.astype(gh_ref.dtype)

    for c in range(chunks):
        for dy in range(1, ny):
            ycopy(c, dy).wait_send()
        for d in range(2):
            for j in range(reach(c, d)):
                rcopy(c, d, j).wait_send()
    if halves == 2:
        pair().wait_send()
    for dx in range(1, nx):
        xcopy(dx).wait_send()


VM = pl.BlockSpec(memory_space=pltpu.VMEM)
LIMIT = 48 * 1024 * 1024


def split(x):
    hi = lax.reduce_precision(x, 8, 7)
    return hi.astype(BF16), (x - hi).astype(BF16)


def two_pass(spec, x, y):
    hi, lo = split(x)
    return jnp.einsum(spec, hi, y, preferred_element_type=F32) + jnp.einsum(spec, lo, y, preferred_element_type=F32)


def per_device(sp, tp, hidden, value_weight, key_vecs, queries, decay_pre, decay_rate, cotangent):
    length = hidden.shape[0]
    heads = decay_rate.shape[0]
    head_width = cotangent.shape[2]
    groups = key_vecs.shape[1]
    state = key_vecs.shape[2]
    per = heads // groups
    features = hidden.shape[1]
    columns = value_weight.shape[1]
    ny = inner_size(sp)
    nz = sp // ny
    values = jnp.dot(hidden, value_weight, preferred_element_type=F32).astype(BF16)
    v = values.reshape(length, groups, per, head_width)
    cot = cotangent.reshape(length, groups, per, head_width)
    log_decay = -decay_rate[None, :] * jax.nn.softplus(decay_pre)
    tri = jnp.tril(jnp.ones((length, length), F32))
    cum = jnp.dot(tri, log_decay, precision=lax.Precision.HIGHEST)
    tot = cum[-1]
    to_end = jnp.exp(tot[None] - cum).reshape(length, groups, per, 1)
    ecum = jnp.exp(cum).reshape(length, groups, per, 1)
    local_state = two_pass("sgip,sgn->gipn", to_end * v.astype(F32), key_vecs)
    local_pull = two_pass("sgip,sgn->gipn", ecum * cot.astype(F32), queries)
    both = jnp.stack([local_state, local_pull], axis=2).reshape(heads, 2, head_width, state)
    rows = features // sp
    hq = heads // ny
    pr = head_width // nz
    halves = 2 if tp % 2 == 0 else 1
    dec = jnp.broadcast_to(jnp.exp(tot)[:, None, None], (heads, pr, state))
    ht = jnp.transpose(hidden.T.astype(F32).reshape(nz, ny, rows, length), (1, 0, 2, 3))
    scanned, hcol = pl.pallas_call(
        functools.partial(scan_kernel, ny, nz, tp),
        out_shape=(
            jax.ShapeDtypeStruct(both.shape, F32),
            jax.ShapeDtypeStruct((nz, rows, ny * length), BF16),
        ),
        in_specs=[VM] * 3,
        out_specs=(VM, VM),
        scratch_shapes=[
            pltpu.VMEM((ny, hq) + both.shape[1:], F32),
            pltpu.VMEM((ny, hq, pr, state), F32),
            pltpu.VMEM((nz, hq, 3, pr, state), F32),
            pltpu.VMEM((nz, hq, 3, pr, state), F32),
            pltpu.VMEM((nz, hq, 2, pr, state), F32),
            pltpu.VMEM((nz, hq, 2, pr, state), F32),
            pltpu.VMEM((ny, hq) + both.shape[1:], F32),
            pltpu.VMEM((ny, hq) + both.shape[1:], F32),
            pltpu.VMEM((ny, nz, rows, length), F32),
            pltpu.SemaphoreType.DMA((ny,)),
            pltpu.SemaphoreType.DMA((ny,)),
            pltpu.SemaphoreType.DMA((ny, hq)),
            pltpu.SemaphoreType.DMA((ny, hq)),
            pltpu.SemaphoreType.DMA((nz, hq)),
            pltpu.SemaphoreType.DMA((nz, hq)),
            pltpu.SemaphoreType.DMA((nz, hq)),
            pltpu.SemaphoreType.DMA((nz, hq)),
            pltpu.SemaphoreType.DMA((ny, hq)),
            pltpu.SemaphoreType.DMA((ny, hq)),
            pltpu.SemaphoreType.DMA((ny,)),
            pltpu.SemaphoreType.DMA((ny,)),
            pltpu.SemaphoreType.DMA((ny,)),
            pltpu.SemaphoreType.DMA((ny,)),
        ],
        compiler_params=pltpu.CompilerParams(collective_id=0, has_side_effects=True, vmem_limit_bytes=LIMIT),
        name="scan_states",
    )(both, dec, ht)
    state_in = scanned[:, 0].reshape(groups, per, head_width, state)
    state_grad = scanned[:, 1].reshape(groups, per, head_width, state)

    cum_h = cum.T
    causal = jnp.tril(jnp.ones((length, length), dtype=bool))[None]
    across = cum_h[:, :, None] - cum_h[:, None, :]
    damping = jnp.where(causal, jnp.exp(jnp.where(causal, across, 0.0)), 0.0).reshape(groups, per, length, length)
    scores = jnp.einsum("tgn,sgn->gts", queries, key_vecs, preferred_element_type=F32)
    pair = jnp.einsum("tgip,sgip->gits", cot, v, preferred_element_type=F32)
    dscore = pair * damping
    flux = dscore * scores[:, None]
    net = (jnp.sum(flux, axis=3) - jnp.sum(flux, axis=2)).reshape(heads, length).T
    dsum = jnp.sum(dscore, axis=1)
    mixed = scores[:, None] * damping
    gq_heads = ecum * two_pass("gipn,tgip->tgin", state_in, cot)
    gk_heads = to_end * two_pass("gipn,tgip->tgin", state_grad, v)
    gv = two_pass("gits,tgip->sgip", mixed, cot) + to_end * two_pass(
        "gipn,sgn->sgip", state_grad, key_vecs
    )
    gq = two_pass("gts,sgn->tgn", dsum, key_vecs) + jnp.sum(gq_heads, axis=2)
    gk = two_pass("gts,tgn->sgn", dsum, queries) + jnp.sum(gk_heads, axis=2)
    qgq = jnp.sum(gq_heads * queries.astype(F32)[:, :, None], axis=3).reshape(length, heads)
    kgk = jnp.sum(gk_heads * key_vecs.astype(F32)[:, :, None], axis=3).reshape(length, heads)
    through = jnp.exp(tot) * jnp.sum(state_in * state_grad, axis=(2, 3)).reshape(heads)
    suffix = jnp.dot(tri.T, net + qgq, precision=lax.Precision.HIGHEST)
    prefix = jnp.dot(tri - jnp.eye(length, dtype=F32), kgk, precision=lax.Precision.HIGHEST)
    grad_decay = (suffix + prefix + through[None]) * -decay_rate[None] * jax.nn.sigmoid(decay_pre)

    grad_flat = gv.reshape(length, columns).astype(BF16)
    ghp = lax.dot_general(grad_flat, value_weight, (((1,), (1,)), ((), ())), preferred_element_type=F32)
    width = min(columns, 128)
    chunks = columns // width
    own = length // tp
    far = nz // 2
    ghp = jnp.transpose(ghp.reshape(tp // halves, halves, own, features), (1, 0, 2, 3))
    grad_weight, grad_hidden = pl.pallas_call(
        functools.partial(grads_kernel, ny, nz, tp, width),
        out_shape=(
            jax.ShapeDtypeStruct((rows, columns), F32),
            jax.ShapeDtypeStruct((own, features), BF16),
        ),
        in_specs=[VM] * 3,
        out_specs=(VM, VM),
        scratch_shapes=[
            pltpu.VMEM((ny, chunks, length, width), F32),
            pltpu.VMEM((chunks, nz, rows, width), F32),
            pltpu.VMEM((2, chunks, far, rows, width), F32),
            pltpu.VMEM((tp // halves, own, features), F32),
            pltpu.VMEM((tp // halves, own, features), F32),
            pltpu.VMEM((tp // halves, own, features), F32),
            pltpu.SemaphoreType.DMA((ny, chunks)),
            pltpu.SemaphoreType.DMA((ny, chunks)),
            pltpu.SemaphoreType.DMA((2, chunks, far)),
            pltpu.SemaphoreType.DMA((2, chunks, far)),
            pltpu.SemaphoreType.DMA,
            pltpu.SemaphoreType.DMA,
            pltpu.SemaphoreType.DMA((tp // halves,)),
            pltpu.SemaphoreType.DMA((tp // halves,)),
        ],
        compiler_params=pltpu.CompilerParams(collective_id=1, has_side_effects=True, vmem_limit_bytes=LIMIT),
        name="weight_grads",
    )(grad_flat.astype(F32), hcol.reshape(nz * rows, ny * length), ghp)
    return (gq_cast(gk), gq_cast(gq), grad_decay, grad_hidden, grad_weight)


def gq_cast(x):
    return x.astype(BF16)


def solution(mesh):
    return jax.shard_map(
        functools.partial(per_device, mesh.shape["sp"], mesh.shape["tp"]),
        mesh=mesh,
        in_specs=(
            P("sp", None),
            P(None, "tp"),
            P("sp", "tp", None),
            P("sp", "tp", None),
            P("sp", "tp"),
            P("tp"),
            P("sp", "tp", None),
        ),
        out_specs=(
            P("sp", "tp", None),
            P("sp", "tp", None),
            P("sp", "tp"),
            P(("sp", "tp"), None),
            P("sp", "tp"),
        ),
        check_vma=False,
    )
```

time: 176 us -> 105 us (0.60)
  Pallas kernels: 150 us -> 63.9 us
  matrix products: 16.1 us -> 21.5 us
  local copies, waits for them, and re-layouts: 7.88 us -> 12.7 us
  other arithmetic: 1.24 us -> 5.15 us
    pallas_call x1, Pallas kernels: 85.1 us -> 29.8 us  [per_device(): pl.pallas_call(functools.partial(grads_kernel, ny, nz, tp, width), out_sh...]
    pallas_call x1, Pallas kernels: 64.4 us -> 34 us  [per_device(): pl.pallas_call(functools.partial(scan_kernel, ny, nz, tp), out_shape=(jax...]
    convert_element_type x2, local copies, waits for them, and re-layouts: 3.31 us -> 0.23 us  [split(): return (hi.astype(BF16), (x - hi).astype(BF16))]
    dot_general x8, matrix products: 4.9 us -> 7.8 us  [two_pass(): jnp.einsum(spec, lo, y, preferred_element_type=F32)]
    unnamed x40 -> x39, local copies, waits for them, and re-layouts: 2.66 us -> 5 us
where the time goes in v1:
time: 105 us; the launch traced here: 104 us
  Pallas kernels  63.9 us (61%)
  matrix products  21.5 us (20%)
  local copies, waits for them, and re-layouts  12.7 us (12%)
  other arithmetic  5.15 us (5%)
    pallas_call x1, Pallas kernels, per_device(): pl.pallas_call(functools.partial(scan_kernel, ny, nz, tp), out_shape=(jax...  34 us
    pallas_call x1, Pallas kernels, per_device(): pl.pallas_call(functools.partial(grads_kernel, ny, nz, tp, width), out_sh...  29.8 us
    dot_general x8, matrix products, two_pass(): jnp.einsum(spec, lo, y, preferred_element_type=F32)  7.8 us
    unnamed x39, local copies, waits for them, and re-layouts  5 us
    dot_general x8, matrix products, two_pass(): jnp.einsum(spec, hi, y, preferred_element_type=F32)  4.39 us
    dot_general x1, matrix products, per_device(): jnp.dot(hidden, value_weight, preferred_element_type=F32).astype(BF16)  2.2 us

profile of v1, /device:TPU:2, one launch (start us, length us, event | category | flops | bytes accessed | tf_op | source)
XLA Modules:
  0.0 104.2 jit_solution(1250562132698125753)
XLA Ops:
  1.5 0.9 fusion.58
  2.9 2.2 %fusion.27 = (bf16[128,512]{1,0:T(8,128)(2,1)S(1)}, bf16[128,512]{1,0:T(8,128)(2,1)S(1)}, bf16[128,512]{1,0:T(8,128)(2,1)}) fusion(f32[128,512]{1,0:T(8,128)S(1)} %copy.43, bf16[128,2048]{1,0:T(8,128)(2,1)} %param.7, bf16[2048,512]{1,0:T(8,128)(2,1)S(1)} %copy-done), kind=kOutput, calls=%fused_computation.57 | convolution fusion | flops 268894208 | bytes 3276800 | tf_op jit(solution)/shard_map/dot_general | solution.py:325
  6.2 1.0 copy.46
  7.2 1.1 %transpose.120 = f32[128,2048]{0,1:T(8,128)S(1)} convert(bf16[128,2048]{0,1:T(8,128)(2,1)} %copy.46) | non-fusion elementwise | flops 262144 | bytes 1572864 | tf_op jit(solution)/shard_map/transpose | solution.py:342
  8.4 34.0 %scan_states.1 = (f32[8,2,64,128]{3,2,1,0:T(8,128)S(1)}, bf16[8,64,512]{2,1,0:T(8,128)(2,1)S(1)}) custom-call(f32[8,2,64,128]{3,2,1,0:T(8,128)S(1)} %maximum_bitcast_fusion.both_ref, f32[8,8,128]{2,1,0:T(8,128)S(1)} %broadcast_in_dim.48.dec_ref, f32[4,8,64,128]{3,2,1,0:T(8,128)S(1)} %bitcast.157), custom_call_target="tpu_custom_call" | custom-call | tf_op jit(solution)/shard_map/scan_states/pallas_call | solution.py:343
  45.0 1.8 %convolution_bitcast_fusion.ghp_ref = f32[2,4,16,2048]{3,2,1,0:T(8,128)} fusion(bf16[2048,512]{1,0:T(8,128)(2,1)S(1)} %copy-done, bf16[4,2,16,512]{3,2,1,0:T(8,128)(2,1)S(1)} %convert_element_type.175), kind=kOutput, calls=%fused_computation | convolution fusion | flops 268435456 | bytes 3276800 | tf_op jit(solution)/shard_map/dot_general | solution.py:408
  47.6 1.1 %copy.58.gv_ref = f32[128,512]{1,0:T(8,128)S(1)} copy(f32[128,512]{0,1:T(8,128)} %bitcast_convert_fusion) | data formatting | bytes 524288 | tf_op jit(solution)/shard_map/convert_element_type | solution.py:440
  48.7 1.2 %copy-done.1 = f32[2,4,16,2048]{3,2,1,0:T(8,128)S(1)} copy-done((f32[2,4,16,2048]{3,2,1,0:T(8,128)S(1)}, f32[2,4,16,2048]{3,2,1,0:T(8,128)}, u32[]{:S(2)}) %copy-start.1) | copy-done | bytes 1048600
  49.9 29.8 %weight_grads.1 = (f32[64,512]{1,0:T(8,128)S(1)}, bf16[16,2048]{1,0:T(8,128)(2,1)S(1)}) custom-call(f32[128,512]{1,0:T(8,128)S(1)} %copy.58.gv_ref, bf16[512,512]{1,0:T(8,128)(2,1)S(1)} %bitcast.158, f32[2,4,16,2048]{3,2,1,0:T(8,128)S(1)} %copy-done.1), custom_call_target="tpu_custom_call" | custom-call | tf_op jit(solution)/shard_map/weight_grads/pallas_call | solution.py:414
  80.3 1.2 %fusion.49 = f32[8,128,128]{2,1,0:T(8,128)S(1)} fusion(bf16[128,8,64]{0,2,1:T(8,128)(2,1)} %param.13, f32[8,2,64,128]{3,2,1,0:T(8,128)S(1)} %get-tuple-element.9), kind=kOutput, calls=%fused_computation.78 | convolution fusion | flops 16908288 | bytes 917504 | tf_op jit(solution)/shard_map/gipn,tgip->tgin/dot_general | solution.py:311
  81.6 1.4 %bitcast_convert_fusion.2 = f32[128,128]{1,0:T(8,128)} fusion(bf16[128,1,128]{2,0,1:T(8,128)(2,1)} %param.10), kind=kLoop, calls=%fused_computation.109 | loop fusion | flops 16384 | bytes 98304 | tf_op jit(solution)/shard_map/mul | solution.py:400
  83.0 0.9 copy.51
  83.9 1.8 %multiply_reduce_fusion.1 = (f32[128,8]{0,1:T(8,128)S(1)}, f32[128,128]{0,1:T(8,128)}) fusion(f32[128,128]{0,1:T(8,128)S(1)} %copy.51, f32[8,128,128]{2,1,0:T(8,128)S(1)} %fusion.49, bf16[128,8,64]{0,2,1:T(8,128)(2,1)} %param.13, f32[8,2,64,128]{3,2,1,0:T(8,128)S(1)} %get-tuple-element.9, f32[128,8]{0,1:T(8,128)S(1)} %get-tuple-element.23), kind=kOutput, calls=%fused_computation.41 | convolution fusion | flops 17611776 | bytes 1056768 | tf_op jit(solution)/shard_map/gipn,tgip->tgin/dot_general | solution.py:311
  85.8 1.0 copy.42
  86.8 2.0 %multiply_reduce_fusion.2 = (f32[8,128]{1,0:T(8,128)S(1)}, f32[8,128]{1,0:T(8,128)S(1)}, f32[128,128]{0,1:T(8,128)}) fusion(f32[128,128]{0,1:T(8,128)} %copy-done.13, f32[8,128]{1,0:T(8,128)S(1)} %bitcast.168, pred[128,128]{0,1:T(8,128)(4,1)S(1)} %copy-done.15, bf16[128,8,64]{0,2,1:T(8,128)(2,1)S(1)} %bitcast.160, bf16[128,8,64]{0,2,1:T(8,128)(2,1)S(1)} %copy-done.8), kind=kOutput, calls=%fused_computation.44 | convolution fusion | flops 17807360 | bytes 421888 | tf_op jit(solution)/shard_map/tgip,sgip->gits/dot_general | solution.py:387
  90.5 1.6 %copy.52 = f32[128,128]{0,1:T(8,128)} copy(f32[128,128]{1,0:T(8,128)} %bitcast_convert_fusion.1) | data formatting | bytes 131072 | tf_op jit(solution)/shard_map/mul | solution.py:401
  92.1 1.8 %multiply_reduce_fusion = (f32[128,8]{0,1:T(8,128)S(1)}, f32[128,128]{0,1:T(8,128)}) fusion(f32[128,128]{0,1:T(8,128)} %copy.52, f32[8,128,128]{1,2,0:T(8,128)S(1)} %fusion.48, bf16[128,8,64]{0,2,1:T(8,128)(2,1)S(1)} %bitcast.162, f32[8,2,64,128]{3,2,1,0:T(8,128)S(1)} %get-tuple-element.9, f32[128,8]{0,1:T(8,128)S(1)} %get-tuple-element.22), kind=kOutput, calls=%fused_computation.40 | convolution fusion | flops 17611776 | bytes 1056768 | tf_op jit(solution)/shard_map/gipn,tgip->tgin/dot_general | solution.py:311
  94.3 1.5 %fusion.22 = f32[128,8]{0,1:T(8,128)} fusion(f32[128,8]{0,1:T(8,128)S(1)} %copy-done.17, f32[128,8]{0,1:T(8,128)S(1)} %get-tuple-element.15, f32[128,8]{0,1:T(8,128)} %param.11, f32[8]{0:T(128)S(1)} %multiply_reduce_fusion.5, f32[8]{0:T(128)} %copy-done.16), kind=kOutput, calls=%fused_computation.34 | convolution fusion | flops 1661952 | bytes 16448 | tf_op jit(solution)/shard_map/dot_general | solution.py:404
  95.8 0.9 copy.49
  96.7 1.0 fusion.70
  97.7 1.6 %fusion.18 = bf16[128,1,128]{2,0,1:T(8,128)(2,1)} fusion(f32[128,128]{1,0:T(8,128)S(1)} %fusion.70, f32[128,128]{1,0:T(8,128)S(1)} %copy.49, bf16[128,1,128]{2,0,1:T(8,128)(2,1)S(1)} %copy-done.10, f32[128,128]{0,1:T(8,128)} %get-tuple-element.17), kind=kOutput, calls=%fused_computation.29 | convolution fusion | flops 4292608 | bytes 262144 | tf_op jit(solution)/shard_map/gts,sgn->tgn/dot_general | solution.py:311
  99.4 0.9 copy.48
  100.3 1.0 fusion.76
  101.3 1.6 %fusion.19 = bf16[128,1,128]{2,0,1:T(8,128)(2,1)} fusion(f32[128,128]{1,0:T(8,128)S(1)} %fusion.76, f32[128,128]{1,0:T(8,128)S(1)} %copy.48, bf16[128,1,128]{2,0,1:T(8,128)(2,1)S(1)} %copy-done.12, f32[128,128]{0,1:T(8,128)} %get-tuple-element.17), kind=kOutput, calls=%fused_computation.30 | convolution fusion | flops 4292608 | bytes 262144 | tf_op jit(solution)/shard_map/gts,tgn->sgn/dot_general | solution.py:311
  (67 shorter events, 9.7 us)
Async XLA Ops:
  0.6 2.2 %copy-start = (bf16[2048,512]{1,0:T(8,128)(2,1)S(1)}, bf16[2048,512]{1,0:T(8,128)(2,1)}, u32[]{:S(2)}) copy-start(bf16[2048,512]{1,0:T(8,128)(2,1)} %param.8) | copy-start | bytes 6291460
  1.5 1.2 %copy-start.16 = (f32[8]{0:T(128)}, f32[8]{0:T(128)S(1)}, u32[]{:S(2)}) copy-start(f32[8]{0:T(128)S(1)} %neg.12) | copy-start | bytes 100
  2.7 2.5 %copy-start.9 = (bf16[128,1,128]{2,0,1:T(8,128)(2,1)S(1)}, bf16[128,1,128]{2,0,1:T(8,128)(2,1)}, u32[]{:S(2)}) copy-start(bf16[128,1,128]{2,0,1:T(8,128)(2,1)} %param.9) | copy-start | bytes 98308
  2.8 2.8 %copy-start.7 = (bf16[128,8,64]{0,2,1:T(8,128)(2,1)S(1)}, bf16[128,8,64]{0,2,1:T(8,128)(2,1)}, u32[]{:S(2)}) copy-start(bf16[128,8,64]{0,2,1:T(8,128)(2,1)} %param.13) | copy-start | bytes 393220
  2.8 2.8 %copy-start.11 = (bf16[128,1,128]{2,0,1:T(8,128)(2,1)S(1)}, bf16[128,1,128]{2,0,1:T(8,128)(2,1)}, u32[]{:S(2)}) copy-start(bf16[128,1,128]{2,0,1:T(8,128)(2,1)} %param.10) | copy-start | bytes 98308
  5.0 1.1 %copy-start.6 = (bf16[128,2048]{1,0:T(8,128)(2,1)S(1)}, bf16[128,2048]{1,0:T(8,128)(2,1)}, u32[]{:S(2)}) copy-start(bf16[128,2048]{1,0:T(8,128)(2,1)} %param.7) | copy-start | bytes 1572868
  42.4 0.8 copy-start.2
  43.8 0.8 copy-start.13
  43.8 0.8 copy-start.14
  45.0 3.6 %copy-start.3 = (bf16[8,64,512]{2,1,0:T(8,128)(2,1)S(1)}, bf16[8,64,512]{2,1,0:T(8,128)(2,1)}, u32[]{:S(2)}) copy-start(bf16[8,64,512]{2,1,0:T(8,128)(2,1)} %copy-done.2) | copy-start | bytes 1572868
  48.6 1.2 %copy-start.1 = (f32[2,4,16,2048]{3,2,1,0:T(8,128)S(1)}, f32[2,4,16,2048]{3,2,1,0:T(8,128)}, u32[]{:S(2)}) copy-start(f32[2,4,16,2048]{3,2,1,0:T(8,128)} %convolution_bitcast_fusion.ghp_ref) | copy-start | bytes 3145732
  79.7 0.6 copy-start.4
  80.3 6.5 %copy-start.8 = (bf16[128,8,64]{0,2,1:T(8,128)(2,1)S(1)}, bf16[128,8,64]{0,2,1:T(8,128)(2,1)}, u32[]{:S(2)}) copy-start(bf16[128,8,64]{0,2,1:T(8,128)(2,1)} %param.13) | copy-start | bytes 393220
  80.3 6.5 %copy-start.15 = (pred[128,128]{0,1:T(8,128)(4,1)S(1)}, pred[128,128]{0,1:T(8,128)(4,1)}, u32[]{:S(2)}) copy-start(pred[128,128]{0,1:T(8,128)(4,1)} %copy-done.14) | copy-start | bytes 49156
  81.6 8.3 %copy-start.10 = (bf16[128,1,128]{2,0,1:T(8,128)(2,1)S(1)}, bf16[128,1,128]{2,0,1:T(8,128)(2,1)}, u32[]{:S(2)}) copy-start(bf16[128,1,128]{2,0,1:T(8,128)(2,1)} %param.9) | copy-start | bytes 98308
  88.8 11.5 %copy-start.12 = (bf16[128,1,128]{2,0,1:T(8,128)(2,1)S(1)}, bf16[128,1,128]{2,0,1:T(8,128)(2,1)}, u32[]{:S(2)}) copy-start(bf16[128,1,128]{2,0,1:T(8,128)(2,1)} %param.10) | copy-start | bytes 98308
  88.8 14.1 %copy-start.5 = (bf16[16,2048]{1,0:T(8,128)(2,1)S(1)}, bf16[16,2048]{1,0:T(8,128)(2,1)}, u32[]{:S(2)}) copy-start(bf16[16,2048]{1,0:T(8,128)(2,1)} %copy-done.4) | copy-start | bytes 196612
  89.6 4.7 %copy-start.17 = (f32[128,8]{0,1:T(8,128)S(1)}, f32[128,8]{0,1:T(8,128)}, u32[]{:S(2)}) copy-start(f32[128,8]{0,1:T(8,128)} %fusion.56) | copy-start | bytes 12292

commit v2 on v1

v2 whole, which is shorter than its diff:
```python
import functools

import jax
import jax.numpy as jnp
from jax import lax
from jax.experimental import pallas as pl
from jax.experimental.pallas import tpu as pltpu
from jax.sharding import PartitionSpec as P

MESH = pl.DeviceIdType.MESH
F32 = jnp.float32
BF16 = jnp.bfloat16
HIGH = lax.Precision.HIGHEST
LANES = 128
SUB = 8


def inner_size(count):
    size = 1
    while size * size * 4 <= count:
        size *= 2
    while count % size:
        size -= 1
    return size


def remote(src, dst, send, recv, axis, index):
    return pltpu.make_async_remote_copy(
        src_ref=src, dst_ref=dst, send_sem=send, recv_sem=recv, device_id={axis: index}, device_id_type=MESH
    )


def nn(a, b, precision=None):
    return jnp.dot(a, b, preferred_element_type=F32, precision=precision)


def nt(a, b, precision=None):
    return lax.dot_general(a, b, (((1,), (1,)), ((), ())), preferred_element_type=F32, precision=precision)


def split(x):
    hi = x.astype(BF16)
    return hi, (x - hi.astype(F32)).astype(BF16)


def mixer_kernel(ny, nz, ntp, hid_hbm, w_hbm, key_hbm, qry_hbm, pre_hbm, rate_ref, cot_hbm,
                 gk_ref, gq_ref, gd_ref, gh_ref, gw_ref,
                 hid, wt, key, qry, pre, cot,
                 ecot, tend, xval, damp, gvloc, gvb, kgs, rows8, cols8, gkl, gql,
                 sbuf, decb, ybuf, ydec, tz, zbuf, cz, zcar, ob, scr, ht, hg, hcol,
                 gath, part, ring, ghp, pland, red, xland,
                 insem, dsend, drecv, ysend, yrecv, tsend, trecv, csend, crecv, osend, orecv,
                 hsend, hrecv, fsend, frecv, gsend, grecv, rsend, rrecv, psend, precv, xsend, xrecv):
    me = lax.axis_index("sp")
    mine = lax.axis_index("tp")
    z, y = me // ny, me % ny
    length, features = hid.shape
    heads = rate_ref.shape[1]
    columns = cot.shape[1]
    width = columns // heads
    tiles = columns // LANES
    per = LANES // width
    state = key.shape[1]
    nr = state // nz
    rows = gw_ref.shape[0]
    own = gh_ref.shape[0]
    halves = 2 if ntp % 2 == 0 else 1
    core, x, nx = mine % halves, mine // halves, ntp // halves
    partner = mine + 1 - 2 * core
    hz = nz // halves
    steps = insem.shape[0] - 4
    depth = features // steps
    ydev = [z * ny + (y + dy) % ny for dy in range(ny)]
    zdev = [((z + dz) % nz) * ny + y for dz in range(nz)]

    small = [
        pltpu.make_async_copy(pre_hbm, pre, insem.at[0]),
        pltpu.make_async_copy(qry_hbm, qry, insem.at[1]),
        pltpu.make_async_copy(cot_hbm, cot, insem.at[2]),
        pltpu.make_async_copy(key_hbm, key, insem.at[3]),
    ]
    for copy in small:
        copy.start()
    wcopies, hcopies = [], []
    for k in range(steps):
        at = pl.ds(k * depth, depth)
        wcopies.append(pltpu.make_async_copy(w_hbm.at[at, :], wt.at[at, :], insem.at[4 + k]))
    hload = pltpu.make_async_copy(hid_hbm, hid, hsend.at[y])
    hload.start()
    for copy in wcopies:
        copy.start()

    barrier = pltpu.get_barrier_semaphore()
    for dev in ydev[1:] + zdev[1:]:
        pl.semaphore_signal(barrier, inc=1, device_id={"sp": dev}, device_id_type=MESH)
    if halves == 2:
        pl.semaphore_signal(barrier, inc=1, device_id={"tp": partner}, device_id_type=MESH)
    for dx in range(1, nx):
        pl.semaphore_signal(barrier, inc=1, device_id={"tp": ((x + dx) % nx) * halves + core}, device_id_type=MESH)

    def dcopy(dy, arrive=False):
        there = (y + dy) % ny
        slot = there if arrive else y
        return remote(decb.at[there], ydec.at[slot], dsend.at[there], drecv.at[slot], "sp", ydev[dy])

    def ycopy(m, dy, arrive=False):
        there = (y + dy) % ny
        slot = there if arrive else y
        return remote(sbuf.at[m, there], ybuf.at[m, slot], ysend.at[m, there], yrecv.at[m, slot], "sp", ydev[dy])

    def tcopy(m, dz, arrive=False):
        there = (z + dz) % nz
        slot = there if arrive else z
        return remote(tz.at[m, there], zbuf.at[m, slot], tsend.at[m, there], trecv.at[m, slot], "sp", zdev[dz])

    def ccopy(m, dz, arrive=False):
        there = (z + dz) % nz
        slot = there if arrive else z
        return remote(cz.at[m, there], zcar.at[m, slot], csend.at[m, there], crecv.at[m, slot], "sp", zdev[dz])

    def ocopy(m, dy, arrive=False):
        there = (y + dy) % ny
        slot = there if arrive else y
        return remote(ob.at[m, there], scr.at[m, slot], osend.at[m, there], orecv.at[m, slot], "sp", ydev[dy])

    def section(k):
        return pl.ds(pl.multiple_of(k * hz, hz), hz)

    def hcopy(dy, arrive=False):
        there = (y + dy) % ny
        slot = there if arrive else y
        return remote(
            ht.at[there, section(core)], hg.at[slot, section(core)], hsend.at[there], hrecv.at[slot], "sp", ydev[dy]
        )

    def share(dy, which):
        there = (y + dy) % ny
        block = hg.at[there, section(which)]
        return remote(block, block, fsend.at[there], frecv.at[there], "tp", partner)

    def gcopy(c, dy, arrive=False):
        there = (y + dy) % ny
        slot = there if arrive else y
        return remote(gath.at[slot, c], gath.at[slot, c], gsend.at[there, c], grecv.at[slot, c], "sp", ydev[dy])

    def pair():
        return remote(ghp.at[1 - core], pland, psend, precv, "tp", partner)

    def xcopy(dx, arrive=False):
        there = (x + dx) % nx
        slot = there if arrive else x
        return remote(red.at[there], xland.at[slot], xsend.at[there], xrecv.at[slot], "tp", there * halves + core)

    def reach(c, d):
        far = nz // 2
        return far if (c + d) % 2 == 0 else nz - 1 - far

    def rcopy(c, d, j):
        target = (z + reach(c, d)) % nz if d == 0 else (z + nz - reach(c, d)) % nz
        src = part.at[c, target] if j == 0 else ring.at[d, c, j - 1]
        return remote(
            src, ring.at[d, c, j], rsend.at[d, c, j], rrecv.at[d, c, j], "sp", zdev[1] if d == 0 else zdev[nz - 1]
        )

    row_at = lax.broadcasted_iota(jnp.int32, (length, length), 0)
    col_at = lax.broadcasted_iota(jnp.int32, (length, length), 1)
    eye = (row_at == col_at).astype(BF16)
    seg = (
        lax.broadcasted_iota(jnp.int32, (heads, columns), 1) // width
        == lax.broadcasted_iota(jnp.int32, (heads, columns), 0)
    ).astype(F32)
    lane = lax.broadcasted_iota(jnp.int32, (length, LANES), 1) // width

    def tile(q):
        return slice(q * LANES, (q + 1) * LANES)

    small[0].wait()
    p = pre[...]
    rate = rate_ref[...]
    log_decay = -rate * (jnp.maximum(p, 0.0) + jnp.log1p(jnp.exp(-jnp.abs(p))))
    cum = nn((row_at >= col_at).astype(F32), log_decay, HIGH)
    cumx = nn(cum, seg, HIGH)
    totx = cumx[length - 1:length]
    decx = jnp.exp(totx)
    small[1].wait()
    small[2].wait()
    ec = jnp.exp(cumx) * cot[...].astype(F32)
    ecot[...] = ec
    qryt = nt(eye, qry[...]).astype(BF16)
    hi, lo = split(ec)
    pull = nn(qryt, hi) + nn(qryt, lo)
    for q in range(tiles):
        sbuf[0, q] = pull[:, tile(q)]
        decb[q] = jnp.broadcast_to(decx[:, tile(q)], (SUB, LANES))

    pl.semaphore_wait(barrier, ny - 1 + nz - 1 + halves - 1 + nx - 1)
    for dy in range(1, ny):
        dcopy(dy).start()
        ycopy(0, dy).start()
    ydec[y] = decb[y]
    ybuf[0, y] = sbuf[0, y]

    tend[...] = jnp.exp(totx - cumx)
    small[3].wait()
    hload.wait()
    values = jnp.zeros((length, columns), F32)
    for k in range(steps):
        wcopies[k].wait()
        values = values + nn(hid[:, k * depth:(k + 1) * depth], wt[k * depth:(k + 1) * depth, :])
    vals = values.astype(BF16)
    xv = tend[...] * vals.astype(F32)
    xval[...] = xv
    keyt = nt(eye, key[...]).astype(BF16)
    hi, lo = split(xv)
    push = nn(keyt, hi) + nn(keyt, lo)
    for q in range(tiles):
        sbuf[1, q] = push[:, tile(q)]
    for dy in range(1, ny):
        ycopy(1, dy).start()
    ybuf[1, y] = sbuf[1, y]

    for b in range(features // LANES):
        block = nt(eye, hid[:, tile(b)])
        for i in range(LANES // rows):
            owner = b * LANES // rows + i
            ht[owner % ny, owner // ny] = block[i * rows:(i + 1) * rows]
    for dy in range(1, ny):
        hcopy(dy).start()
    hcol[:, :, pl.ds(pl.multiple_of(y * length, LANES), length)] = ht[y].astype(BF16)

    def stage_y(m):
        if m == 0:
            for dy in range(1, ny):
                dcopy(dy, True).wait_recv()
        for dy in range(1, ny):
            ycopy(m, dy, True).wait_recv()
        order = list(range(ny)) if m == 1 else list(reversed(range(ny)))
        run = ybuf[m, order[0]]
        for yy in order[1:]:
            run = ydec[yy][:1] * run + ybuf[m, yy]
        prod = ydec[0]
        for yy in range(1, ny):
            prod = prod * ydec[yy]
        for k in range(nz):
            tz[m, k, :nr] = run[k * nr:(k + 1) * nr]
            tz[m, k, nr:] = prod
        for dz in range(1, nz):
            tcopy(m, dz).start()
        zbuf[m, z] = tz[m, z]

    def stage_z(m):
        for dz in range(1, nz):
            tcopy(m, dz, True).wait_recv()
        run = jnp.zeros((nr, LANES), F32)
        for zz in (list(range(nz)) if m == 1 else list(reversed(range(nz)))):
            cz[m, zz] = run
            run = zbuf[m, zz, nr:nr + 1] * run + zbuf[m, zz, :nr]
        for dz in range(1, nz):
            ccopy(m, dz).start()
        zcar[m, z] = cz[m, z]

    def stage_c(m):
        for dz in range(1, nz):
            ccopy(m, dz, True).wait_recv()
        now = zcar[m].reshape(state, LANES)
        for yy in (list(range(ny)) if m == 1 else list(reversed(range(ny)))):
            ob[m, yy] = now
            now = ydec[yy][:1] * now + ybuf[m, yy]
        for dy in range(1, ny):
            ocopy(m, dy).start()
        scr[m, y] = ob[m, y]

    stage_y(0)

    cumt = nt((
        lax.broadcasted_iota(jnp.int32, (heads, heads), 0) == lax.broadcasted_iota(jnp.int32, (heads, heads), 1)
    ).astype(F32), cum, HIGH)
    causal = row_at <= col_at
    scores = nt(key[...], qry[...])
    for q in range(tiles):
        lefts, rights = [], []
        ct = cot[:, tile(q)]
        for i in range(per):
            h = q * per + i
            across = cumt[h:h + 1, :] - cum[:, h:h + 1]
            dm = jnp.where(causal, jnp.exp(jnp.where(causal, across, 0.0)), 0.0)
            damp[h] = dm
            lefts.extend(split(scores * dm))
            masked = jnp.where(lane == i, ct, jnp.zeros_like(ct))
            rights.extend([masked, masked])
        gvloc[q] = nn(jnp.concatenate(lefts, axis=1), jnp.concatenate(rights, axis=0))

    stage_y(1)

    dsum = jnp.zeros((length, length), F32)
    for q in range(tiles):
        vt = vals[:, tile(q)]
        both = nt(
            jnp.concatenate([jnp.where(lane == i, vt, jnp.zeros_like(vt)) for i in range(per)], axis=0),
            cot[:, tile(q)],
        )
        for i in range(per):
            h = q * per + i
            ds = both[i * length:(i + 1) * length] * damp[h]
            flux = ds * scores
            dsum = dsum + ds
            rows8[h:h + 1, :] = jnp.sum(flux, axis=0, keepdims=True)
            cols8[:, h:h + 1] = jnp.sum(flux, axis=1, keepdims=True)

    stage_z(0)

    hi, lo = split(dsum)
    gkl[...] = nn(hi, qry[...]) + nn(lo, qry[...])
    hi, lo = split(dsum.T)
    gql[...] = nn(hi, key[...]) + nn(lo, key[...])
    for dy in range(1, ny):
        hcopy(dy, True).wait_recv()
        if halves == 2:
            share(dy, core).start()

    stage_z(1)
    stage_c(0)

    for dy in range(1, ny):
        there = (y + dy) % ny
        if halves == 2:
            share(dy, 1 - core).wait_recv()
        hcol[:, :, pl.ds(pl.multiple_of(there * length, LANES), length)] = hg[there].astype(BF16)

    stage_c(1)

    for dy in range(1, ny):
        ocopy(0, dy, True).wait_recv()
    for q in range(tiles):
        hi, lo = split(scr[0, q])
        kg = nn(key[...], hi) + nn(key[...], lo)
        kgs[:, tile(q)] = kg
        gb = (gvloc[q] + tend[:, tile(q)] * kg).astype(BF16)
        gvb[:, tile(q)] = gb
        gath[y, q] = gb.astype(F32)
        for dy in range(1, ny):
            gcopy(q, dy).start()

    def multiply(c):
        for dy in range(1, ny):
            gcopy(c, dy, True).wait_recv()
        block = gath[:, c].reshape(ny * length, LANES).astype(BF16)
        part[c] = nn(hcol[...].reshape(nz * rows, ny * length), block).reshape(nz, rows, LANES)
        for d in range(2):
            if reach(c, d) > 0:
                rcopy(c, d, 0).start()

    def hop(c, d, j):
        rcopy(c, d, j).wait_recv()
        left = reach(c, d) - 1 - j
        if left > 0:
            target = (z + left) % nz if d == 0 else (z + nz - left) % nz
            ring[d, c, j] = ring[d, c, j] + part[c, target]
            rcopy(c, d, j + 1).start()

    def project():
        for t in range(ntp):
            block = nt(gvb[t * own:(t + 1) * own, :], wt[...]) if own % 16 else None
            if block is not None:
                ghp[t % halves, t // halves] = block
        if own % 16 == 0:
            block = nt(gvb[...], wt[...])
            for t in range(ntp):
                ghp[t % halves, t // halves] = block[t * own:(t + 1) * own]
        if halves == 2:
            pair().start()

    def pairs():
        if halves == 2:
            pair().wait_recv()
            red[...] = ghp[core] + pland[...]
        else:
            red[...] = ghp[0]
        for dx in range(1, nx):
            xcopy(dx).start()

    def state_grads():
        for dy in range(1, ny):
            ocopy(1, dy, True).wait_recv()
        gq = gql[...]
        gk = gkl[...]
        into, pulled, through = [], [], []
        for q in range(tiles):
            si, sg = scr[1, q], scr[0, q]
            sih, sil = split(si)
            sgh, sgl = split(sg)
            eq, xq = ecot[:, tile(q)], xval[:, tile(q)]
            eh, el = split(eq)
            xh, xl = split(xq)
            gq = gq + (nt(eh, sih) + nt(el, sih) + nt(eh, sil))
            gk = gk + (nt(xh, sgh) + nt(xl, sgh) + nt(xh, sgl))
            into.append(eq * (nn(qry[...], sih) + nn(qry[...], sil)))
            pulled.append(xq * kgs[:, tile(q)])
            through.append(jnp.sum(si * sg, axis=0, keepdims=True))
        gq_ref[...] = gq.astype(BF16)
        gk_ref[...] = gk.astype(BF16)
        suffix_in = nt(jnp.concatenate(into, axis=1), seg, HIGH) - cols8[...]
        prefix_in = nt(jnp.concatenate(pulled, axis=1), seg, HIGH)
        crossing = nt(jnp.broadcast_to(decx * jnp.concatenate(through, axis=1), (SUB, columns)), seg, HIGH)[:1]
        later = (row_at <= col_at).astype(F32)
        total = (
            nn(later, suffix_in, HIGH) + nt(later, rows8[...], HIGH)
            + nn((row_at > col_at).astype(F32), prefix_in, HIGH) + crossing
        )
        gd_ref[...] = total * -rate * (1.0 / (1.0 + jnp.exp(-p)))

    tasks = [(0.0, project), (4.5, pairs), (5.5, state_grads)]
    for c in range(tiles):
        ready = 5.0 + 2.5 * c
        tasks.append((ready, functools.partial(multiply, c)))
        for d in range(2):
            for j in range(reach(c, d)):
                tasks.append((ready + 3.4 * (j + 1), functools.partial(hop, c, d, j)))
    for _, task in sorted(tasks, key=lambda item: item[0]):
        task()

    total = red[x]
    for dx in range(1, nx):
        xcopy(dx, True).wait_recv()
        total = total + xland[(x + dx) % nx]
    gh_ref[...] = total.astype(gh_ref.dtype)

    for c in range(tiles):
        total = part[c, z]
        for d in range(2):
            if reach(c, d) > 0:
                total = total + ring[d, c, reach(c, d) - 1]
        gw_ref[:, tile(c)] = total

    for dy in range(1, ny):
        dcopy(dy).wait_send()
        hcopy(dy).wait_send()
        if halves == 2:
            share(dy, core).wait_send()
        for m in range(2):
            ycopy(m, dy).wait_send()
            ocopy(m, dy).wait_send()
        for c in range(tiles):
            gcopy(c, dy).wait_send()
    for dz in range(1, nz):
        for m in range(2):
            tcopy(m, dz).wait_send()
            ccopy(m, dz).wait_send()
    for c in range(tiles):
        for d in range(2):
            for j in range(reach(c, d)):
                rcopy(c, d, j).wait_send()
    if halves == 2:
        pair().wait_send()
    for dx in range(1, nx):
        xcopy(dx).wait_send()


VM = pl.BlockSpec(memory_space=pltpu.VMEM)
ANY = pl.BlockSpec(memory_space=pl.ANY)
LIMIT = 48 * 1024 * 1024


def per_device(sp, tp, hidden, value_weight, key_vecs, queries, decay_pre, decay_rate, cotangent):
    length, features = hidden.shape
    heads = decay_rate.shape[0]
    state = key_vecs.shape[2]
    columns = value_weight.shape[1]
    ny = inner_size(sp)
    nz = sp // ny
    tiles = columns // LANES
    nr = state // nz
    rows = features // sp
    own = length // tp
    halves = 2 if tp % 2 == 0 else 1
    nx = tp // halves
    far = nz // 2
    steps = 4
    vm = pltpu.VMEM
    dma = pltpu.SemaphoreType.DMA
    gk, gq, gd, gh, gw = pl.pallas_call(
        functools.partial(mixer_kernel, ny, nz, tp),
        out_shape=(
            jax.ShapeDtypeStruct((length, state), BF16),
            jax.ShapeDtypeStruct((length, state), BF16),
            jax.ShapeDtypeStruct((length, heads), F32),
            jax.ShapeDtypeStruct((own, features), BF16),
            jax.ShapeDtypeStruct((rows, columns), F32),
        ),
        in_specs=[ANY, ANY, ANY, ANY, ANY, VM, ANY],
        out_specs=(VM,) * 5,
        scratch_shapes=[
            vm((length, features), BF16),
            vm((features, columns), BF16),
            vm((length, state), BF16),
            vm((length, state), BF16),
            vm((length, heads), F32),
            vm((length, columns), BF16),
            vm((length, columns), F32),
            vm((length, columns), F32),
            vm((length, columns), F32),
            vm((heads, length, length), F32),
            vm((tiles, length, LANES), F32),
            vm((length, columns), BF16),
            vm((length, columns), F32),
            vm((heads, length), F32),
            vm((length, heads), F32),
            vm((length, state), F32),
            vm((length, state), F32),
            vm((2, ny, state, LANES), F32),
            vm((ny, SUB, LANES), F32),
            vm((2, ny, state, LANES), F32),
            vm((ny, SUB, LANES), F32),
            vm((2, nz, nr + SUB, LANES), F32),
            vm((2, nz, nr + SUB, LANES), F32),
            vm((2, nz, nr, LANES), F32),
            vm((2, nz, nr, LANES), F32),
            vm((2, ny, state, LANES), F32),
            vm((2, ny, state, LANES), F32),
            vm((ny, nz, rows, length), F32),
            vm((ny, nz, rows, length), F32),
            vm((nz, rows, ny * length), BF16),
            vm((ny, tiles, length, LANES), F32),
            vm((tiles, nz, rows, LANES), F32),
            vm((2, tiles, far, rows, LANES), F32),
            vm((halves, nx, own, features), F32),
            vm((nx, own, features), F32),
            vm((nx, own, features), F32),
            vm((nx, own, features), F32),
            dma((4 + steps,)),
            dma((ny,)), dma((ny,)),
            dma((2, ny)), dma((2, ny)),
            dma((2, nz)), dma((2, nz)),
            dma((2, nz)), dma((2, nz)),
            dma((2, ny)), dma((2, ny)),
            dma((ny,)), dma((ny,)),
            dma((ny,)), dma((ny,)),
            dma((ny, tiles)), dma((ny, tiles)),
            dma((2, tiles, far)), dma((2, tiles, far)),
            dma, dma,
            dma((nx,)), dma((nx,)),
        ],
        compiler_params=pltpu.CompilerParams(collective_id=0, has_side_effects=True, vmem_limit_bytes=LIMIT),
        name="mixer_backward",
    )(
        hidden, value_weight, key_vecs.reshape(length, state), queries.reshape(length, state), decay_pre,
        decay_rate.reshape(1, heads), cotangent.reshape(length, columns),
    )
    return gk.reshape(key_vecs.shape), gq.reshape(key_vecs.shape), gd, gh, gw


def solution(mesh):
    return jax.shard_map(
        functools.partial(per_device, mesh.shape["sp"], mesh.shape["tp"]),
        mesh=mesh,
        in_specs=(
            P("sp", None),
            P(None, "tp"),
            P("sp", "tp", None),
            P("sp", "tp", None),
            P("sp", "tp"),
            P("tp"),
            P("sp", "tp", None),
        ),
        out_specs=(
            P("sp", "tp", None),
            P("sp", "tp", None),
            P("sp", "tp"),
            P(("sp", "tp"), None),
            P("sp", "tp"),
        ),
        check_vma=False,
    )
```

time: 105 us -> 72.6 us (0.69)
  matrix products: 21.5 us -> 0 us
  other arithmetic: 5.15 us -> 0 us
  local copies, waits for them, and re-layouts: 12.7 us -> 9.76 us
  Pallas kernels: 63.9 us -> 61.7 us
    dot_general x23 -> x0, matrix products: 21.5 us -> none  [the longest x8 7.8 us: two_pass(): jnp.einsum(spec, lo, y, preferred_element_type=F32)]
    unnamed x39 -> x16, local copies, waits for them, and re-layouts: 5 us -> 8.76 us
    convert_element_type x6 -> x0, local copies, waits for them, and re-layouts: 2.73 us -> none  [the longest x1 1.08 us: per_device(): grad_flat.astype(F32)]
    mul x4 -> x0, local copies, waits for them, and re-layouts: 2.65 us -> none  [the longest x1 1.56 us: per_device(): gk_heads * key_vecs.astype(F32)[:, :, None]]
    mul x3 -> x0, other arithmetic: 2.21 us -> none  [the longest x1 1.39 us: per_device(): gq_heads * queries.astype(F32)[:, :, None]]
    pallas_call x2 -> x1, Pallas kernels: 63.9 us -> 61.7 us  [per_device(): pl.pallas_call(functools.partial(mixer_kernel, ny, nz, tp), out_shape=(ja...]
    reduce_sum x3 -> x0, local copies, waits for them, and re-layouts: 1.94 us -> none  [the longest x1 0.93 us: per_device(): gq = two_pass('gts,sgn->tgn', dsum, key_vecs) + jnp.sum(gq_heads, axis=2)]
    transpose x1 -> x0, other arithmetic: 1.11 us -> none  [per_device(): jnp.transpose(hidden.T.astype(F32).reshape(nz, ny, rows, length), (1, 0,...]
where the time goes in v2:
time: 72.6 us; the launch traced here: 72.1 us
  Pallas kernels  61.7 us (85%)
  local copies, waits for them, and re-layouts  9.76 us (13%)
    pallas_call x1, Pallas kernels, per_device(): pl.pallas_call(functools.partial(mixer_kernel, ny, nz, tp), out_shape=(ja...  61.7 us
    unnamed x16, local copies, waits for them, and re-layouts  8.76 us

profile of v2, /device:TPU:2, one launch (start us, length us, event | category | flops | bytes accessed | tf_op | source)
XLA Modules:
  0.0 72.1 jit_solution(15579837475902902040)
XLA Ops:
  0.6 0.8 %copy.15.pre_hbm = f32[128,8]{1,0:T(8,128)S(1)} copy(f32[128,8]{0,1:T(8,128)} %param.11) | data formatting | bytes 8192 | tf_op args[4]
  1.4 1.0 %copy.16.cot_hbm = bf16[128,512]{1,0:T(8,128)(2,1)S(1)} copy(bf16[128,512]{0,1:T(8,128)(2,1)} %bitcast.11) | data formatting | bytes 262144 | tf_op jit(solution)/shard_map/reshape | solution.py:547
  2.4 0.0 copy-start
  2.4 1.6 %copy-done = bf16[2048,512]{1,0:T(8,128)(2,1)S(1)} copy-done((bf16[2048,512]{1,0:T(8,128)(2,1)S(1)}, bf16[2048,512]{1,0:T(8,128)(2,1)}, u32[]{:S(2)}) %copy-start) | copy-done | bytes 2097176
  4.0 0.0 copy-start.1
  4.0 1.0 %copy-done.1 = bf16[128,2048]{1,0:T(8,128)(2,1)S(1)} copy-done((bf16[128,2048]{1,0:T(8,128)(2,1)S(1)}, bf16[128,2048]{1,0:T(8,128)(2,1)}, u32[]{:S(2)}) %copy-start.1) | copy-done | bytes 524312
  5.1 0.0 copy-start.2
  5.1 0.8 %copy-done.2 = bf16[128,1,128]{2,0,1:T(8,128)(2,1)S(1)} copy-done((bf16[128,1,128]{2,0,1:T(8,128)(2,1)S(1)}, bf16[128,1,128]{2,0,1:T(8,128)(2,1)}, u32[]{:S(2)}) %copy-start.2) | copy-done | bytes 32792
  5.8 0.0 copy-start.3
  5.8 0.8 %copy-done.3 = bf16[128,1,128]{2,0,1:T(8,128)(2,1)S(1)} copy-done((bf16[128,1,128]{2,0,1:T(8,128)(2,1)S(1)}, bf16[128,1,128]{2,0,1:T(8,128)(2,1)}, u32[]{:S(2)}) %copy-start.3) | copy-done | bytes 32792
  6.6 0.0 copy-start.4
  6.6 0.7 copy-done.4
  7.2 61.7 %mixer_backward.1 = (bf16[128,128]{1,0:T(8,128)(2,1)S(1)}, bf16[128,128]{1,0:T(8,128)(2,1)S(1)}, f32[128,8]{1,0:T(8,128)S(1)}, bf16[16,2048]{1,0:T(8,128)(2,1)S(1)}, f32[64,512]{1,0:T(8,128)S(1)}) custom-call(bf16[128,2048]{1,0:T(8,128)(2,1)S(1)} %copy-done.1, bf16[2048,512]{1,0:T(8,128)(2,1)S(1)} %copy-done, bf16[128,128]{1,0:T(8,128)(2,1)S(1)} %bitcast.6, ...), custom_call_target="tpu_custom_call" | custom-call | tf_op jit(solution)/shard_map/mixer_backward/pallas_call | solution.py:481
  68.9 0.7 copy.17
  69.6 0.6 copy.22
  70.2 0.6 copy.23
  70.8 0.6 copy.24
  71.5 0.7 copy.25
Async XLA Ops:
  2.4 1.6 %copy-start = (bf16[2048,512]{1,0:T(8,128)(2,1)S(1)}, bf16[2048,512]{1,0:T(8,128)(2,1)}, u32[]{:S(2)}) copy-start(bf16[2048,512]{1,0:T(8,128)(2,1)} %w_hbm.1) | copy-start | bytes 6291460
  4.0 1.0 %copy-start.1 = (bf16[128,2048]{1,0:T(8,128)(2,1)S(1)}, bf16[128,2048]{1,0:T(8,128)(2,1)}, u32[]{:S(2)}) copy-start(bf16[128,2048]{1,0:T(8,128)(2,1)} %hid_hbm.1) | copy-start | bytes 1572868
  5.1 0.8 %copy-start.2 = (bf16[128,1,128]{2,0,1:T(8,128)(2,1)S(1)}, bf16[128,1,128]{2,0,1:T(8,128)(2,1)}, u32[]{:S(2)}) copy-start(bf16[128,1,128]{2,0,1:T(8,128)(2,1)} %param.9) | copy-start | bytes 98308
  5.8 0.8 %copy-start.3 = (bf16[128,1,128]{2,0,1:T(8,128)(2,1)S(1)}, bf16[128,1,128]{2,0,1:T(8,128)(2,1)}, u32[]{:S(2)}) copy-start(bf16[128,1,128]{2,0,1:T(8,128)(2,1)} %param.10) | copy-start | bytes 98308
  6.6 0.7 copy-start.4

commit v3 on v2

--- a/solution.py
+++ b/solution.py
@@ -43,19 +43,19 @@
     return hi, (x - hi.astype(F32)).astype(BF16)
 
 
-def mixer_kernel(ny, nz, ntp, hid_hbm, w_hbm, key_hbm, qry_hbm, pre_hbm, rate_ref, cot_hbm,
-                 gk_ref, gq_ref, gd_ref, gh_ref, gw_ref,
-                 hid, wt, key, qry, pre, cot,
+def mixer_kernel(ny, nz, ntp, hid_hbm, w_hbm, key_hbm, qry_hbm, pre_hbm, rate_hbm, cot_hbm,
+                 gk_out, gq_out, gd_out, gh_out, gw_out,
+                 gk_ref, gq_ref, gd_ref, gh_ref, gw_ref, hid, wt, key, qry, pre, rate_ref, cott, cot,
                  ecot, tend, xval, damp, gvloc, gvb, kgs, rows8, cols8, gkl, gql,
                  sbuf, decb, ybuf, ydec, tz, zbuf, cz, zcar, ob, scr, ht, hg, hcol,
                  gath, part, ring, ghp, pland, red, xland,
                  insem, dsend, drecv, ysend, yrecv, tsend, trecv, csend, crecv, osend, orecv,
-                 hsend, hrecv, fsend, frecv, gsend, grecv, rsend, rrecv, psend, precv, xsend, xrecv):
+                 hsend, hrecv, fsend, frecv, gsend, grecv, rsend, rrecv, psend, precv, xsend, xrecv, outsem):
     me = lax.axis_index("sp")
     mine = lax.axis_index("tp")
     z, y = me // ny, me % ny
     length, features = hid.shape
-    heads = rate_ref.shape[1]
+    heads = pre.shape[0]
     columns = cot.shape[1]
     width = columns // heads
     tiles = columns // LANES
@@ -67,21 +67,22 @@
     halves = 2 if ntp % 2 == 0 else 1
     core, x, nx = mine % halves, mine // halves, ntp // halves
     partner = mine + 1 - 2 * core
-    hz = nz // halves
-    steps = insem.shape[0] - 4
+    hz = nz // ntp
+    steps = insem.shape[0] - 5
     depth = features // steps
     ydev = [z * ny + (y + dy) % ny for dy in range(ny)]
     zdev = [((z + dz) % nz) * ny + y for dz in range(nz)]
 
     small = [
         pltpu.make_async_copy(pre_hbm, pre, insem.at[0]),
+        pltpu.make_async_copy(rate_hbm, rate_ref, insem.at[4 + steps]),
         pltpu.make_async_copy(qry_hbm, qry, insem.at[1]),
-        pltpu.make_async_copy(cot_hbm, cot, insem.at[2]),
+        pltpu.make_async_copy(cot_hbm, cott, insem.at[2]),
         pltpu.make_async_copy(key_hbm, key, insem.at[3]),
     ]
     for copy in small:
         copy.start()
-    wcopies, hcopies = [], []
+    wcopies = []
     for k in range(steps):
         at = pl.ds(k * depth, depth)
         wcopies.append(pltpu.make_async_copy(w_hbm.at[at, :], wt.at[at, :], insem.at[4 + k]))
@@ -90,13 +91,21 @@
     for copy in wcopies:
         copy.start()
 
+    outs = [
+        pltpu.make_async_copy(gk_ref, gk_out, outsem.at[0]),
+        pltpu.make_async_copy(gq_ref, gq_out, outsem.at[1]),
+        pltpu.make_async_copy(gd_ref, gd_out, outsem.at[2]),
+        pltpu.make_async_copy(gh_ref, gh_out, outsem.at[3]),
+    ]
+    for c in range(tiles):
+        at = pl.ds(c * LANES, LANES)
+        outs.append(pltpu.make_async_copy(gw_ref.at[:, at], gw_out.at[:, at], outsem.at[4 + c]))
+
     barrier = pltpu.get_barrier_semaphore()
     for dev in ydev[1:] + zdev[1:]:
         pl.semaphore_signal(barrier, inc=1, device_id={"sp": dev}, device_id_type=MESH)
-    if halves == 2:
-        pl.semaphore_signal(barrier, inc=1, device_id={"tp": partner}, device_id_type=MESH)
-    for dx in range(1, nx):
-        pl.semaphore_signal(barrier, inc=1, device_id={"tp": ((x + dx) % nx) * halves + core}, device_id_type=MESH)
+    for dt in range(1, ntp):
+        pl.semaphore_signal(barrier, inc=1, device_id={"tp": (mine + dt) % ntp}, device_id_type=MESH)
 
     def dcopy(dy, arrive=False):
         there = (y + dy) % ny
@@ -130,19 +139,31 @@
         there = (y + dy) % ny
         slot = there if arrive else y
         return remote(
-            ht.at[there, section(core)], hg.at[slot, section(core)], hsend.at[there], hrecv.at[slot], "sp", ydev[dy]
+            ht.at[there, section(mine)], hg.at[slot, section(mine)], hsend.at[there], hrecv.at[slot], "sp", ydev[dy]
         )
 
-    def share(dy, which):
+    def share(dy, dt, arrive=False):
         there = (y + dy) % ny
+        peer = (mine + dt) % ntp
+        which = peer if arrive else mine
         block = hg.at[there, section(which)]
-        return remote(block, block, fsend.at[there], frecv.at[there], "tp", partner)
+        return remote(block, block, fsend.at[there, peer], frecv.at[there, which], "tp", peer)
 
     def gcopy(c, dy, arrive=False):
         there = (y + dy) % ny
         slot = there if arrive else y
         return remote(gath.at[slot, c], gath.at[slot, c], gsend.at[there, c], grecv.at[slot, c], "sp", ydev[dy])
 
+    relayed = ny == 4
+
+    def near(c):
+        return ny - 1 if c % 2 == 0 else 1
+
+    def fcopy(c):
+        to = ny - near(c)
+        block = gath.at[(y + near(c)) % ny, c]
+        return remote(block, block, gsend.at[(y + 2) % ny, c], grecv.at[(y + near(c)) % ny, c], "sp", ydev[to])
+
     def pair():
         return remote(ghp.at[1 - core], pland, psend, precv, "tp", partner)
 
@@ -155,12 +176,38 @@
         far = nz // 2
         return far if (c + d) % 2 == 0 else nz - 1 - far
 
+    def fast(c):
+        return nz == 8 and c >= tiles - 2
+
+    def ahead(k, d):
+        return (z + k) % nz if d == 0 else (z + nz - k) % nz
+
     def rcopy(c, d, j):
-        target = (z + reach(c, d)) % nz if d == 0 else (z + nz - reach(c, d)) % nz
-        src = part.at[c, target] if j == 0 else ring.at[d, c, j - 1]
+        src = part.at[c, ahead(reach(c, d), d)] if j == 0 else ring.at[d, c, j - 1]
         return remote(
             src, ring.at[d, c, j], rsend.at[d, c, j], rrecv.at[d, c, j], "sp", zdev[1] if d == 0 else zdev[nz - 1]
         )
+
+    def scopy(c, d, j):
+        if j == 0:
+            src, hops = part.at[c, ahead(4, d)], 2
+        elif j == 1:
+            src, hops = part.at[c, ahead(3, d)], 2
+        elif j == 2:
+            src, hops = (ring.at[d, c, 0] if reach(c, d) == 4 else part.at[c, ahead(2, d)]), 2
+        else:
+            src, hops = ring.at[d, c, 1], 1
+        return remote(
+            src, ring.at[d, c, j], rsend.at[d, c, j], rrecv.at[d, c, j], "sp", zdev[hops if d == 0 else nz - hops]
+        )
+
+    def slots(c, d):
+        if fast(c):
+            return (0, 1, 2, 3) if reach(c, d) == 4 else (1, 2, 3)
+        return tuple(range(reach(c, d)))
+
+    def sent(c, d, j):
+        return scopy(c, d, j) if fast(c) else rcopy(c, d, j)
 
     row_at = lax.broadcasted_iota(jnp.int32, (length, length), 0)
     col_at = lax.broadcasted_iota(jnp.int32, (length, length), 1)
@@ -174,16 +221,24 @@
     def tile(q):
         return slice(q * LANES, (q + 1) * LANES)
 
+    same = (
+        lax.broadcasted_iota(jnp.int32, (heads, heads), 0) == lax.broadcasted_iota(jnp.int32, (heads, heads), 1)
+    ).astype(F32)
     small[0].wait()
+    small[1].wait()
     p = pre[...]
-    rate = rate_ref[...]
+    rate = nt(same, jnp.broadcast_to(rate_ref[...], (heads, heads)), HIGH)[:, :1]
     log_decay = -rate * (jnp.maximum(p, 0.0) + jnp.log1p(jnp.exp(-jnp.abs(p))))
-    cum = nn((row_at >= col_at).astype(F32), log_decay, HIGH)
+    lower = (row_at >= col_at).astype(F32)
+    cum = nt(lower, log_decay, HIGH)
+    cumt = nt(log_decay, lower, HIGH)
     cumx = nn(cum, seg, HIGH)
     totx = cumx[length - 1:length]
     decx = jnp.exp(totx)
-    small[1].wait()
     small[2].wait()
+    small[3].wait()
+    for q in range(tiles):
+        cot[:, tile(q)] = nt(eye, cott[tile(q), :]).astype(BF16)
     ec = jnp.exp(cumx) * cot[...].astype(F32)
     ecot[...] = ec
     qryt = nt(eye, qry[...]).astype(BF16)
@@ -193,7 +248,8 @@
         sbuf[0, q] = pull[:, tile(q)]
         decb[q] = jnp.broadcast_to(decx[:, tile(q)], (SUB, LANES))
 
-    pl.semaphore_wait(barrier, ny - 1 + nz - 1 + halves - 1 + nx - 1)
+    with jax.named_scope("barrier"):
+        pl.semaphore_wait(barrier, ny - 1 + nz - 1 + ntp - 1)
     for dy in range(1, ny):
         dcopy(dy).start()
         ycopy(0, dy).start()
@@ -201,7 +257,7 @@
     ybuf[0, y] = sbuf[0, y]
 
     tend[...] = jnp.exp(totx - cumx)
-    small[3].wait()
+    small[4].wait()
     hload.wait()
     values = jnp.zeros((length, columns), F32)
     for k in range(steps):
@@ -215,8 +271,9 @@
     push = nn(keyt, hi) + nn(keyt, lo)
     for q in range(tiles):
         sbuf[1, q] = push[:, tile(q)]
-    for dy in range(1, ny):
-        ycopy(1, dy).start()
+    with jax.named_scope("send_y1"):
+        for dy in range(1, ny):
+            ycopy(1, dy).start()
     ybuf[1, y] = sbuf[1, y]
 
     for b in range(features // LANES):
@@ -224,8 +281,9 @@
         for i in range(LANES // rows):
             owner = b * LANES // rows + i
             ht[owner % ny, owner // ny] = block[i * rows:(i + 1) * rows]
-    for dy in range(1, ny):
-        hcopy(dy).start()
+    with jax.named_scope("send_h"):
+        for dy in range(1, ny):
+            hcopy(dy).start()
     hcol[:, :, pl.ds(pl.multiple_of(y * length, LANES), length)] = ht[y].astype(BF16)
 
     def stage_y(m):
@@ -270,11 +328,9 @@
             ocopy(m, dy).start()
         scr[m, y] = ob[m, y]
 
-    stage_y(0)
-
-    cumt = nt((
-        lax.broadcasted_iota(jnp.int32, (heads, heads), 0) == lax.broadcasted_iota(jnp.int32, (heads, heads), 1)
-    ).astype(F32), cum, HIGH)
+    with jax.named_scope("stage_y0"):
+        stage_y(0)
+
     causal = row_at <= col_at
     scores = nt(key[...], qry[...])
     for q in range(tiles):
@@ -290,7 +346,11 @@
             rights.extend([masked, masked])
         gvloc[q] = nn(jnp.concatenate(lefts, axis=1), jnp.concatenate(rights, axis=0))
 
-    stage_y(1)
+    with jax.named_scope("stage_z0"):
+        stage_z(0)
+
+    with jax.named_scope("stage_y1"):
+        stage_y(1)
 
     dsum = jnp.zeros((length, length), F32)
     for q in range(tiles):
@@ -307,30 +367,28 @@
             rows8[h:h + 1, :] = jnp.sum(flux, axis=0, keepdims=True)
             cols8[:, h:h + 1] = jnp.sum(flux, axis=1, keepdims=True)
 
-    stage_z(0)
+    with jax.named_scope("hid_y"):
+        for dy in range(1, ny):
+            hcopy(dy, True).wait_recv()
+            for dt in range(1, ntp):
+                share(dy, dt).start()
+
+    with jax.named_scope("stage_c0"):
+        stage_c(0)
 
     hi, lo = split(dsum)
     gkl[...] = nn(hi, qry[...]) + nn(lo, qry[...])
     hi, lo = split(dsum.T)
     gql[...] = nn(hi, key[...]) + nn(lo, key[...])
-    for dy in range(1, ny):
-        hcopy(dy, True).wait_recv()
-        if halves == 2:
-            share(dy, core).start()
-
-    stage_z(1)
-    stage_c(0)
-
-    for dy in range(1, ny):
-        there = (y + dy) % ny
-        if halves == 2:
-            share(dy, 1 - core).wait_recv()
-        hcol[:, :, pl.ds(pl.multiple_of(there * length, LANES), length)] = hg[there].astype(BF16)
-
-    stage_c(1)
-
-    for dy in range(1, ny):
-        ocopy(0, dy, True).wait_recv()
+    with jax.named_scope("stage_z1"):
+        stage_z(1)
+
+    with jax.named_scope("stage_c1"):
+        stage_c(1)
+
+    with jax.named_scope("wait_o0"):
+        for dy in range(1, ny):
+            ocopy(0, dy, True).wait_recv()
     for q in range(tiles):
         hi, lo = split(scr[0, q])
         kg = nn(key[...], hi) + nn(key[...], lo)
@@ -339,34 +397,61 @@
         gvb[:, tile(q)] = gb
         gath[y, q] = gb.astype(F32)
         for dy in range(1, ny):
-            gcopy(q, dy).start()
+            if not (relayed and dy == 2):
+                gcopy(q, dy).start()
+
+    def columns_in():
+        for dy in range(1, ny):
+            there = (y + dy) % ny
+            for dt in range(1, ntp):
+                share(dy, dt, True).wait_recv()
+            hcol[:, :, pl.ds(pl.multiple_of(there * length, LANES), length)] = hg[there].astype(BF16)
+
+    def relay(c):
+        gcopy(c, near(c), True).wait_recv()
+        fcopy(c).start()
 
     def multiply(c):
         for dy in range(1, ny):
-            gcopy(c, dy, True).wait_recv()
+            if not (relayed and dy == near(c)):
+                gcopy(c, dy, True).wait_recv()
         block = gath[:, c].reshape(ny * length, LANES).astype(BF16)
         part[c] = nn(hcol[...].reshape(nz * rows, ny * length), block).reshape(nz, rows, LANES)
         for d in range(2):
-            if reach(c, d) > 0:
+            if fast(c):
+                for j in slots(c, d):
+                    if j < 2 or (j == 2 and reach(c, d) == 3):
+                        scopy(c, d, j).start()
+            elif reach(c, d) > 0:
                 rcopy(c, d, 0).start()
 
     def hop(c, d, j):
         rcopy(c, d, j).wait_recv()
         left = reach(c, d) - 1 - j
         if left > 0:
-            target = (z + left) % nz if d == 0 else (z + nz - left) % nz
-            ring[d, c, j] = ring[d, c, j] + part[c, target]
+            ring[d, c, j] = ring[d, c, j] + part[c, ahead(left, d)]
             rcopy(c, d, j + 1).start()
 
+    def step(c, d, j):
+        scopy(c, d, j).wait_recv()
+        if j < 2:
+            ring[d, c, j] = ring[d, c, j] + part[c, ahead(2 - j, d)]
+            scopy(c, d, j + 2).start()
+
+    def total_weight(c):
+        total = part[c, z]
+        for d in range(2):
+            if fast(c):
+                total = total + (ring[d, c, 2] + ring[d, c, 3])
+            elif reach(c, d) > 0:
+                total = total + ring[d, c, reach(c, d) - 1]
+        gw_ref[:, tile(c)] = total
+        outs[4 + c].start()
+
     def project():
+        block = nt(gvb[...], wt[...])
         for t in range(ntp):
-            block = nt(gvb[t * own:(t + 1) * own, :], wt[...]) if own % 16 else None
-            if block is not None:
-                ghp[t % halves, t // halves] = block
-        if own % 16 == 0:
-            block = nt(gvb[...], wt[...])
-            for t in range(ntp):
-                ghp[t % halves, t // halves] = block[t * own:(t + 1) * own]
+            ghp[t % halves, t // halves] = block[t * own:(t + 1) * own]
         if halves == 2:
             pair().start()
 
@@ -380,8 +465,9 @@
             xcopy(dx).start()
 
     def state_grads():
-        for dy in range(1, ny):
-            ocopy(1, dy, True).wait_recv()
+        with jax.named_scope("wait_o1"):
+            for dy in range(1, ny):
+                ocopy(1, dy, True).wait_recv()
         gq = gql[...]
         gk = gkl[...]
         into, pulled, through = [], [], []
@@ -399,66 +485,90 @@
             through.append(jnp.sum(si * sg, axis=0, keepdims=True))
         gq_ref[...] = gq.astype(BF16)
         gk_ref[...] = gk.astype(BF16)
-        suffix_in = nt(jnp.concatenate(into, axis=1), seg, HIGH) - cols8[...]
-        prefix_in = nt(jnp.concatenate(pulled, axis=1), seg, HIGH)
-        crossing = nt(jnp.broadcast_to(decx * jnp.concatenate(through, axis=1), (SUB, columns)), seg, HIGH)[:1]
-        later = (row_at <= col_at).astype(F32)
+        suffix_in = nt(seg, jnp.concatenate(into, axis=1), HIGH) - nt(same, cols8[...], HIGH) + rows8[...]
+        prefix_in = nt(seg, jnp.concatenate(pulled, axis=1), HIGH)
+        crossing = nt(seg, jnp.broadcast_to(decx * jnp.concatenate(through, axis=1), (SUB, columns)), HIGH)[:, :1]
         total = (
-            nn(later, suffix_in, HIGH) + nt(later, rows8[...], HIGH)
-            + nn((row_at > col_at).astype(F32), prefix_in, HIGH) + crossing
+            nn(suffix_in, lower, HIGH) + nn(prefix_in, (row_at < col_at).astype(F32), HIGH) + crossing
         )
         gd_ref[...] = total * -rate * (1.0 / (1.0 + jnp.exp(-p)))
-
-    tasks = [(0.0, project), (4.5, pairs), (5.5, state_grads)]
+        for copy in outs[:3]:
+            copy.start()
+
+    def total_hidden():
+        total = red[x]
+        for dx in range(1, nx):
+            xcopy(dx, True).wait_recv()
+            total = total + xland[(x + dx) % nx]
+        gh_ref[...] = total.astype(gh_ref.dtype)
+        outs[3].start()
+
+    tasks = [
+        (0.0, "project", project), (1.0, "columns_in", columns_in), (9.0, "pairs", pairs),
+        (3.0, "state_grads", state_grads), (18.0, "total_hidden", total_hidden),
+    ]
     for c in range(tiles):
-        ready = 5.0 + 2.5 * c
-        tasks.append((ready, functools.partial(multiply, c)))
+        ready = 5.0 + 2.2 * c
+        if relayed:
+            tasks.append((ready - 2.0, f"relay{c}", functools.partial(relay, c)))
+        tasks.append((ready, f"multiply{c}", functools.partial(multiply, c)))
+        last = ready
         for d in range(2):
-            for j in range(reach(c, d)):
-                tasks.append((ready + 3.4 * (j + 1), functools.partial(hop, c, d, j)))
-    for _, task in sorted(tasks, key=lambda item: item[0]):
-        task()
-
-    total = red[x]
-    for dx in range(1, nx):
-        xcopy(dx, True).wait_recv()
-        total = total + xland[(x + dx) % nx]
-    gh_ref[...] = total.astype(gh_ref.dtype)
-
-    for c in range(tiles):
-        total = part[c, z]
-        for d in range(2):
-            if reach(c, d) > 0:
-                total = total + ring[d, c, reach(c, d) - 1]
-        gw_ref[:, tile(c)] = total
+            for j in slots(c, d):
+                if fast(c):
+                    at = ready + (3.6 if j < 2 else 7.2) + 0.2 * (j % 2)
+                    tasks.append((at, f"step{c}{d}{j}", functools.partial(step, c, d, j)))
+                else:
+                    at = ready + 2.7 * (j + 1)
+                    tasks.append((at, f"hop{c}{d}{j}", functools.partial(hop, c, d, j)))
+                last = max(last, at)
+        tasks.append((last + 0.01, f"total{c}", functools.partial(total_weight, c)))
+    for _, name, task in sorted(tasks, key=lambda item: item[0]):
+        with jax.named_scope(name):
+            task()
 
     for dy in range(1, ny):
         dcopy(dy).wait_send()
         hcopy(dy).wait_send()
-        if halves == 2:
-            share(dy, core).wait_send()
+        for dt in range(1, ntp):
+            share(dy, dt).wait_send()
         for m in range(2):
             ycopy(m, dy).wait_send()
             ocopy(m, dy).wait_send()
         for c in range(tiles):
-            gcopy(c, dy).wait_send()
+            (fcopy(c) if relayed and dy == 2 else gcopy(c, dy)).wait_send()
     for dz in range(1, nz):
         for m in range(2):
             tcopy(m, dz).wait_send()
             ccopy(m, dz).wait_send()
     for c in range(tiles):
         for d in range(2):
-            for j in range(reach(c, d)):
-                rcopy(c, d, j).wait_send()
+            for j in slots(c, d):
+                sent(c, d, j).wait_send()
     if halves == 2:
         pair().wait_send()
     for dx in range(1, nx):
         xcopy(dx).wait_send()
-
-
-VM = pl.BlockSpec(memory_space=pltpu.VMEM)
-ANY = pl.BlockSpec(memory_space=pl.ANY)
-LIMIT = 48 * 1024 * 1024
+    for copy in outs:
+        copy.wait()
+
+
+def finish_kernel(*refs):
+    count = (len(refs) - 1) // 3
+    ins, outs, held, sems = refs[:count], refs[count:2 * count], refs[2 * count:3 * count], refs[-1]
+    loads = [pltpu.make_async_copy(ins[k], held[k], sems.at[0, k]) for k in range(count)]
+    stores = [pltpu.make_async_copy(held[k], outs[k], sems.at[1, k]) for k in range(count)]
+    for load in loads:
+        load.start()
+    for load, store in zip(loads, stores):
+        load.wait()
+        store.start()
+    for store in stores:
+        store.wait()
+
+
+HBM = pl.BlockSpec(memory_space=pltpu.HBM)
+LIMIT = 60 * 1024 * 1024
 
 
 def per_device(sp, tp, hidden, value_weight, key_vecs, queries, decay_pre, decay_rate, cotangent):
@@ -478,23 +588,30 @@
     steps = 4
     vm = pltpu.VMEM
     dma = pltpu.SemaphoreType.DMA
-    gk, gq, gd, gh, gw = pl.pallas_call(
+    outs = pl.pallas_call(
         functools.partial(mixer_kernel, ny, nz, tp),
         out_shape=(
             jax.ShapeDtypeStruct((length, state), BF16),
             jax.ShapeDtypeStruct((length, state), BF16),
-            jax.ShapeDtypeStruct((length, heads), F32),
+            jax.ShapeDtypeStruct((heads, length), F32),
             jax.ShapeDtypeStruct((own, features), BF16),
             jax.ShapeDtypeStruct((rows, columns), F32),
         ),
-        in_specs=[ANY, ANY, ANY, ANY, ANY, VM, ANY],
-        out_specs=(VM,) * 5,
+        in_specs=[HBM] * 7,
+        out_specs=(HBM,) * 5,
         scratch_shapes=[
+            vm((length, state), BF16),
+            vm((length, state), BF16),
+            vm((heads, length), F32),
+            vm((own, features), BF16),
+            vm((rows, columns), F32),
             vm((length, features), BF16),
             vm((features, columns), BF16),
             vm((length, state), BF16),
             vm((length, state), BF16),
-            vm((length, heads), F32),
+            vm((heads, length), F32),
+            vm((1, heads), F32),
+            vm((columns, length), BF16),
             vm((length, columns), BF16),
             vm((length, columns), F32),
             vm((length, columns), F32),
@@ -527,26 +644,36 @@
             vm((nx, own, features), F32),
             vm((nx, own, features), F32),
             vm((nx, own, features), F32),
-            dma((4 + steps,)),
+            dma((5 + steps,)),
             dma((ny,)), dma((ny,)),
             dma((2, ny)), dma((2, ny)),
             dma((2, nz)), dma((2, nz)),
             dma((2, nz)), dma((2, nz)),
             dma((2, ny)), dma((2, ny)),
             dma((ny,)), dma((ny,)),
-            dma((ny,)), dma((ny,)),
+            dma((ny, tp)), dma((ny, tp)),
             dma((ny, tiles)), dma((ny, tiles)),
             dma((2, tiles, far)), dma((2, tiles, far)),
             dma, dma,
             dma((nx,)), dma((nx,)),
+            dma((4 + tiles,)),
         ],
         compiler_params=pltpu.CompilerParams(collective_id=0, has_side_effects=True, vmem_limit_bytes=LIMIT),
         name="mixer_backward",
     )(
-        hidden, value_weight, key_vecs.reshape(length, state), queries.reshape(length, state), decay_pre,
-        decay_rate.reshape(1, heads), cotangent.reshape(length, columns),
+        hidden, value_weight, key_vecs.reshape(length, state), queries.reshape(length, state), decay_pre.T,
+        decay_rate.reshape(1, heads), cotangent.reshape(length, columns).T,
     )
-    return gk.reshape(key_vecs.shape), gq.reshape(key_vecs.shape), gd, gh, gw
+    gk, gq, gd, gh, gw = pl.pallas_call(
+        finish_kernel,
+        out_shape=tuple(jax.ShapeDtypeStruct(o.shape, o.dtype) for o in outs),
+        in_specs=[HBM] * 5,
+        out_specs=(HBM,) * 5,
+        scratch_shapes=[vm(o.shape, o.dtype) for o in outs] + [dma((2, 5))],
+        compiler_params=pltpu.CompilerParams(vmem_limit_bytes=LIMIT),
+        name="write_out",
+    )(*outs)
+    return gk.reshape(key_vecs.shape), gq.reshape(key_vecs.shape), gd.T, gh, gw
 
 
 def solution(mesh):

time: 72.6 us -> 68.1 us (0.938)
  local copies, waits for them, and re-layouts: 9.76 us -> 0 us
  Pallas kernels: 61.7 us -> 67.3 us
    unnamed x16 -> x0, local copies, waits for them, and re-layouts: 8.76 us -> none
    pallas_call x1, Pallas kernels: 61.7 us -> 65.6 us  [per_device(): pl.pallas_call(functools.partial(mixer_kernel, ny, nz, tp), out_shape=(ja...]
    pallas_call x0 -> x1, Pallas kernels: none -> 1.72 us  [per_device(): pl.pallas_call(finish_kernel, out_shape=tuple((jax.ShapeDtypeStruct(o.sha...]
    reshape x1 -> x0, local copies, waits for them, and re-layouts: 1 us -> none  [per_device(): cotangent.reshape(length, columns)]
where the time goes in v3:
time: 68.1 us; the launch traced here: 67.9 us
  Pallas kernels  67.3 us (99%)
    pallas_call x1, Pallas kernels, per_device(): pl.pallas_call(functools.partial(mixer_kernel, ny, nz, tp), out_shape=(ja...  65.6 us
    pallas_call x1, Pallas kernels, per_device(): pl.pallas_call(finish_kernel, out_shape=tuple((jax.ShapeDtypeStruct(o.sha...  1.72 us

profile of v3, /device:TPU:2, one launch (start us, length us, event | category | flops | bytes accessed | tf_op | source)
XLA Modules:
  0.0 67.9 jit_solution(1297947503172042008)
XLA Ops:
  0.6 65.6 %mixer_backward.1 = (bf16[128,128]{1,0:T(8,128)(2,1)}, bf16[128,128]{1,0:T(8,128)(2,1)}, f32[8,128]{1,0:T(8,128)}, bf16[16,2048]{1,0:T(8,128)(2,1)}, f32[64,512]{1,0:T(8,128)}) custom-call(bf16[128,2048]{1,0:T(8,128)(2,1)} %hid_hbm.1, bf16[2048,512]{1,0:T(8,128)(2,1)} %w_hbm.1, bf16[128,128]{1,0:T(8,128)(2,1)} %bitcast.11, bf16[128,128]{1,0:T(8,128)(2,1)} %bitcast.12, ...), custom_call_target="tpu_custom_call" | custom-call | tf_op jit(solution)/shard_map/mixer_backward/pallas_call | solution.py:591
  66.2 1.7 %write_out.1 = (bf16[128,128]{1,0:T(8,128)(2,1)}, bf16[128,128]{1,0:T(8,128)(2,1)}, f32[8,128]{1,0:T(8,128)}, bf16[16,2048]{1,0:T(8,128)(2,1)}, f32[64,512]{1,0:T(8,128)}) custom-call(bf16[128,128]{1,0:T(8,128)(2,1)} %get-tuple-element.15.refs_0_, bf16[128,128]{1,0:T(8,128)(2,1)} %get-tuple-element.16.refs_1_, f32[8,128]{1,0:T(8,128)} %get-tuple-element.17.refs_2_, ...), custom_call_target="tpu_custom_call" | custom-call | tf_op jit(solution)/shard_map/write_out/pallas_call | solution.py:667

commit v4 on v3

--- a/solution.py
+++ b/solution.py
@@ -49,7 +49,7 @@
                  ecot, tend, xval, damp, gvloc, gvb, kgs, rows8, cols8, gkl, gql,
                  sbuf, decb, ybuf, ydec, tz, zbuf, cz, zcar, ob, scr, ht, hg, hcol,
                  gath, part, ring, ghp, pland, red, xland,
-                 insem, dsend, drecv, ysend, yrecv, tsend, trecv, csend, crecv, osend, orecv,
+                 insem, wsem, dsend, drecv, ysend, yrecv, tsend, trecv, csend, crecv, osend, orecv,
                  hsend, hrecv, fsend, frecv, gsend, grecv, rsend, rrecv, psend, precv, xsend, xrecv, outsem):
     me = lax.axis_index("sp")
     mine = lax.axis_index("tp")
@@ -68,14 +68,14 @@
     core, x, nx = mine % halves, mine // halves, ntp // halves
     partner = mine + 1 - 2 * core
     hz = nz // ntp
-    steps = insem.shape[0] - 5
+    steps = wsem.shape[0]
     depth = features // steps
     ydev = [z * ny + (y + dy) % ny for dy in range(ny)]
     zdev = [((z + dz) % nz) * ny + y for dz in range(nz)]
 
     small = [
         pltpu.make_async_copy(pre_hbm, pre, insem.at[0]),
-        pltpu.make_async_copy(rate_hbm, rate_ref, insem.at[4 + steps]),
+        pltpu.make_async_copy(rate_hbm, rate_ref, insem.at[4]),
         pltpu.make_async_copy(qry_hbm, qry, insem.at[1]),
         pltpu.make_async_copy(cot_hbm, cott, insem.at[2]),
         pltpu.make_async_copy(key_hbm, key, insem.at[3]),
@@ -85,8 +85,8 @@
     wcopies = []
     for k in range(steps):
         at = pl.ds(k * depth, depth)
-        wcopies.append(pltpu.make_async_copy(w_hbm.at[at, :], wt.at[at, :], insem.at[4 + k]))
-    hload = pltpu.make_async_copy(hid_hbm, hid, hsend.at[y])
+        wcopies.append(pltpu.make_async_copy(w_hbm.at[at, :], wt.at[at, :], wsem.at[k]))
+    hload = pltpu.make_async_copy(hid_hbm, hid, insem.at[5])
     hload.start()
     for copy in wcopies:
         copy.start()
@@ -99,7 +99,7 @@
     ]
     for c in range(tiles):
         at = pl.ds(c * LANES, LANES)
-        outs.append(pltpu.make_async_copy(gw_ref.at[:, at], gw_out.at[:, at], outsem.at[4 + c]))
+        outs.append(pltpu.make_async_copy(gw_ref.at[:, at], gw_out.at[:, at], outsem.at[4]))
 
     barrier = pltpu.get_barrier_semaphore()
     for dev in ydev[1:] + zdev[1:]:
@@ -110,27 +110,27 @@
     def dcopy(dy, arrive=False):
         there = (y + dy) % ny
         slot = there if arrive else y
-        return remote(decb.at[there], ydec.at[slot], dsend.at[there], drecv.at[slot], "sp", ydev[dy])
+        return remote(decb.at[there], ydec.at[slot], dsend, drecv, "sp", ydev[dy])
 
     def ycopy(m, dy, arrive=False):
         there = (y + dy) % ny
         slot = there if arrive else y
-        return remote(sbuf.at[m, there], ybuf.at[m, slot], ysend.at[m, there], yrecv.at[m, slot], "sp", ydev[dy])
+        return remote(sbuf.at[m, there], ybuf.at[m, slot], ysend.at[m], yrecv.at[m], "sp", ydev[dy])
 
     def tcopy(m, dz, arrive=False):
         there = (z + dz) % nz
         slot = there if arrive else z
-        return remote(tz.at[m, there], zbuf.at[m, slot], tsend.at[m, there], trecv.at[m, slot], "sp", zdev[dz])
+        return remote(tz.at[m, there], zbuf.at[m, slot], tsend.at[m], trecv.at[m], "sp", zdev[dz])
 
     def ccopy(m, dz, arrive=False):
         there = (z + dz) % nz
         slot = there if arrive else z
-        return remote(cz.at[m, there], zcar.at[m, slot], csend.at[m, there], crecv.at[m, slot], "sp", zdev[dz])
+        return remote(cz.at[m, there], zcar.at[m, slot], csend.at[m], crecv.at[m], "sp", zdev[dz])
 
     def ocopy(m, dy, arrive=False):
         there = (y + dy) % ny
         slot = there if arrive else y
-        return remote(ob.at[m, there], scr.at[m, slot], osend.at[m, there], orecv.at[m, slot], "sp", ydev[dy])
+        return remote(ob.at[m, there], scr.at[m, slot], osend.at[m], orecv.at[m], "sp", ydev[dy])
 
     def section(k):
         return pl.ds(pl.multiple_of(k * hz, hz), hz)
@@ -139,7 +139,7 @@
         there = (y + dy) % ny
         slot = there if arrive else y
         return remote(
-            ht.at[there, section(mine)], hg.at[slot, section(mine)], hsend.at[there], hrecv.at[slot], "sp", ydev[dy]
+            ht.at[there, section(mine)], hg.at[slot, section(mine)], hsend, hrecv, "sp", ydev[dy]
         )
 
     def share(dy, dt, arrive=False):
@@ -147,22 +147,12 @@
         peer = (mine + dt) % ntp
         which = peer if arrive else mine
         block = hg.at[there, section(which)]
-        return remote(block, block, fsend.at[there, peer], frecv.at[there, which], "tp", peer)
+        return remote(block, block, fsend, frecv, "tp", peer)
 
     def gcopy(c, dy, arrive=False):
         there = (y + dy) % ny
         slot = there if arrive else y
-        return remote(gath.at[slot, c], gath.at[slot, c], gsend.at[there, c], grecv.at[slot, c], "sp", ydev[dy])
-
-    relayed = ny == 4
-
-    def near(c):
-        return ny - 1 if c % 2 == 0 else 1
-
-    def fcopy(c):
-        to = ny - near(c)
-        block = gath.at[(y + near(c)) % ny, c]
-        return remote(block, block, gsend.at[(y + 2) % ny, c], grecv.at[(y + near(c)) % ny, c], "sp", ydev[to])
+        return remote(gath.at[slot, c], gath.at[slot, c], gsend, grecv.at[c], "sp", ydev[dy])
 
     def pair():
         return remote(ghp.at[1 - core], pland, psend, precv, "tp", partner)
@@ -170,7 +160,7 @@
     def xcopy(dx, arrive=False):
         there = (x + dx) % nx
         slot = there if arrive else x
-        return remote(red.at[there], xland.at[slot], xsend.at[there], xrecv.at[slot], "tp", there * halves + core)
+        return remote(red.at[there], xland.at[slot], xsend, xrecv, "tp", there * halves + core)
 
     def reach(c, d):
         far = nz // 2
@@ -185,7 +175,7 @@
     def rcopy(c, d, j):
         src = part.at[c, ahead(reach(c, d), d)] if j == 0 else ring.at[d, c, j - 1]
         return remote(
-            src, ring.at[d, c, j], rsend.at[d, c, j], rrecv.at[d, c, j], "sp", zdev[1] if d == 0 else zdev[nz - 1]
+            src, ring.at[d, c, j], rsend, rrecv.at[slot_at(c, d, j)], "sp", zdev[1] if d == 0 else zdev[nz - 1]
         )
 
     def scopy(c, d, j):
@@ -198,7 +188,7 @@
         else:
             src, hops = ring.at[d, c, 1], 1
         return remote(
-            src, ring.at[d, c, j], rsend.at[d, c, j], rrecv.at[d, c, j], "sp", zdev[hops if d == 0 else nz - hops]
+            src, ring.at[d, c, j], rsend, rrecv.at[slot_at(c, d, j)], "sp", zdev[hops if d == 0 else nz - hops]
         )
 
     def slots(c, d):
@@ -206,8 +196,13 @@
             return (0, 1, 2, 3) if reach(c, d) == 4 else (1, 2, 3)
         return tuple(range(reach(c, d)))
 
-    def sent(c, d, j):
-        return scopy(c, d, j) if fast(c) else rcopy(c, d, j)
+    ring_slots = sorted({(c, d, min(j, 2) if fast(c) else j) for c in range(tiles) for d in range(2) for j in slots(c, d)})
+
+    def slot_at(c, d, j):
+        return ring_slots.index((c, d, min(j, 2) if fast(c) else j))
+
+    def bulk(ref, send, recv):
+        return remote(ref, ref, send, recv, "sp", ydev[1])
 
     row_at = lax.broadcasted_iota(jnp.int32, (length, length), 0)
     col_at = lax.broadcasted_iota(jnp.int32, (length, length), 1)
@@ -256,9 +251,17 @@
     ydec[y] = decb[y]
     ybuf[0, y] = sbuf[0, y]
 
+    hload.wait()
+    for b in range(features // LANES):
+        block = nt(eye, hid[:, tile(b)])
+        for i in range(LANES // rows):
+            owner = b * LANES // rows + i
+            ht[owner % ny, owner // ny] = block[i * rows:(i + 1) * rows]
+    with jax.named_scope("send_h"):
+        for dy in range(1, ny):
+            hcopy(dy).start()
     tend[...] = jnp.exp(totx - cumx)
     small[4].wait()
-    hload.wait()
     values = jnp.zeros((length, columns), F32)
     for k in range(steps):
         wcopies[k].wait()
@@ -276,22 +279,12 @@
             ycopy(1, dy).start()
     ybuf[1, y] = sbuf[1, y]
 
-    for b in range(features // LANES):
-        block = nt(eye, hid[:, tile(b)])
-        for i in range(LANES // rows):
-            owner = b * LANES // rows + i
-            ht[owner % ny, owner // ny] = block[i * rows:(i + 1) * rows]
-    with jax.named_scope("send_h"):
-        for dy in range(1, ny):
-            hcopy(dy).start()
     hcol[:, :, pl.ds(pl.multiple_of(y * length, LANES), length)] = ht[y].astype(BF16)
 
     def stage_y(m):
         if m == 0:
-            for dy in range(1, ny):
-                dcopy(dy, True).wait_recv()
-        for dy in range(1, ny):
-            ycopy(m, dy, True).wait_recv()
+            bulk(ydec.at[:ny - 1], dsend, drecv).wait_recv()
+        bulk(ybuf.at[m, :ny - 1], ysend.at[m], yrecv.at[m]).wait_recv()
         order = list(range(ny)) if m == 1 else list(reversed(range(ny)))
         run = ybuf[m, order[0]]
         for yy in order[1:]:
@@ -307,8 +300,7 @@
         zbuf[m, z] = tz[m, z]
 
     def stage_z(m):
-        for dz in range(1, nz):
-            tcopy(m, dz, True).wait_recv()
+        bulk(zbuf.at[m, :nz - 1], tsend.at[m], trecv.at[m]).wait_recv()
         run = jnp.zeros((nr, LANES), F32)
         for zz in (list(range(nz)) if m == 1 else list(reversed(range(nz)))):
             cz[m, zz] = run
@@ -318,8 +310,7 @@
         zcar[m, z] = cz[m, z]
 
     def stage_c(m):
-        for dz in range(1, nz):
-            ccopy(m, dz, True).wait_recv()
+        bulk(zcar.at[m, :nz - 1], csend.at[m], crecv.at[m]).wait_recv()
         now = zcar[m].reshape(state, LANES)
         for yy in (list(range(ny)) if m == 1 else list(reversed(range(ny)))):
             ob[m, yy] = now
@@ -346,6 +337,12 @@
             rights.extend([masked, masked])
         gvloc[q] = nn(jnp.concatenate(lefts, axis=1), jnp.concatenate(rights, axis=0))
 
+    with jax.named_scope("hid_y"):
+        bulk(hg.at[:ny - 1, :hz], hsend, hrecv).wait_recv()
+        for dt in range(1, ntp):
+            for dy in range(1, ny):
+                share(dy, dt).start()
+
     with jax.named_scope("stage_z0"):
         stage_z(0)
 
@@ -367,12 +364,6 @@
             rows8[h:h + 1, :] = jnp.sum(flux, axis=0, keepdims=True)
             cols8[:, h:h + 1] = jnp.sum(flux, axis=1, keepdims=True)
 
-    with jax.named_scope("hid_y"):
-        for dy in range(1, ny):
-            hcopy(dy, True).wait_recv()
-            for dt in range(1, ntp):
-                share(dy, dt).start()
-
     with jax.named_scope("stage_c0"):
         stage_c(0)
 
@@ -383,12 +374,8 @@
     with jax.named_scope("stage_z1"):
         stage_z(1)
 
-    with jax.named_scope("stage_c1"):
-        stage_c(1)
-
     with jax.named_scope("wait_o0"):
-        for dy in range(1, ny):
-            ocopy(0, dy, True).wait_recv()
+        bulk(scr.at[0, :ny - 1], osend.at[0], orecv.at[0]).wait_recv()
     for q in range(tiles):
         hi, lo = split(scr[0, q])
         kg = nn(key[...], hi) + nn(key[...], lo)
@@ -396,25 +383,18 @@
         gb = (gvloc[q] + tend[:, tile(q)] * kg).astype(BF16)
         gvb[:, tile(q)] = gb
         gath[y, q] = gb.astype(F32)
-        for dy in range(1, ny):
-            if not (relayed and dy == 2):
-                gcopy(q, dy).start()
+        for dy in sorted(range(1, ny), key=lambda dy: -min(dy, ny - dy)):
+            gcopy(q, dy).start()
 
     def columns_in():
+        if ntp > 1:
+            bulk(hg.at[:ny - 1, :nz - hz], fsend, frecv).wait_recv()
         for dy in range(1, ny):
             there = (y + dy) % ny
-            for dt in range(1, ntp):
-                share(dy, dt, True).wait_recv()
             hcol[:, :, pl.ds(pl.multiple_of(there * length, LANES), length)] = hg[there].astype(BF16)
 
-    def relay(c):
-        gcopy(c, near(c), True).wait_recv()
-        fcopy(c).start()
-
     def multiply(c):
-        for dy in range(1, ny):
-            if not (relayed and dy == near(c)):
-                gcopy(c, dy, True).wait_recv()
+        bulk(gath.at[:ny - 1, c], gsend, grecv.at[c]).wait_recv()
         block = gath[:, c].reshape(ny * length, LANES).astype(BF16)
         part[c] = nn(hcol[...].reshape(nz * rows, ny * length), block).reshape(nz, rows, LANES)
         for d in range(2):
@@ -433,8 +413,10 @@
             rcopy(c, d, j + 1).start()
 
     def step(c, d, j):
-        scopy(c, d, j).wait_recv()
-        if j < 2:
+        if j == 2:
+            bulk(ring.at[d, c, 2:4], rsend, rrecv.at[slot_at(c, d, 2)]).wait_recv()
+        else:
+            scopy(c, d, j).wait_recv()
             ring[d, c, j] = ring[d, c, j] + part[c, ahead(2 - j, d)]
             scopy(c, d, j + 2).start()
 
@@ -466,8 +448,7 @@
 
     def state_grads():
         with jax.named_scope("wait_o1"):
-            for dy in range(1, ny):
-                ocopy(1, dy, True).wait_recv()
+            bulk(scr.at[1, :ny - 1], osend.at[1], orecv.at[1]).wait_recv()
         gq = gql[...]
         gk = gkl[...]
         into, pulled, through = [], [], []
@@ -497,24 +478,41 @@
 
     def total_hidden():
         total = red[x]
+        if nx > 1:
+            bulk(xland.at[:nx - 1], xsend, xrecv).wait_recv()
         for dx in range(1, nx):
-            xcopy(dx, True).wait_recv()
             total = total + xland[(x + dx) % nx]
         gh_ref[...] = total.astype(gh_ref.dtype)
         outs[3].start()
 
+    def drain():
+        bulk(decb.at[:ny - 1], dsend, drecv).wait_send()
+        bulk(ht.at[:ny - 1, :hz], hsend, hrecv).wait_send()
+        if ntp > 1:
+            bulk(hg.at[:ny - 1, :nz - hz], fsend, frecv).wait_send()
+        for m in range(2):
+            bulk(sbuf.at[m, :ny - 1], ysend.at[m], yrecv.at[m]).wait_send()
+            bulk(tz.at[m, :nz - 1], tsend.at[m], trecv.at[m]).wait_send()
+            bulk(cz.at[m, :nz - 1], csend.at[m], crecv.at[m]).wait_send()
+            bulk(ob.at[m, :ny - 1], osend.at[m], orecv.at[m]).wait_send()
+        bulk(gath.at[:ny - 1], gsend, grecv.at[0]).wait_send()
+        if halves == 2:
+            pair().wait_send()
+
     tasks = [
-        (0.0, "project", project), (1.0, "columns_in", columns_in), (9.0, "pairs", pairs),
-        (3.0, "state_grads", state_grads), (18.0, "total_hidden", total_hidden),
+        (0.0, "project", project), (0.9, "columns_in", columns_in), (1.0, "stage_c1", functools.partial(stage_c, 1)),
+        (7.2, "pairs", pairs), (13.0, "state_grads", state_grads), (15.0, "drain", drain),
+        (18.2, "total_hidden", total_hidden),
     ]
+    arrive = (6.5, 8.0, 10.5, 12.0)
     for c in range(tiles):
-        ready = 5.0 + 2.2 * c
-        if relayed:
-            tasks.append((ready - 2.0, f"relay{c}", functools.partial(relay, c)))
+        ready = arrive[c % 4] + 7.0 * (c // 4)
         tasks.append((ready, f"multiply{c}", functools.partial(multiply, c)))
         last = ready
         for d in range(2):
             for j in slots(c, d):
+                if fast(c) and j == 3:
+                    continue
                 if fast(c):
                     at = ready + (3.6 if j < 2 else 7.2) + 0.2 * (j % 2)
                     tasks.append((at, f"step{c}{d}{j}", functools.partial(step, c, d, j)))
@@ -527,30 +525,14 @@
         with jax.named_scope(name):
             task()
 
-    for dy in range(1, ny):
-        dcopy(dy).wait_send()
-        hcopy(dy).wait_send()
-        for dt in range(1, ntp):
-            share(dy, dt).wait_send()
-        for m in range(2):
-            ycopy(m, dy).wait_send()
-            ocopy(m, dy).wait_send()
-        for c in range(tiles):
-            (fcopy(c) if relayed and dy == 2 else gcopy(c, dy)).wait_send()
-    for dz in range(1, nz):
-        for m in range(2):
-            tcopy(m, dz).wait_send()
-            ccopy(m, dz).wait_send()
-    for c in range(tiles):
-        for d in range(2):
-            for j in slots(c, d):
-                sent(c, d, j).wait_send()
-    if halves == 2:
-        pair().wait_send()
-    for dx in range(1, nx):
-        xcopy(dx).wait_send()
-    for copy in outs:
-        copy.wait()
+    with jax.named_scope("drain_ring"):
+        bulk(part.at[:, :nz - 1], rsend, rrecv.at[0]).wait_send()
+        if nx > 1:
+            bulk(red.at[:nx - 1], xsend, xrecv).wait_send()
+    with jax.named_scope("outs"):
+        for copy in outs[:4]:
+            copy.wait()
+        pltpu.make_async_copy(gw_ref, gw_out, outsem.at[4]).wait()
 
 
 def finish_kernel(*refs):
@@ -585,7 +567,7 @@
     halves = 2 if tp % 2 == 0 else 1
     nx = tp // halves
     far = nz // 2
-    steps = 4
+    steps = 2
     vm = pltpu.VMEM
     dma = pltpu.SemaphoreType.DMA
     outs = pl.pallas_call(
@@ -644,19 +626,19 @@
             vm((nx, own, features), F32),
             vm((nx, own, features), F32),
             vm((nx, own, features), F32),
-            dma((5 + steps,)),
-            dma((ny,)), dma((ny,)),
-            dma((2, ny)), dma((2, ny)),
-            dma((2, nz)), dma((2, nz)),
-            dma((2, nz)), dma((2, nz)),
-            dma((2, ny)), dma((2, ny)),
-            dma((ny,)), dma((ny,)),
-            dma((ny, tp)), dma((ny, tp)),
-            dma((ny, tiles)), dma((ny, tiles)),
-            dma((2, tiles, far)), dma((2, tiles, far)),
+            dma((6,)), dma((steps,)),
             dma, dma,
-            dma((nx,)), dma((nx,)),
-            dma((4 + tiles,)),
+            dma((2,)), dma((2,)),
+            dma((2,)), dma((2,)),
+            dma((2,)), dma((2,)),
+            dma((2,)), dma((2,)),
+            dma, dma,
+            dma, dma,
+            dma, dma((tiles,)),
+            dma, dma((tiles * (nz - 1) - (4 if nz == 8 else 0),)),
+            dma, dma,
+            dma, dma,
+            dma((5,)),
         ],
         compiler_params=pltpu.CompilerParams(collective_id=0, has_side_effects=True, vmem_limit_bytes=LIMIT),
         name="mixer_backward",

time: 68.1 us -> 57.6 us (0.85); the launches traced: 67.9 us -> 56.8 us
  Pallas kernels: 67.3 us -> 56.1 us
    pallas_call x1, Pallas kernels: 65.6 us -> 54.4 us  [per_device(): pl.pallas_call(functools.partial(mixer_kernel, ny, nz, tp), out_shape=(ja...]
where the time goes in v4:
time: 57.6 us; the launch traced here: 56.8 us
  Pallas kernels  56.1 us (97%)
  between operations  0.64 us (1%)
    pallas_call x1, Pallas kernels, per_device(): pl.pallas_call(functools.partial(mixer_kernel, ny, nz, tp), out_shape=(ja...  54.4 us
    pallas_call x1, Pallas kernels, per_device(): pl.pallas_call(finish_kernel, out_shape=tuple((jax.ShapeDtypeStruct(o.sha...  1.72 us

profile of v4, /device:TPU:2, one launch (start us, length us, event | category | flops | bytes accessed | tf_op | source)
XLA Modules:
  0.0 56.8 jit_solution(8916882979484515276)
XLA Ops:
  0.6 54.4 %mixer_backward.1 = (bf16[128,128]{1,0:T(8,128)(2,1)}, bf16[128,128]{1,0:T(8,128)(2,1)}, f32[8,128]{1,0:T(8,128)}, bf16[16,2048]{1,0:T(8,128)(2,1)}, f32[64,512]{1,0:T(8,128)}) custom-call(bf16[128,2048]{1,0:T(8,128)(2,1)} %hid_hbm.1, bf16[2048,512]{1,0:T(8,128)(2,1)} %w_hbm.1, bf16[128,128]{1,0:T(8,128)(2,1)} %bitcast.11, bf16[128,128]{1,0:T(8,128)(2,1)} %bitcast.12, ...), custom_call_target="tpu_custom_call" | custom-call | tf_op jit(solution)/shard_map/mixer_backward/pallas_call | solution.py:573
  55.0 1.7 %write_out.1 = (bf16[128,128]{1,0:T(8,128)(2,1)}, bf16[128,128]{1,0:T(8,128)(2,1)}, f32[8,128]{1,0:T(8,128)}, bf16[16,2048]{1,0:T(8,128)(2,1)}, f32[64,512]{1,0:T(8,128)}) custom-call(bf16[128,128]{1,0:T(8,128)(2,1)} %get-tuple-element.15.refs_0_, bf16[128,128]{1,0:T(8,128)(2,1)} %get-tuple-element.16.refs_1_, f32[8,128]{1,0:T(8,128)} %get-tuple-element.17.refs_2_, ...), custom_call_target="tpu_custom_call" | custom-call | tf_op jit(solution)/shard_map/write_out/pallas_call | solution.py:649

commit v5 on v4

--- a/solution.py
+++ b/solution.py
@@ -61,7 +61,10 @@
     tiles = columns // LANES
     per = LANES // width
     state = key.shape[1]
-    nr = state // nz
+    groups = sbuf.shape[1]
+    pack = tiles // groups
+    rw = state // ny
+    pr = pack * rw // nz
     rows = gw_ref.shape[0]
     own = gh_ref.shape[0]
     halves = 2 if ntp % 2 == 0 else 1
@@ -108,29 +111,24 @@
         pl.semaphore_signal(barrier, inc=1, device_id={"tp": (mine + dt) % ntp}, device_id_type=MESH)
 
     def dcopy(dy, arrive=False):
+        slot = (y + dy) % ny if arrive else y
+        return remote(decb, ydec.at[slot], dsend, drecv, "sp", ydev[dy])
+
+    def ycopy(m, g, dy):
         there = (y + dy) % ny
-        slot = there if arrive else y
-        return remote(decb.at[there], ydec.at[slot], dsend, drecv, "sp", ydev[dy])
-
-    def ycopy(m, dy, arrive=False):
+        return remote(sbuf.at[m, g, there], ybuf.at[m, g, y], ysend, yrecv.at[m, g], "sp", ydev[dy])
+
+    def tcopy(m, g, dz):
+        there = (z + dz) % nz
+        return remote(tz.at[m, g, there], zbuf.at[m, g, z], tsend, trecv.at[m, g], "sp", zdev[dz])
+
+    def ccopy(m, g, dz):
+        there = (z + dz) % nz
+        return remote(cz.at[m, g, there], zcar.at[m, g, z], csend, crecv.at[m, g], "sp", zdev[dz])
+
+    def ocopy(m, g, dy):
         there = (y + dy) % ny
-        slot = there if arrive else y
-        return remote(sbuf.at[m, there], ybuf.at[m, slot], ysend.at[m], yrecv.at[m], "sp", ydev[dy])
-
-    def tcopy(m, dz, arrive=False):
-        there = (z + dz) % nz
-        slot = there if arrive else z
-        return remote(tz.at[m, there], zbuf.at[m, slot], tsend.at[m], trecv.at[m], "sp", zdev[dz])
-
-    def ccopy(m, dz, arrive=False):
-        there = (z + dz) % nz
-        slot = there if arrive else z
-        return remote(cz.at[m, there], zcar.at[m, slot], csend.at[m], crecv.at[m], "sp", zdev[dz])
-
-    def ocopy(m, dy, arrive=False):
-        there = (y + dy) % ny
-        slot = there if arrive else y
-        return remote(ob.at[m, there], scr.at[m, slot], osend.at[m], orecv.at[m], "sp", ydev[dy])
+        return remote(ob.at[m, g, there], scr.at[m, g, y], osend, orecv.at[m, g], "sp", ydev[dy])
 
     def section(k):
         return pl.ds(pl.multiple_of(k * hz, hz), hz)
@@ -239,17 +237,25 @@
     qryt = nt(eye, qry[...]).astype(BF16)
     hi, lo = split(ec)
     pull = nn(qryt, hi) + nn(qryt, lo)
+    def spread(m, whole):
+        for g in range(groups):
+            for yy in range(ny):
+                for i in range(pack):
+                    sbuf[m, g, yy, i * rw:(i + 1) * rw] = whole[yy * rw:(yy + 1) * rw, tile(g * pack + i)]
+
+    spread(0, pull)
     for q in range(tiles):
-        sbuf[0, q] = pull[:, tile(q)]
-        decb[q] = jnp.broadcast_to(decx[:, tile(q)], (SUB, LANES))
+        decb[q:q + 1, :] = decx[:, tile(q)]
 
     with jax.named_scope("barrier"):
         pl.semaphore_wait(barrier, ny - 1 + nz - 1 + ntp - 1)
     for dy in range(1, ny):
         dcopy(dy).start()
-        ycopy(0, dy).start()
-    ydec[y] = decb[y]
-    ybuf[0, y] = sbuf[0, y]
+    for g in range(groups):
+        for dy in range(1, ny):
+            ycopy(0, g, dy).start()
+    ydec[y] = decb[...]
+    ybuf[0, :, y] = sbuf[0, :, y]
 
     hload.wait()
     for b in range(features // LANES):
@@ -272,55 +278,72 @@
     keyt = nt(eye, key[...]).astype(BF16)
     hi, lo = split(xv)
     push = nn(keyt, hi) + nn(keyt, lo)
-    for q in range(tiles):
-        sbuf[1, q] = push[:, tile(q)]
+    spread(1, push)
     with jax.named_scope("send_y1"):
-        for dy in range(1, ny):
-            ycopy(1, dy).start()
-    ybuf[1, y] = sbuf[1, y]
+        for g in range(groups):
+            for dy in range(1, ny):
+                ycopy(1, g, dy).start()
+    ybuf[1, :, y] = sbuf[1, :, y]
 
     hcol[:, :, pl.ds(pl.multiple_of(y * length, LANES), length)] = ht[y].astype(BF16)
 
-    def stage_y(m):
-        if m == 0:
+    def scan_order(m, count):
+        return list(range(count)) if m == 1 else list(reversed(range(count)))
+
+    def stage_y(m, g):
+        if m == 0 and g == 0:
             bulk(ydec.at[:ny - 1], dsend, drecv).wait_recv()
-        bulk(ybuf.at[m, :ny - 1], ysend.at[m], yrecv.at[m]).wait_recv()
-        order = list(range(ny)) if m == 1 else list(reversed(range(ny)))
-        run = ybuf[m, order[0]]
-        for yy in order[1:]:
-            run = ydec[yy][:1] * run + ybuf[m, yy]
-        prod = ydec[0]
-        for yy in range(1, ny):
-            prod = prod * ydec[yy]
-        for k in range(nz):
-            tz[m, k, :nr] = run[k * nr:(k + 1) * nr]
-            tz[m, k, nr:] = prod
-        for dz in range(1, nz):
-            tcopy(m, dz).start()
-        zbuf[m, z] = tz[m, z]
-
-    def stage_z(m):
-        bulk(zbuf.at[m, :nz - 1], tsend.at[m], trecv.at[m]).wait_recv()
-        run = jnp.zeros((nr, LANES), F32)
-        for zz in (list(range(nz)) if m == 1 else list(reversed(range(nz)))):
-            cz[m, zz] = run
-            run = zbuf[m, zz, nr:nr + 1] * run + zbuf[m, zz, :nr]
-        for dz in range(1, nz):
-            ccopy(m, dz).start()
-        zcar[m, z] = cz[m, z]
-
-    def stage_c(m):
-        bulk(zcar.at[m, :nz - 1], csend.at[m], crecv.at[m]).wait_recv()
-        now = zcar[m].reshape(state, LANES)
-        for yy in (list(range(ny)) if m == 1 else list(reversed(range(ny)))):
-            ob[m, yy] = now
-            now = ydec[yy][:1] * now + ybuf[m, yy]
-        for dy in range(1, ny):
-            ocopy(m, dy).start()
-        scr[m, y] = ob[m, y]
-
-    with jax.named_scope("stage_y0"):
-        stage_y(0)
+        bulk(ybuf.at[m, g, :ny - 1], ysend, yrecv.at[m, g]).wait_recv()
+        order = scan_order(m, ny)
+        for i in range(pack):
+            q, at = g * pack + i, slice(i * rw, (i + 1) * rw)
+            run = ybuf[m, g, order[0], at]
+            for yy in order[1:]:
+                run = ydec[yy, q:q + 1] * run + ybuf[m, g, yy, at]
+            prod = ydec[0, q:q + 1]
+            for yy in range(1, ny):
+                prod = prod * ydec[yy, q:q + 1]
+            prod = jnp.broadcast_to(prod, (SUB, LANES))
+            for k in range(rw // pr):
+                tz[m, g, i * (rw // pr) + k, :pr] = run[k * pr:(k + 1) * pr]
+                tz[m, g, i * (rw // pr) + k, pr:] = prod
+        for dz in sorted(range(1, nz), key=lambda dz: -min(dz, nz - dz)):
+            tcopy(m, g, dz).start()
+        zbuf[m, g, z] = tz[m, g, z]
+
+    def stage_z(m, g):
+        bulk(zbuf.at[m, g, :nz - 1], tsend, trecv.at[m, g]).wait_recv()
+        run = jnp.zeros((pr, LANES), F32)
+        for zz in scan_order(m, nz):
+            cz[m, g, zz] = run
+            run = zbuf[m, g, zz, pr:pr + 1] * run + zbuf[m, g, zz, :pr]
+        for dz in sorted(range(1, nz), key=lambda dz: -min(dz, nz - dz)):
+            ccopy(m, g, dz).start()
+        zcar[m, g, z] = cz[m, g, z]
+
+    def stage_c(m, g):
+        bulk(zcar.at[m, g, :nz - 1], csend, crecv.at[m, g]).wait_recv()
+        carry = zcar[m, g].reshape(pack * rw, LANES)
+        for i in range(pack):
+            q, at = g * pack + i, slice(i * rw, (i + 1) * rw)
+            now = carry[at]
+            for yy in scan_order(m, ny):
+                ob[m, g, yy, at] = now
+                now = ydec[yy, q:q + 1] * now + ybuf[m, g, yy, at]
+        for dy in sorted(range(1, ny), key=lambda dy: -min(dy, ny - dy)):
+            ocopy(m, g, dy).start()
+        scr[m, g, y] = ob[m, g, y]
+
+    def stage(name, work, m):
+        for g in range(groups):
+            with jax.named_scope(f"{name}{m}{g}"):
+                work(m, g)
+
+    def state_tile(m, q):
+        g, i = q // pack, q % pack
+        return scr[m, g, :, i * rw:(i + 1) * rw].reshape(state, LANES)
+
+    stage("stage_y", stage_y, 0)
 
     causal = row_at <= col_at
     scores = nt(key[...], qry[...])
@@ -343,11 +366,9 @@
             for dy in range(1, ny):
                 share(dy, dt).start()
 
-    with jax.named_scope("stage_z0"):
-        stage_z(0)
-
-    with jax.named_scope("stage_y1"):
-        stage_y(1)
+    stage("stage_z", stage_z, 0)
+
+    stage("stage_y", stage_y, 1)
 
     dsum = jnp.zeros((length, length), F32)
     for q in range(tiles):
@@ -364,27 +385,26 @@
             rows8[h:h + 1, :] = jnp.sum(flux, axis=0, keepdims=True)
             cols8[:, h:h + 1] = jnp.sum(flux, axis=1, keepdims=True)
 
-    with jax.named_scope("stage_c0"):
-        stage_c(0)
+    stage("stage_c", stage_c, 0)
 
     hi, lo = split(dsum)
     gkl[...] = nn(hi, qry[...]) + nn(lo, qry[...])
     hi, lo = split(dsum.T)
     gql[...] = nn(hi, key[...]) + nn(lo, key[...])
-    with jax.named_scope("stage_z1"):
-        stage_z(1)
-
-    with jax.named_scope("wait_o0"):
-        bulk(scr.at[0, :ny - 1], osend.at[0], orecv.at[0]).wait_recv()
-    for q in range(tiles):
-        hi, lo = split(scr[0, q])
-        kg = nn(key[...], hi) + nn(key[...], lo)
-        kgs[:, tile(q)] = kg
-        gb = (gvloc[q] + tend[:, tile(q)] * kg).astype(BF16)
-        gvb[:, tile(q)] = gb
-        gath[y, q] = gb.astype(F32)
-        for dy in sorted(range(1, ny), key=lambda dy: -min(dy, ny - dy)):
-            gcopy(q, dy).start()
+    stage("stage_z", stage_z, 1)
+
+    for g in range(groups):
+        with jax.named_scope(f"wait_o0{g}"):
+            bulk(scr.at[0, g, :ny - 1], osend, orecv.at[0, g]).wait_recv()
+        for q in range(g * pack, (g + 1) * pack):
+            hi, lo = split(state_tile(0, q))
+            kg = nn(key[...], hi) + nn(key[...], lo)
+            kgs[:, tile(q)] = kg
+            gb = (gvloc[q] + tend[:, tile(q)] * kg).astype(BF16)
+            gvb[:, tile(q)] = gb
+            gath[y, q] = gb.astype(F32)
+            for dy in sorted(range(1, ny), key=lambda dy: -min(dy, ny - dy)):
+                gcopy(q, dy).start()
 
     def columns_in():
         if ntp > 1:
@@ -446,35 +466,41 @@
         for dx in range(1, nx):
             xcopy(dx).start()
 
-    def state_grads():
+    def key_grads():
+        gk = gkl[...]
+        pulled = []
+        for q in range(tiles):
+            sgh, sgl = split(state_tile(0, q))
+            xq = xval[:, tile(q)]
+            xh, xl = split(xq)
+            gk = gk + (nt(xh, sgh) + nt(xl, sgh) + nt(xh, sgl))
+            pulled.append(xq * kgs[:, tile(q)])
+        gk_ref[...] = gk.astype(BF16)
+        outs[0].start()
+        prefix_in = nt(seg, jnp.concatenate(pulled, axis=1), HIGH)
+        gd_ref[...] = nn(prefix_in, (row_at < col_at).astype(F32), HIGH)
+
+    def query_grads():
         with jax.named_scope("wait_o1"):
-            bulk(scr.at[1, :ny - 1], osend.at[1], orecv.at[1]).wait_recv()
+            for g in range(groups):
+                bulk(scr.at[1, g, :ny - 1], osend, orecv.at[1, g]).wait_recv()
         gq = gql[...]
-        gk = gkl[...]
-        into, pulled, through = [], [], []
+        into, through = [], []
         for q in range(tiles):
-            si, sg = scr[1, q], scr[0, q]
+            si, sg = state_tile(1, q), state_tile(0, q)
             sih, sil = split(si)
-            sgh, sgl = split(sg)
-            eq, xq = ecot[:, tile(q)], xval[:, tile(q)]
+            eq = ecot[:, tile(q)]
             eh, el = split(eq)
-            xh, xl = split(xq)
             gq = gq + (nt(eh, sih) + nt(el, sih) + nt(eh, sil))
-            gk = gk + (nt(xh, sgh) + nt(xl, sgh) + nt(xh, sgl))
             into.append(eq * (nn(qry[...], sih) + nn(qry[...], sil)))
-            pulled.append(xq * kgs[:, tile(q)])
             through.append(jnp.sum(si * sg, axis=0, keepdims=True))
         gq_ref[...] = gq.astype(BF16)
-        gk_ref[...] = gk.astype(BF16)
+        outs[1].start()
         suffix_in = nt(seg, jnp.concatenate(into, axis=1), HIGH) - nt(same, cols8[...], HIGH) + rows8[...]
-        prefix_in = nt(seg, jnp.concatenate(pulled, axis=1), HIGH)
         crossing = nt(seg, jnp.broadcast_to(decx * jnp.concatenate(through, axis=1), (SUB, columns)), HIGH)[:, :1]
-        total = (
-            nn(suffix_in, lower, HIGH) + nn(prefix_in, (row_at < col_at).astype(F32), HIGH) + crossing
-        )
+        total = nn(suffix_in, lower, HIGH) + gd_ref[...] + crossing
         gd_ref[...] = total * -rate * (1.0 / (1.0 + jnp.exp(-p)))
-        for copy in outs[:3]:
-            copy.start()
+        outs[2].start()
 
     def total_hidden():
         total = red[x]
@@ -486,25 +512,25 @@
         outs[3].start()
 
     def drain():
-        bulk(decb.at[:ny - 1], dsend, drecv).wait_send()
+        bulk(ydec.at[:ny - 1], dsend, drecv).wait_send()
         bulk(ht.at[:ny - 1, :hz], hsend, hrecv).wait_send()
         if ntp > 1:
             bulk(hg.at[:ny - 1, :nz - hz], fsend, frecv).wait_send()
-        for m in range(2):
-            bulk(sbuf.at[m, :ny - 1], ysend.at[m], yrecv.at[m]).wait_send()
-            bulk(tz.at[m, :nz - 1], tsend.at[m], trecv.at[m]).wait_send()
-            bulk(cz.at[m, :nz - 1], csend.at[m], crecv.at[m]).wait_send()
-            bulk(ob.at[m, :ny - 1], osend.at[m], orecv.at[m]).wait_send()
+        bulk(sbuf.at[:, :, :ny - 1], ysend, yrecv.at[0, 0]).wait_send()
+        bulk(tz.at[:, :, :nz - 1], tsend, trecv.at[0, 0]).wait_send()
+        bulk(cz.at[:, :, :nz - 1], csend, crecv.at[0, 0]).wait_send()
+        bulk(ob.at[:, :, :ny - 1], osend, orecv.at[0, 0]).wait_send()
         bulk(gath.at[:ny - 1], gsend, grecv.at[0]).wait_send()
         if halves == 2:
             pair().wait_send()
 
     tasks = [
-        (0.0, "project", project), (0.9, "columns_in", columns_in), (1.0, "stage_c1", functools.partial(stage_c, 1)),
-        (7.2, "pairs", pairs), (13.0, "state_grads", state_grads), (15.0, "drain", drain),
+        (1.0, "project", project), (1.9, "columns_in", columns_in),
+        (2.0, "stage_c1", functools.partial(stage, "stage_c", stage_c, 1)), (3.0, "key_grads", key_grads),
+        (9.6, "pairs", pairs), (15.2, "query_grads", query_grads), (15.1, "drain", drain),
         (18.2, "total_hidden", total_hidden),
     ]
-    arrive = (6.5, 8.0, 10.5, 12.0)
+    arrive = (4.5, 6.0, 8.5, 11.0)
     for c in range(tiles):
         ready = arrive[c % 4] + 7.0 * (c // 4)
         tasks.append((ready, f"multiply{c}", functools.partial(multiply, c)))
@@ -514,10 +540,10 @@
                 if fast(c) and j == 3:
                     continue
                 if fast(c):
-                    at = ready + (3.6 if j < 2 else 7.2) + 0.2 * (j % 2)
+                    at = ready + (4.0 if j < 2 else 8.0) + 0.2 * (j % 2)
                     tasks.append((at, f"step{c}{d}{j}", functools.partial(step, c, d, j)))
                 else:
-                    at = ready + 2.7 * (j + 1)
+                    at = ready + 3.5 * (j + 1)
                     tasks.append((at, f"hop{c}{d}{j}", functools.partial(hop, c, d, j)))
                 last = max(last, at)
         tasks.append((last + 0.01, f"total{c}", functools.partial(total_weight, c)))
@@ -561,7 +587,10 @@
     ny = inner_size(sp)
     nz = sp // ny
     tiles = columns // LANES
-    nr = state // nz
+    groups = 2
+    pack = tiles // groups
+    rw = state // ny
+    pr = pack * rw // nz
     rows = features // sp
     own = length // tp
     halves = 2 if tp % 2 == 0 else 1
@@ -606,16 +635,16 @@
             vm((length, heads), F32),
             vm((length, state), F32),
             vm((length, state), F32),
-            vm((2, ny, state, LANES), F32),
+            vm((2, groups, ny, pack * rw, LANES), F32),
+            vm((SUB, LANES), F32),
+            vm((2, groups, ny, pack * rw, LANES), F32),
             vm((ny, SUB, LANES), F32),
-            vm((2, ny, state, LANES), F32),
-            vm((ny, SUB, LANES), F32),
-            vm((2, nz, nr + SUB, LANES), F32),
-            vm((2, nz, nr + SUB, LANES), F32),
-            vm((2, nz, nr, LANES), F32),
-            vm((2, nz, nr, LANES), F32),
-            vm((2, ny, state, LANES), F32),
-            vm((2, ny, state, LANES), F32),
+            vm((2, groups, nz, pr + SUB, LANES), F32),
+            vm((2, groups, nz, pr + SUB, LANES), F32),
+            vm((2, groups, nz, pr, LANES), F32),
+            vm((2, groups, nz, pr, LANES), F32),
+            vm((2, groups, ny, pack * rw, LANES), F32),
+            vm((2, groups, ny, pack * rw, LANES), F32),
             vm((ny, nz, rows, length), F32),
             vm((ny, nz, rows, length), F32),
             vm((nz, rows, ny * length), BF16),
@@ -628,14 +657,14 @@
             vm((nx, own, features), F32),
             dma((6,)), dma((steps,)),
             dma, dma,
-            dma((2,)), dma((2,)),
-            dma((2,)), dma((2,)),
-            dma((2,)), dma((2,)),
-            dma((2,)), dma((2,)),
+            dma, dma((2, groups)),
+            dma, dma((2, groups)),
+            dma, dma((2, groups)),
+            dma, dma((2, groups)),
             dma, dma,
             dma, dma,
             dma, dma((tiles,)),
-            dma, dma((tiles * (nz - 1) - (4 if nz == 8 else 0),)),
+            dma, dma((tiles * (nz - 1) - (2 * 2 if nz == 8 else 0),)),
             dma, dma,
             dma, dma,
             dma((5,)),

time: 57.6 us -> 54.2 us (0.941); the launches traced: 56.8 us -> 54 us
  Pallas kernels: 56.1 us -> 53.4 us
    pallas_call x1, Pallas kernels: 54.4 us -> 51.7 us  [per_device(): pl.pallas_call(functools.partial(mixer_kernel, ny, nz, tp), out_shape=(ja...]
where the time goes in v5:
time: 54.2 us; the launch traced here: 54 us
  Pallas kernels  53.4 us (99%)
  between operations  0.64 us (1%)
    pallas_call x1, Pallas kernels, per_device(): pl.pallas_call(functools.partial(mixer_kernel, ny, nz, tp), out_shape=(ja...  51.7 us
    pallas_call x1, Pallas kernels, per_device(): pl.pallas_call(finish_kernel, out_shape=tuple((jax.ShapeDtypeStruct(o.sha...  1.72 us

profile of v5, /device:TPU:2, one launch (start us, length us, event | category | flops | bytes accessed | tf_op | source)
XLA Modules:
  0.0 54.0 jit_solution(10019153916740245242)
XLA Ops:
  0.6 51.7 %mixer_backward.1 = (bf16[128,128]{1,0:T(8,128)(2,1)}, bf16[128,128]{1,0:T(8,128)(2,1)}, f32[8,128]{1,0:T(8,128)}, bf16[16,2048]{1,0:T(8,128)(2,1)}, f32[64,512]{1,0:T(8,128)}) custom-call(bf16[128,2048]{1,0:T(8,128)(2,1)} %hid_hbm.1, bf16[2048,512]{1,0:T(8,128)(2,1)} %w_hbm.1, bf16[128,128]{1,0:T(8,128)(2,1)} %bitcast.11, bf16[128,128]{1,0:T(8,128)(2,1)} %bitcast.12, ...), custom_call_target="tpu_custom_call" | custom-call | tf_op jit(solution)/shard_map/mixer_backward/pallas_call | solution.py:602
  52.3 1.7 %write_out.1 = (bf16[128,128]{1,0:T(8,128)(2,1)}, bf16[128,128]{1,0:T(8,128)(2,1)}, f32[8,128]{1,0:T(8,128)}, bf16[16,2048]{1,0:T(8,128)(2,1)}, f32[64,512]{1,0:T(8,128)}) custom-call(bf16[128,128]{1,0:T(8,128)(2,1)} %get-tuple-element.15.refs_0_, bf16[128,128]{1,0:T(8,128)(2,1)} %get-tuple-element.16.refs_1_, f32[8,128]{1,0:T(8,128)} %get-tuple-element.17.refs_2_, ...), custom_call_target="tpu_custom_call" | custom-call | tf_op jit(solution)/shard_map/write_out/pallas_call | solution.py:678

commit v6 on v5

--- a/solution.py
+++ b/solution.py
@@ -47,7 +47,7 @@
                  gk_out, gq_out, gd_out, gh_out, gw_out,
                  gk_ref, gq_ref, gd_ref, gh_ref, gw_ref, hid, wt, key, qry, pre, rate_ref, cott, cot,
                  ecot, tend, xval, damp, gvloc, gvb, kgs, rows8, cols8, gkl, gql,
-                 sbuf, decb, ybuf, ydec, tz, zbuf, cz, zcar, ob, scr, ht, hg, hcol,
+                 sbuf, decb, ybuf, ydec, tz, zbuf, cz, zcar, crow, ob, scr, ht, hg, hcol,
                  gath, part, ring, ghp, pland, red, xland,
                  insem, wsem, dsend, drecv, ysend, yrecv, tsend, trecv, csend, crecv, osend, orecv,
                  hsend, hrecv, fsend, frecv, gsend, grecv, rsend, rrecv, psend, precv, xsend, xrecv, outsem):
@@ -303,10 +303,9 @@
             prod = ydec[0, q:q + 1]
             for yy in range(1, ny):
                 prod = prod * ydec[yy, q:q + 1]
-            prod = jnp.broadcast_to(prod, (SUB, LANES))
             for k in range(rw // pr):
                 tz[m, g, i * (rw // pr) + k, :pr] = run[k * pr:(k + 1) * pr]
-                tz[m, g, i * (rw // pr) + k, pr:] = prod
+                tz[m, g, i * (rw // pr) + k, pr:pr + 1] = prod
         for dz in sorted(range(1, nz), key=lambda dz: -min(dz, nz - dz)):
             tcopy(m, g, dz).start()
         zbuf[m, g, z] = tz[m, g, z]
@@ -323,7 +322,9 @@
 
     def stage_c(m, g):
         bulk(zcar.at[m, g, :nz - 1], csend, crecv.at[m, g]).wait_recv()
-        carry = zcar[m, g].reshape(pack * rw, LANES)
+        for k in range(nz):
+            crow[m, g, k * pr:(k + 1) * pr] = zcar[m, g, k]
+        carry = crow[m, g]
         for i in range(pack):
             q, at = g * pack + i, slice(i * rw, (i + 1) * rw)
             now = carry[at]
@@ -587,7 +588,7 @@
     ny = inner_size(sp)
     nz = sp // ny
     tiles = columns // LANES
-    groups = 2
+    groups = tiles
     pack = tiles // groups
     rw = state // ny
     pr = pack * rw // nz
@@ -639,10 +640,11 @@
             vm((SUB, LANES), F32),
             vm((2, groups, ny, pack * rw, LANES), F32),
             vm((ny, SUB, LANES), F32),
-            vm((2, groups, nz, pr + SUB, LANES), F32),
-            vm((2, groups, nz, pr + SUB, LANES), F32),
+            vm((2, groups, nz, -(-(pr + 1) // SUB) * SUB, LANES), F32),
+            vm((2, groups, nz, -(-(pr + 1) // SUB) * SUB, LANES), F32),
             vm((2, groups, nz, pr, LANES), F32),
             vm((2, groups, nz, pr, LANES), F32),
+            vm((2, groups, pack * rw, LANES), F32),
             vm((2, groups, ny, pack * rw, LANES), F32),
             vm((2, groups, ny, pack * rw, LANES), F32),
             vm((ny, nz, rows, length), F32),

time: 54.2 us -> 53.4 us (0.985)
  Pallas kernels: 53.4 us -> 52.5 us
    pallas_call x1, Pallas kernels: 51.7 us -> 50.8 us  [per_device(): pl.pallas_call(functools.partial(mixer_kernel, ny, nz, tp), out_shape=(ja...]
where the time goes in v6:
time: 53.4 us; the launch traced here: 53.2 us
  Pallas kernels  52.5 us (98%)
  between operations  0.64 us (1%)
    pallas_call x1, Pallas kernels, per_device(): pl.pallas_call(functools.partial(mixer_kernel, ny, nz, tp), out_shape=(ja...  50.8 us
    pallas_call x1, Pallas kernels, per_device(): pl.pallas_call(finish_kernel, out_shape=tuple((jax.ShapeDtypeStruct(o.sha...  1.72 us

profile of v6, /device:TPU:2, one launch (start us, length us, event | category | flops | bytes accessed | tf_op | source)
XLA Modules:
  0.0 53.2 jit_solution(7487053318000949377)
XLA Ops:
  0.6 50.8 %mixer_backward.1 = (bf16[128,128]{1,0:T(8,128)(2,1)}, bf16[128,128]{1,0:T(8,128)(2,1)}, f32[8,128]{1,0:T(8,128)}, bf16[16,2048]{1,0:T(8,128)(2,1)}, f32[64,512]{1,0:T(8,128)}) custom-call(bf16[128,2048]{1,0:T(8,128)(2,1)} %hid_hbm.1, bf16[2048,512]{1,0:T(8,128)(2,1)} %w_hbm.1, bf16[128,128]{1,0:T(8,128)(2,1)} %bitcast.11, bf16[128,128]{1,0:T(8,128)(2,1)} %bitcast.12, ...), custom_call_target="tpu_custom_call" | custom-call | tf_op jit(solution)/shard_map/mixer_backward/pallas_call | solution.py:603
  51.5 1.7 %write_out.1 = (bf16[128,128]{1,0:T(8,128)(2,1)}, bf16[128,128]{1,0:T(8,128)(2,1)}, f32[8,128]{1,0:T(8,128)}, bf16[16,2048]{1,0:T(8,128)(2,1)}, f32[64,512]{1,0:T(8,128)}) custom-call(bf16[128,128]{1,0:T(8,128)(2,1)} %get-tuple-element.15.refs_0_, bf16[128,128]{1,0:T(8,128)(2,1)} %get-tuple-element.16.refs_1_, f32[8,128]{1,0:T(8,128)} %get-tuple-element.17.refs_2_, ...), custom_call_target="tpu_custom_call" | custom-call | tf_op jit(solution)/shard_map/write_out/pallas_call | solution.py:680

commit v7 on v6

--- a/solution.py
+++ b/solution.py
@@ -76,6 +76,12 @@
     ydev = [z * ny + (y + dy) % ny for dy in range(ny)]
     zdev = [((z + dz) % nz) * ny + y for dz in range(nz)]
 
+    barrier = pltpu.get_barrier_semaphore()
+    for dev in [zdev[dz] for dz in sorted(range(1, nz), key=lambda dz: -min(dz, nz - dz))] + ydev[1:]:
+        pl.semaphore_signal(barrier, inc=1, device_id={"sp": dev}, device_id_type=MESH)
+    for dt in range(1, ntp):
+        pl.semaphore_signal(barrier, inc=1, device_id={"tp": (mine + dt) % ntp}, device_id_type=MESH)
+
     small = [
         pltpu.make_async_copy(pre_hbm, pre, insem.at[0]),
         pltpu.make_async_copy(rate_hbm, rate_ref, insem.at[4]),
@@ -104,12 +110,6 @@
         at = pl.ds(c * LANES, LANES)
         outs.append(pltpu.make_async_copy(gw_ref.at[:, at], gw_out.at[:, at], outsem.at[4]))
 
-    barrier = pltpu.get_barrier_semaphore()
-    for dev in ydev[1:] + zdev[1:]:
-        pl.semaphore_signal(barrier, inc=1, device_id={"sp": dev}, device_id_type=MESH)
-    for dt in range(1, ntp):
-        pl.semaphore_signal(barrier, inc=1, device_id={"tp": (mine + dt) % ntp}, device_id_type=MESH)
-
     def dcopy(dy, arrive=False):
         slot = (y + dy) % ny if arrive else y
         return remote(decb, ydec.at[slot], dsend, drecv, "sp", ydev[dy])
@@ -177,27 +177,23 @@
         )
 
     def scopy(c, d, j):
-        if j == 0:
-            src, hops = part.at[c, ahead(4, d)], 2
-        elif j == 1:
-            src, hops = part.at[c, ahead(3, d)], 2
-        elif j == 2:
-            src, hops = (ring.at[d, c, 0] if reach(c, d) == 4 else part.at[c, ahead(2, d)]), 2
-        else:
-            src, hops = ring.at[d, c, 1], 1
+        src, hops = (part.at[c, ahead(j + 2, d)], j + 1) if j < 3 else (ring.at[d, c, 0], 1)
         return remote(
             src, ring.at[d, c, j], rsend, rrecv.at[slot_at(c, d, j)], "sp", zdev[hops if d == 0 else nz - hops]
         )
 
     def slots(c, d):
         if fast(c):
-            return (0, 1, 2, 3) if reach(c, d) == 4 else (1, 2, 3)
+            return tuple(range(reach(c, d) - 1)) + (3,)
         return tuple(range(reach(c, d)))
 
-    ring_slots = sorted({(c, d, min(j, 2) if fast(c) else j) for c in range(tiles) for d in range(2) for j in slots(c, d)})
+    def step_of(c, j):
+        return j // 3 if fast(c) else j
+
+    ring_slots = sorted({(c, d, step_of(c, j)) for c in range(tiles) for d in range(2) for j in slots(c, d)})
 
     def slot_at(c, d, j):
-        return ring_slots.index((c, d, min(j, 2) if fast(c) else j))
+        return ring_slots.index((c, d, step_of(c, j)))
 
     def bulk(ref, send, recv):
         return remote(ref, ref, send, recv, "sp", ydev[1])
@@ -420,9 +416,8 @@
         part[c] = nn(hcol[...].reshape(nz * rows, ny * length), block).reshape(nz, rows, LANES)
         for d in range(2):
             if fast(c):
-                for j in slots(c, d):
-                    if j < 2 or (j == 2 and reach(c, d) == 3):
-                        scopy(c, d, j).start()
+                for j in reversed(range(reach(c, d) - 1)):
+                    scopy(c, d, j).start()
             elif reach(c, d) > 0:
                 rcopy(c, d, 0).start()
 
@@ -434,18 +429,22 @@
             rcopy(c, d, j + 1).start()
 
     def step(c, d, j):
-        if j == 2:
-            bulk(ring.at[d, c, 2:4], rsend, rrecv.at[slot_at(c, d, 2)]).wait_recv()
+        if j == 3:
+            scopy(c, d, 3).wait_recv()
         else:
-            scopy(c, d, j).wait_recv()
-            ring[d, c, j] = ring[d, c, j] + part[c, ahead(2 - j, d)]
-            scopy(c, d, j + 2).start()
+            count = reach(c, d) - 1
+            bulk(ring.at[d, c, :count], rsend, rrecv.at[slot_at(c, d, 0)]).wait_recv()
+            total = part[c, ahead(1, d)]
+            for k in range(count):
+                total = total + ring[d, c, k]
+            ring[d, c, 0] = total
+            scopy(c, d, 3).start()
 
     def total_weight(c):
         total = part[c, z]
         for d in range(2):
             if fast(c):
-                total = total + (ring[d, c, 2] + ring[d, c, 3])
+                total = total + ring[d, c, 3]
             elif reach(c, d) > 0:
                 total = total + ring[d, c, reach(c, d) - 1]
         gw_ref[:, tile(c)] = total
@@ -527,8 +526,8 @@
 
     tasks = [
         (1.0, "project", project), (1.9, "columns_in", columns_in),
-        (2.0, "stage_c1", functools.partial(stage, "stage_c", stage_c, 1)), (3.0, "key_grads", key_grads),
-        (9.6, "pairs", pairs), (15.2, "query_grads", query_grads), (15.1, "drain", drain),
+        (6.1, "stage_c1", functools.partial(stage, "stage_c", stage_c, 1)), (3.0, "key_grads", key_grads),
+        (9.6, "pairs", pairs), (17.9, "query_grads", query_grads), (18.0, "drain", drain),
         (18.2, "total_hidden", total_hidden),
     ]
     arrive = (4.5, 6.0, 8.5, 11.0)
@@ -538,10 +537,10 @@
         last = ready
         for d in range(2):
             for j in slots(c, d):
-                if fast(c) and j == 3:
+                if fast(c) and j not in (0, 3):
                     continue
                 if fast(c):
-                    at = ready + (4.0 if j < 2 else 8.0) + 0.2 * (j % 2)
+                    at = ready + (4.0 if j < 3 else 8.0) + 0.1 * d
                     tasks.append((at, f"step{c}{d}{j}", functools.partial(step, c, d, j)))
                 else:
                     at = ready + 3.5 * (j + 1)
@@ -666,7 +665,7 @@
             dma, dma,
             dma, dma,
             dma, dma((tiles,)),
-            dma, dma((tiles * (nz - 1) - (2 * 2 if nz == 8 else 0),)),
+            dma, dma((tiles * (nz - 1) - (3 * 2 if nz == 8 else 0),)),
             dma, dma,
             dma, dma,
             dma((5,)),

time: 53.4 us -> 53.1 us (level)
  Pallas kernels: 52.5 us -> 51.9 us
    pallas_call x1, Pallas kernels: 50.8 us -> 50.2 us  [per_device(): pl.pallas_call(functools.partial(mixer_kernel, ny, nz, tp), out_shape=(ja...]
where the time goes in v7:
time: 53.1 us; the launch traced here: 52.5 us
  Pallas kernels  51.9 us (98%)
  between operations  0.64 us (1%)
    pallas_call x1, Pallas kernels, per_device(): pl.pallas_call(functools.partial(mixer_kernel, ny, nz, tp), out_shape=(ja...  50.2 us
    pallas_call x1, Pallas kernels, per_device(): pl.pallas_call(finish_kernel, out_shape=tuple((jax.ShapeDtypeStruct(o.sha...  1.72 us

profile of v7, /device:TPU:2, one launch (start us, length us, event | category | flops | bytes accessed | tf_op | source)
XLA Modules:
  0.0 52.5 jit_solution(16615719144975074360)
XLA Ops:
  0.6 50.2 %mixer_backward.1 = (bf16[128,128]{1,0:T(8,128)(2,1)}, bf16[128,128]{1,0:T(8,128)(2,1)}, f32[8,128]{1,0:T(8,128)}, bf16[16,2048]{1,0:T(8,128)(2,1)}, f32[64,512]{1,0:T(8,128)}) custom-call(bf16[128,2048]{1,0:T(8,128)(2,1)} %hid_hbm.1, bf16[2048,512]{1,0:T(8,128)(2,1)} %w_hbm.1, bf16[128,128]{1,0:T(8,128)(2,1)} %bitcast.11, bf16[128,128]{1,0:T(8,128)(2,1)} %bitcast.12, ...), custom_call_target="tpu_custom_call" | custom-call | tf_op jit(solution)/shard_map/mixer_backward/pallas_call | solution.py:602
  50.8 1.7 %write_out.1 = (bf16[128,128]{1,0:T(8,128)(2,1)}, bf16[128,128]{1,0:T(8,128)(2,1)}, f32[8,128]{1,0:T(8,128)}, bf16[16,2048]{1,0:T(8,128)(2,1)}, f32[64,512]{1,0:T(8,128)}) custom-call(bf16[128,128]{1,0:T(8,128)(2,1)} %get-tuple-element.15.refs_0_, bf16[128,128]{1,0:T(8,128)(2,1)} %get-tuple-element.16.refs_1_, f32[8,128]{1,0:T(8,128)} %get-tuple-element.17.refs_2_, ...), custom_call_target="tpu_custom_call" | custom-call | tf_op jit(solution)/shard_map/write_out/pallas_call | solution.py:679

commit v8 on v7

--- a/solution.py
+++ b/solution.py
@@ -365,8 +365,6 @@
 
     stage("stage_z", stage_z, 0)
 
-    stage("stage_y", stage_y, 1)
-
     dsum = jnp.zeros((length, length), F32)
     for q in range(tiles):
         vt = vals[:, tile(q)]
@@ -384,12 +382,12 @@
 
     stage("stage_c", stage_c, 0)
 
+    stage("stage_y", stage_y, 1)
+
     hi, lo = split(dsum)
     gkl[...] = nn(hi, qry[...]) + nn(lo, qry[...])
     hi, lo = split(dsum.T)
     gql[...] = nn(hi, key[...]) + nn(lo, key[...])
-    stage("stage_z", stage_z, 1)
-
     for g in range(groups):
         with jax.named_scope(f"wait_o0{g}"):
             bulk(scr.at[0, g, :ny - 1], osend, orecv.at[0, g]).wait_recv()
@@ -402,6 +400,8 @@
             gath[y, q] = gb.astype(F32)
             for dy in sorted(range(1, ny), key=lambda dy: -min(dy, ny - dy)):
                 gcopy(q, dy).start()
+
+    stage("stage_z", stage_z, 1)
 
     def columns_in():
         if ntp > 1:

time: 53.1 us -> 52.9 us (level)
  no operation moved by 1% of the time
where the time goes in v8:
time: 52.9 us; the launch traced here: 52.7 us
  Pallas kernels  52.1 us (98%)
  between operations  0.64 us (1%)
    pallas_call x1, Pallas kernels, per_device(): pl.pallas_call(functools.partial(mixer_kernel, ny, nz, tp), out_shape=(ja...  50.4 us
    pallas_call x1, Pallas kernels, per_device(): pl.pallas_call(finish_kernel, out_shape=tuple((jax.ShapeDtypeStruct(o.sha...  1.72 us

profile of v8, /device:TPU:2, one launch (start us, length us, event | category | flops | bytes accessed | tf_op | source)
XLA Modules:
  0.0 52.7 jit_solution(18171752630318092252)
XLA Ops:
  0.6 50.4 %mixer_backward.1 = (bf16[128,128]{1,0:T(8,128)(2,1)}, bf16[128,128]{1,0:T(8,128)(2,1)}, f32[8,128]{1,0:T(8,128)}, bf16[16,2048]{1,0:T(8,128)(2,1)}, f32[64,512]{1,0:T(8,128)}) custom-call(bf16[128,2048]{1,0:T(8,128)(2,1)} %hid_hbm.1, bf16[2048,512]{1,0:T(8,128)(2,1)} %w_hbm.1, bf16[128,128]{1,0:T(8,128)(2,1)} %bitcast.11, bf16[128,128]{1,0:T(8,128)(2,1)} %bitcast.12, ...), custom_call_target="tpu_custom_call" | custom-call | tf_op jit(solution)/shard_map/mixer_backward/pallas_call | solution.py:602
  51.0 1.7 %write_out.1 = (bf16[128,128]{1,0:T(8,128)(2,1)}, bf16[128,128]{1,0:T(8,128)(2,1)}, f32[8,128]{1,0:T(8,128)}, bf16[16,2048]{1,0:T(8,128)(2,1)}, f32[64,512]{1,0:T(8,128)}) custom-call(bf16[128,128]{1,0:T(8,128)(2,1)} %get-tuple-element.15.refs_0_, bf16[128,128]{1,0:T(8,128)(2,1)} %get-tuple-element.16.refs_1_, f32[8,128]{1,0:T(8,128)} %get-tuple-element.17.refs_2_, ...), custom_call_target="tpu_custom_call" | custom-call | tf_op jit(solution)/shard_map/write_out/pallas_call | solution.py:679

commit v9 on v8

--- a/solution.py
+++ b/solution.py
@@ -116,19 +116,19 @@
 
     def ycopy(m, g, dy):
         there = (y + dy) % ny
-        return remote(sbuf.at[m, g, there], ybuf.at[m, g, y], ysend, yrecv.at[m, g], "sp", ydev[dy])
+        return remote(sbuf.at[m, g, there], ybuf.at[m, g, y], ysend, yrecv.at[g + m * (groups - g)], "sp", ydev[dy])
 
     def tcopy(m, g, dz):
         there = (z + dz) % nz
-        return remote(tz.at[m, g, there], zbuf.at[m, g, z], tsend, trecv.at[m, g], "sp", zdev[dz])
+        return remote(tz.at[m, g, there], zbuf.at[m, g, z], tsend, trecv.at[g + m * (groups - g)], "sp", zdev[dz])
 
     def ccopy(m, g, dz):
         there = (z + dz) % nz
-        return remote(cz.at[m, g, there], zcar.at[m, g, z], csend, crecv.at[m, g], "sp", zdev[dz])
+        return remote(cz.at[m, g, there], zcar.at[m, g, z], csend, crecv.at[g + m * (groups - g)], "sp", zdev[dz])
 
     def ocopy(m, g, dy):
         there = (y + dy) % ny
-        return remote(ob.at[m, g, there], scr.at[m, g, y], osend, orecv.at[m, g], "sp", ydev[dy])
+        return remote(ob.at[m, g, there], scr.at[m, g, y], osend, orecv.at[g + m * (groups - g)], "sp", ydev[dy])
 
     def section(k):
         return pl.ds(pl.multiple_of(k * hz, hz), hz)
@@ -289,7 +289,10 @@
     def stage_y(m, g):
         if m == 0 and g == 0:
             bulk(ydec.at[:ny - 1], dsend, drecv).wait_recv()
-        bulk(ybuf.at[m, g, :ny - 1], ysend, yrecv.at[m, g]).wait_recv()
+        if m == 0:
+            bulk(ybuf.at[0, g, :ny - 1], ysend, yrecv.at[g]).wait_recv()
+        elif g == 0:
+            bulk(ybuf.at[1, :, :ny - 1], ysend, yrecv.at[groups]).wait_recv()
         order = scan_order(m, ny)
         for i in range(pack):
             q, at = g * pack + i, slice(i * rw, (i + 1) * rw)
@@ -307,7 +310,10 @@
         zbuf[m, g, z] = tz[m, g, z]
 
     def stage_z(m, g):
-        bulk(zbuf.at[m, g, :nz - 1], tsend, trecv.at[m, g]).wait_recv()
+        if m == 0:
+            bulk(zbuf.at[0, g, :nz - 1], tsend, trecv.at[g]).wait_recv()
+        elif g == 0:
+            bulk(zbuf.at[1, :, :nz - 1], tsend, trecv.at[groups]).wait_recv()
         run = jnp.zeros((pr, LANES), F32)
         for zz in scan_order(m, nz):
             cz[m, g, zz] = run
@@ -317,7 +323,10 @@
         zcar[m, g, z] = cz[m, g, z]
 
     def stage_c(m, g):
-        bulk(zcar.at[m, g, :nz - 1], csend, crecv.at[m, g]).wait_recv()
+        if m == 0:
+            bulk(zcar.at[0, g, :nz - 1], csend, crecv.at[g]).wait_recv()
+        elif g == 0:
+            bulk(zcar.at[1, :, :nz - 1], csend, crecv.at[groups]).wait_recv()
         for k in range(nz):
             crow[m, g, k * pr:(k + 1) * pr] = zcar[m, g, k]
         carry = crow[m, g]
@@ -390,7 +399,7 @@
     gql[...] = nn(hi, key[...]) + nn(lo, key[...])
     for g in range(groups):
         with jax.named_scope(f"wait_o0{g}"):
-            bulk(scr.at[0, g, :ny - 1], osend, orecv.at[0, g]).wait_recv()
+            bulk(scr.at[0, g, :ny - 1], osend, orecv.at[g]).wait_recv()
         for q in range(g * pack, (g + 1) * pack):
             hi, lo = split(state_tile(0, q))
             kg = nn(key[...], hi) + nn(key[...], lo)
@@ -482,8 +491,7 @@
 
     def query_grads():
         with jax.named_scope("wait_o1"):
-            for g in range(groups):
-                bulk(scr.at[1, g, :ny - 1], osend, orecv.at[1, g]).wait_recv()
+            bulk(scr.at[1, :, :ny - 1], osend, orecv.at[groups]).wait_recv()
         gq = gql[...]
         into, through = [], []
         for q in range(tiles):
@@ -516,10 +524,10 @@
         bulk(ht.at[:ny - 1, :hz], hsend, hrecv).wait_send()
         if ntp > 1:
             bulk(hg.at[:ny - 1, :nz - hz], fsend, frecv).wait_send()
-        bulk(sbuf.at[:, :, :ny - 1], ysend, yrecv.at[0, 0]).wait_send()
-        bulk(tz.at[:, :, :nz - 1], tsend, trecv.at[0, 0]).wait_send()
-        bulk(cz.at[:, :, :nz - 1], csend, crecv.at[0, 0]).wait_send()
-        bulk(ob.at[:, :, :ny - 1], osend, orecv.at[0, 0]).wait_send()
+        bulk(sbuf.at[:, :, :ny - 1], ysend, yrecv.at[0]).wait_send()
+        bulk(tz.at[:, :, :nz - 1], tsend, trecv.at[0]).wait_send()
+        bulk(cz.at[:, :, :nz - 1], csend, crecv.at[0]).wait_send()
+        bulk(ob.at[:, :, :ny - 1], osend, orecv.at[0]).wait_send()
         bulk(gath.at[:ny - 1], gsend, grecv.at[0]).wait_send()
         if halves == 2:
             pair().wait_send()
@@ -658,10 +666,10 @@
             vm((nx, own, features), F32),
             dma((6,)), dma((steps,)),
             dma, dma,
-            dma, dma((2, groups)),
-            dma, dma((2, groups)),
-            dma, dma((2, groups)),
-            dma, dma((2, groups)),
+            dma, dma((groups + 1,)),
+            dma, dma((groups + 1,)),
+            dma, dma((groups + 1,)),
+            dma, dma((groups + 1,)),
             dma, dma,
             dma, dma,
             dma, dma((tiles,)),

time: 52.9 us -> 52.7 us (level)
  no operation moved by 1% of the time
where the time goes in v9:
time: 52.7 us; the launch traced here: 52.6 us
  Pallas kernels  52 us (99%)
  between operations  0.64 us (1%)
    pallas_call x1, Pallas kernels, per_device(): pl.pallas_call(functools.partial(mixer_kernel, ny, nz, tp), out_shape=(ja...  50.2 us
    pallas_call x1, Pallas kernels, per_device(): pl.pallas_call(finish_kernel, out_shape=tuple((jax.ShapeDtypeStruct(o.sha...  1.72 us

profile of v9, /device:TPU:2, one launch (start us, length us, event | category | flops | bytes accessed | tf_op | source)
XLA Modules:
  0.0 52.6 jit_solution(9467648519378960624)
XLA Ops:
  0.6 50.2 %mixer_backward.1 = (bf16[128,128]{1,0:T(8,128)(2,1)}, bf16[128,128]{1,0:T(8,128)(2,1)}, f32[8,128]{1,0:T(8,128)}, bf16[16,2048]{1,0:T(8,128)(2,1)}, f32[64,512]{1,0:T(8,128)}) custom-call(bf16[128,2048]{1,0:T(8,128)(2,1)} %hid_hbm.1, bf16[2048,512]{1,0:T(8,128)(2,1)} %w_hbm.1, bf16[128,128]{1,0:T(8,128)(2,1)} %bitcast.11, bf16[128,128]{1,0:T(8,128)(2,1)} %bitcast.12, ...), custom_call_target="tpu_custom_call" | custom-call | tf_op jit(solution)/shard_map/mixer_backward/pallas_call | solution.py:610
  50.9 1.7 %write_out.1 = (bf16[128,128]{1,0:T(8,128)(2,1)}, bf16[128,128]{1,0:T(8,128)(2,1)}, f32[8,128]{1,0:T(8,128)}, bf16[16,2048]{1,0:T(8,128)(2,1)}, f32[64,512]{1,0:T(8,128)}) custom-call(bf16[128,128]{1,0:T(8,128)(2,1)} %get-tuple-element.15.refs_0_, bf16[128,128]{1,0:T(8,128)(2,1)} %get-tuple-element.16.refs_1_, f32[8,128]{1,0:T(8,128)} %get-tuple-element.17.refs_2_, ...), custom_call_target="tpu_custom_call" | custom-call | tf_op jit(solution)/shard_map/write_out/pallas_call | solution.py:687

commit v10 on v9

--- a/solution.py
+++ b/solution.py
@@ -572,14 +572,23 @@
 def finish_kernel(*refs):
     count = (len(refs) - 1) // 3
     ins, outs, held, sems = refs[:count], refs[count:2 * count], refs[2 * count:3 * count], refs[-1]
-    loads = [pltpu.make_async_copy(ins[k], held[k], sems.at[0, k]) for k in range(count)]
-    stores = [pltpu.make_async_copy(held[k], outs[k], sems.at[1, k]) for k in range(count)]
-    for load in loads:
+    moves = []
+    for k in range(count):
+        rows = ins[k].shape[0]
+        parts = 4 if rows * ins[k].shape[1] > 20000 and rows % (16 * 4) == 0 else 1
+        for i in range(parts):
+            at = pl.ds(i * (rows // parts), rows // parts)
+            n = len(moves)
+            moves.append((
+                pltpu.make_async_copy(ins[k].at[at], held[k].at[at], sems.at[0, n]),
+                pltpu.make_async_copy(held[k].at[at], outs[k].at[at], sems.at[1, n]),
+            ))
+    for load, _ in moves:
         load.start()
-    for load, store in zip(loads, stores):
+    for load, store in moves:
         load.wait()
         store.start()
-    for store in stores:
+    for _, store in moves:
         store.wait()
 
 
@@ -689,7 +698,7 @@
         out_shape=tuple(jax.ShapeDtypeStruct(o.shape, o.dtype) for o in outs),
         in_specs=[HBM] * 5,
         out_specs=(HBM,) * 5,
-        scratch_shapes=[vm(o.shape, o.dtype) for o in outs] + [dma((2, 5))],
+        scratch_shapes=[vm(o.shape, o.dtype) for o in outs] + [dma((2, 8))],
         compiler_params=pltpu.CompilerParams(vmem_limit_bytes=LIMIT),
         name="write_out",
     )(*outs)

time: 52.7 us -> 52.7 us (level)
  no operation moved by 1% of the time
where the time goes in v10:
time: 52.7 us; the launch traced here: 52.6 us
  Pallas kernels  51.9 us (98%)
  between operations  0.64 us (1%)
    pallas_call x1, Pallas kernels, per_device(): pl.pallas_call(functools.partial(mixer_kernel, ny, nz, tp), out_shape=(ja...  50.2 us
    pallas_call x1, Pallas kernels, per_device(): pl.pallas_call(finish_kernel, out_shape=tuple((jax.ShapeDtypeStruct(o.sha...  1.69 us

profile of v10, /device:TPU:2, one launch (start us, length us, event | category | flops | bytes accessed | tf_op | source)
XLA Modules:
  0.0 52.6 jit_solution(3868327285258802508)
XLA Ops:
  0.6 50.2 %mixer_backward.1 = (bf16[128,128]{1,0:T(8,128)(2,1)}, bf16[128,128]{1,0:T(8,128)(2,1)}, f32[8,128]{1,0:T(8,128)}, bf16[16,2048]{1,0:T(8,128)(2,1)}, f32[64,512]{1,0:T(8,128)}) custom-call(bf16[128,2048]{1,0:T(8,128)(2,1)} %hid_hbm.1, bf16[2048,512]{1,0:T(8,128)(2,1)} %w_hbm.1, bf16[128,128]{1,0:T(8,128)(2,1)} %bitcast.11, bf16[128,128]{1,0:T(8,128)(2,1)} %bitcast.12, ...), custom_call_target="tpu_custom_call" | custom-call | tf_op jit(solution)/shard_map/mixer_backward/pallas_call | solution.py:619
  50.9 1.7 %write_out.1 = (bf16[128,128]{1,0:T(8,128)(2,1)}, bf16[128,128]{1,0:T(8,128)(2,1)}, f32[8,128]{1,0:T(8,128)}, bf16[16,2048]{1,0:T(8,128)(2,1)}, f32[64,512]{1,0:T(8,128)}) custom-call(bf16[128,128]{1,0:T(8,128)(2,1)} %get-tuple-element.15.refs_0_, bf16[128,128]{1,0:T(8,128)(2,1)} %get-tuple-element.16.refs_1_, f32[8,128]{1,0:T(8,128)} %get-tuple-element.17.refs_2_, ...), custom_call_target="tpu_custom_call" | custom-call | tf_op jit(solution)/shard_map/write_out/pallas_call | solution.py:696
